TPU v7x, 32 devices: a whole 2x2x4 slice. The times are simulated.
32 devices in a mesh: sp: 8 (over z, y), tp: 4 (over x, core).
Axes of the slice: x: 2, y: 2, z: 4, core: 2. Of those that a mesh axis runs over, the one named last changes fastest.
Arguments:
- queries: bfloat16 [4096, 1024], P('sp', 'tp'), may hold values from -6 to 6
- keys: bfloat16 [4096, 1024], P('sp', 'tp'), may hold values from -6 to 6
- values: bfloat16 [4096, 1024], P('sp', 'tp'), may hold values from -6 to 6
- cum_gate: float32 [4096, 16], P('sp', 'tp'), as said below
- documents: int32 [4096], P('sp'), may hold values from 0 to 3, never falling along the last dimension, each value on 1 to 2048 neighbouring positions
- head_gain: float32 [1024], P('tp'), may hold values from 0.1 to 1.9
- out_weight: bfloat16 [1024, 2048], replicated, may hold values from -0.1875 to 0.1875
- resid: bfloat16 [4096, 2048], P(('sp', 'tp')), may hold values from -6 to 6
- norm_gain: float32 [2048], replicated, may hold values from 0.1 to 1.9
- routes: int32 [4096, 2], P(('sp', 'tp')), may hold values from 0 to 7, all different within a row; in each aligned block of 128 rows (0 to 127, 128 to 255, ...) at most 64 rows name the same one
- route_weights: float32 [4096, 2], P(('sp', 'tp')), may hold values from 0.25 to 1
- w_gate: bfloat16 [8, 2048, 3584], P('sp', None, 'tp'), may hold values from -0.125 to 0.125
- w_up: bfloat16 [8, 2048, 3584], P('sp', None, 'tp'), may hold values from -0.125 to 0.125
- w_down: bfloat16 [8, 3584, 2048], P('sp', 'tp'), may hold values from -0.09375 to 0.09375
Outputs:
- mixed: bfloat16 [4096, 2048], P(('sp', 'tp'))
Inputs may be any that keep to these rules, and one draw needn't show every extreme that they name: `cum_gate`: along the positions each head's values never rise. `documents`: document numbers never fall along the positions. `routes`: the 2 experts of a row differ. In each aligned block of 128 rows no expert is named more than 64 times; in some blocks an expert is named exactly 64 times.
All inputs are finite; a program needn't handle non-finite values.
Results may differ from a plain program's by a relative error of at most 0.015.
Values may be sent and summed in bfloat16 or wider, within the bound.
No kernel may reach another device: no remote copies, remote signals or barrier semaphores. Data moves between devices by JAX's collectives and lax.ppermute only.
A program may use at most 128 MiB of HBM per device.

v0:
```python
import jax
import jax.numpy as jnp
from jax import lax
from jax.experimental import pallas as pl
from jax.experimental.pallas import tpu as pltpu
from jax.sharding import PartitionSpec as P

EPS = 1e-06
LOG2E = 1.4426950408889634
NEG = -1e30


def bf16_parts(x):
    hi = lax.reduce_precision(x, 8, 7)
    rest = x - hi
    mid = lax.reduce_precision(rest, 8, 7)
    low = rest - mid
    return [part.astype(jnp.bfloat16) for part in (hi, mid, low)]


def attention_kernel(tokens, heads, head_size, tile, sources, *refs):
    valid_ref, docs_ref, q_ref, meta_ref, gain_ref = refs[:5]
    kv_refs = refs[5 : 5 + 2 * sources]
    mine_ref, other_ref = refs[5 + 2 * sources : 7 + 2 * sources]
    m_ref, l_ref, acc_ref = refs[7 + 2 * sources :]
    width = heads * head_size
    halves = tokens // width
    rows = tokens // head_size
    score_scale = head_size ** (-0.5) * LOG2E
    lane = lax.broadcasted_iota(jnp.int32, (1, width), 1)
    in_head = [(lane >= h * head_size) & (lane < (h + 1) * head_size) for h in range(heads)]

    def spread(parts):
        full = jnp.broadcast_to(parts[0], (tile, width))
        for h in range(1, heads):
            full = jnp.where(in_head[h], parts[h], full)
        return full

    def q_tile(step, carry):
        row0 = pl.multiple_of(step * tile, tile)
        q = q_ref[pl.ds(row0, tile), :]
        meta = meta_ref[pl.ds(row0, tile), :]
        q_doc = meta[:, heads : heads + 1]
        first_doc = docs_ref[row0].astype(jnp.float32)

        def visit(source):
            k_ref, v_ref = kv_refs[2 * source], kv_refs[2 * source + 1]
            k = k_ref[:tokens, :]
            v = v_ref[...]
            extra = k_ref[tokens:, :].astype(jnp.float32)
            gates = (extra[:rows] + extra[rows : 2 * rows] + extra[2 * rows : 3 * rows]) * LOG2E
            doc_rows = extra[3 * rows : 3 * rows + halves]
            k_doc = jnp.concatenate([doc_rows[j : j + 1] for j in range(halves)], axis=1)
            allowed = k_doc == q_doc
            if source == 0:
                q_pos = row0 + lax.broadcasted_iota(jnp.int32, (tile, tokens), 0)
                k_pos = lax.broadcasted_iota(jnp.int32, (tile, tokens), 1)
                allowed = allowed & (k_pos <= q_pos)
            total = jnp.zeros((tile, width), jnp.float32)
            rescales = []
            for h in range(heads):
                q_h = jnp.where(in_head[h], q, jnp.zeros((), q.dtype))
                s = lax.dot_general(
                    q_h, k, (((1,), (1,)), ((), ())), preferred_element_type=jnp.float32
                )
                gate_row = jnp.concatenate(
                    [gates[h * halves + j : h * halves + j + 1] for j in range(halves)], axis=1
                )
                s = s * score_scale + (meta[:, h : h + 1] * LOG2E - gate_row)
                s = jnp.where(allowed, s, NEG)
                block_max = jnp.max(s, axis=1, keepdims=True)
                if source == 0:
                    new_max = block_max
                else:
                    old_max = m_ref[h]
                    new_max = jnp.maximum(old_max, block_max)
                    rescale = jnp.exp2(old_max - new_max)
                    rescales.append(rescale)
                p = jnp.exp2(s - new_max)
                block_sum = jnp.sum(p, axis=1, keepdims=True)
                m_ref[h] = new_max
                l_ref[h] = block_sum if source == 0 else l_ref[h] * rescale + block_sum
                v_h = jnp.where(in_head[h], v, jnp.zeros((), v.dtype))
                total = total + jnp.dot(
                    p.astype(jnp.bfloat16), v_h, preferred_element_type=jnp.float32
                )
            if source == 0:
                acc_ref[...] = total
            else:
                acc_ref[...] = acc_ref[...] * spread(rescales) + total

        visit(0)
        for source in range(1, sources):
            last_doc = jnp.max(
                kv_refs[2 * source][tokens + 3 * rows : tokens + 3 * rows + halves, :].astype(
                    jnp.float32
                )
            )

            @pl.when((valid_ref[source] > 0) & (last_doc >= first_doc))
            def _():
                visit(source)

        attended = acc_ref[...] / spread([l_ref[h] for h in range(heads)])
        squares = attended * attended
        means = [
            jnp.sum(jnp.where(in_head[h], squares, 0.0), axis=1, keepdims=True) / head_size
            for h in range(heads)
        ]
        scale = spread([lax.rsqrt(mean + EPS) for mean in means])
        normed = (attended * scale * gain_ref[...]).astype(jnp.bfloat16)
        here = pl.ds(pl.multiple_of((step // 2) * tile, tile), tile)

        @pl.when(step % 2 == valid_ref[sources])
        def _():
            mine_ref[here, :] = normed

        @pl.when(step % 2 != valid_ref[sources])
        def _():
            other_ref[here, :] = normed

        return carry

    lax.fori_loop(0, tokens // tile, q_tile, 0)


def attend(queries, keys, values, cum_gate, documents, head_gain):
    tokens, width = queries.shape
    heads = cum_gate.shape[1]
    head_size = width // heads
    n_sp = lax.axis_size("sp")
    place = lax.axis_index("sp")
    tile = tokens // lax.axis_size("tp")

    gate_rows = [part.T.reshape(-1, width) for part in bf16_parts(cum_gate)]
    doc_rows = documents.astype(jnp.bfloat16).reshape(-1, width)
    used = sum(part.shape[0] for part in gate_rows) + doc_rows.shape[0]
    filler = jnp.zeros((-used % 16, width), jnp.bfloat16)
    keys_more = jnp.concatenate([keys, *gate_rows, doc_rows, filler], axis=0)
    meta = jnp.concatenate(
        [
            cum_gate,
            documents.astype(jnp.float32)[:, None],
            jnp.zeros((tokens, 8 - (heads + 1) % 8), jnp.float32),
        ],
        axis=1,
    )

    reach = n_sp // 4
    ahead = [(i, i + 2) for i in range(n_sp - 2)]
    even_up = [(i, i + 1) for i in range(0, n_sp, 2)]
    odd_down = [(i + 1, i) for i in range(0, n_sp, 2)]

    def chain(first):
        own, other = [first], []
        for step in range(reach + 1):
            pairs = even_up if step == 0 else odd_down if step == reach else even_up + odd_down
            if step > 0:
                own.append(lax.ppermute(own[-1], "sp", ahead))
            other.append(lax.ppermute(own[-1], "sp", pairs))
        return own, other

    key_own, key_other = chain(keys_more)
    value_own, value_other = chain(values)
    group, member = place // 2, place % 2
    blocks, valid = [], []
    for step in range(reach + 1):
        exists = group - step >= 0
        blocks += [key_own[step], value_own[step]]
        valid.append(exists)
        blocks += [key_other[step], value_other[step]]
        if step == 0:
            exists = exists & (member == 1)
        elif step == reach:
            exists = exists & (member == 0)
        valid.append(exists)
    sources = len(valid)
    valid = jnp.stack(valid + [lax.axis_index("tp") % 2 == 1]).astype(jnp.int32)

    def kernel(*refs):
        attention_kernel(tokens, heads, head_size, tile, sources, *refs)

    vmem = pl.BlockSpec(memory_space=pltpu.VMEM)
    smem = pl.BlockSpec(memory_space=pltpu.SMEM)
    return pl.pallas_call(
        kernel,
        out_shape=[jax.ShapeDtypeStruct((tokens // 2, width), jnp.bfloat16)] * 2,
        in_specs=[smem, smem] + [vmem] * (3 + len(blocks)),
        out_specs=[vmem, vmem],
        scratch_shapes=[
            pltpu.VMEM((heads, tile, 1), jnp.float32),
            pltpu.VMEM((heads, tile, 1), jnp.float32),
            pltpu.VMEM((tile, width), jnp.float32),
        ],
        compiler_params=pltpu.CompilerParams(vmem_limit_bytes=50 * 2**20),
        name="attention",
    )(valid, documents, queries, meta, head_gain[None, :], *blocks)


def swap(x, axis, bits):
    return lax.ppermute(x, axis, [(i, i ^ bits) for i in range(lax.axis_size(axis))])


def far_places(n_sp):
    return [k for k in range(n_sp) if k & (n_sp // 2) and not k & (n_sp // 4)]


def expert_groups(n_sp):
    far = far_places(n_sp)
    near = [k ^ (k >> 1) for k in range(n_sp)]
    near = [k for k in near if k not in far]
    size = n_sp // 4
    return [near[:size], near[size : 2 * size], far[::-1], near[2 * size :]]


def project_kernel(experts, capacity, n_tp, far, *refs):
    blocks = n_tp // 2
    place_ref = refs[0]
    pieces = refs[1 : 1 + n_tp]
    weight_ref = refs[1 + n_tp]
    resids = refs[2 + n_tp : 2 + n_tp + blocks]
    routes = refs[2 + n_tp + blocks : 2 + n_tp + 2 * blocks]
    gain_ref = refs[2 + n_tp + 2 * blocks]
    outs = refs[3 + n_tp + 2 * blocks : 3 + n_tp + 2 * blocks + experts]
    stream_ref, wide_ref, packed_ref, slot_ref, pick_ref = refs[3 + n_tp + 2 * blocks + experts :]
    rows, width = resids[0].shape
    part = pieces[0].shape[1]
    place, spot = place_ref[0], place_ref[1]
    across = spot // 2
    n_tile = 512

    inputs = [
        jnp.concatenate(
            [
                piece[pl.ds(pl.multiple_of((across ^ j) * rows, rows), rows), :]
                for j in range(blocks)
            ],
            axis=0,
        )
        for piece in pieces
    ]
    total = jnp.zeros((blocks * rows, 1), jnp.float32)
    for n in range(width // n_tile):
        cols = slice(n * n_tile, (n + 1) * n_tile)
        projected = jnp.zeros((blocks * rows, n_tile), jnp.float32)
        for k in range(n_tp):
            from_row = pl.multiple_of((spot ^ k) * part, part)
            projected = projected + jnp.dot(
                inputs[k],
                weight_ref[pl.ds(from_row, part), cols],
                preferred_element_type=jnp.float32,
            )
        resid = jnp.concatenate([resid_ref[:, cols] for resid_ref in resids], axis=0)
        stream = (resid.astype(jnp.float32) + projected).astype(jnp.bfloat16)
        stream_ref[:, cols] = stream[:rows]
        wide = stream.astype(jnp.float32)
        wide_ref[:, cols] = wide
        total = total + jnp.sum(wide * wide, axis=1, keepdims=True)
    scale = lax.rsqrt(total / width + EPS)

    before = (
        lax.broadcasted_iota(jnp.int32, (rows, rows), 0)
        < lax.broadcasted_iota(jnp.int32, (rows, rows), 1)
    ).astype(jnp.bfloat16)
    expert_ids = lax.broadcasted_iota(jnp.int32, (experts, rows), 0).astype(jnp.float32)
    for j in range(blocks):
        chosen = jnp.zeros((experts, rows), jnp.float32)
        for route in range(2):
            chosen = chosen + (routes[j][route : route + 1, :] == expert_ids).astype(jnp.float32)
        ranks = jnp.dot(chosen.astype(jnp.bfloat16), before, preferred_element_type=jnp.float32)
        slot_ref[j] = jnp.where(chosen > 0.0, ranks, -1.0)
    slot_ids = lax.broadcasted_iota(jnp.int32, (capacity, rows), 0).astype(jnp.float32)
    first, spans = 0, []
    for k in range(experts):
        spans.append(first)
        for j in range(1 if k in far else blocks):
            row_of = slot_ref[j, pl.ds(place ^ k, 1), :]
            for i in range(blocks):
                pick = (slot_ids == row_of) if i == j else jnp.zeros((capacity, rows), jnp.bool_)
                pick_ref[first : first + capacity, i * rows : (i + 1) * rows] = pick.astype(
                    jnp.float32
                ).astype(jnp.bfloat16)
            first += capacity
    spans.append(first)
    for n in range(width // n_tile):
        cols = slice(n * n_tile, (n + 1) * n_tile)
        packed_ref[...] = (wide_ref[:, cols] * scale * gain_ref[:, cols]).astype(jnp.bfloat16)
        picked = jnp.dot(
            pick_ref[...], packed_ref[...], preferred_element_type=jnp.float32
        ).astype(jnp.bfloat16)
        for k in range(experts):
            outs[k][:, cols] = picked[spans[k] : spans[k + 1]]


def expert_kernel(count, *refs):
    inputs = refs[:count]
    gate_ref, up_ref, down_hbm = refs[count : count + 3]
    mine_ref, other_ref, x_ref, hidden_ref, down_ref, sem = refs[count + 3 :]
    mine_rows = mine_ref.shape[0]
    step, steps = pl.program_id(0), hidden_ref.shape[0]
    fetch = pltpu.make_async_copy(down_hbm, down_ref, sem)

    @pl.when(step == 0)
    def _():
        fetch.start()
        row = 0
        for ref in inputs:
            x_ref[row : row + ref.shape[0], :] = ref[...]
            row += ref.shape[0]

    both = jnp.concatenate([gate_ref[...], up_ref[...]], axis=1)
    product = jnp.dot(x_ref[...], both, preferred_element_type=jnp.float32)
    half = product.shape[1] // 2
    gate, up = product[:, :half], product[:, half:]
    hidden_ref[step] = (gate * (1.0 / (1.0 + jnp.exp(-gate))) * up).astype(jnp.bfloat16)

    @pl.when(step == steps - 1)
    def _():
        fetch.wait()
        hidden = jnp.concatenate([hidden_ref[i] for i in range(steps)], axis=1)
        n_tile = 512
        for n in range(down_ref.shape[1] // n_tile):
            cols = slice(n * n_tile, (n + 1) * n_tile)
            out = jnp.dot(
                hidden, down_ref[:, cols], preferred_element_type=jnp.float32
            ).astype(jnp.bfloat16)
            mine_ref[:, cols] = out[:mine_rows]
            other_ref[:, cols] = out[mine_rows:]


def combine_kernel(experts, place_ref, stream_ref, routes_ref, weights_ref, *refs):
    outs = refs[:experts]
    mixed_ref, stack_ref = refs[experts:]
    rows, width = stream_ref.shape
    capacity = outs[0].shape[0]
    for k in range(experts):
        stack_ref[k * capacity : (k + 1) * capacity, :] = outs[k][...]
    expert_ids = lax.broadcasted_iota(jnp.int32, (rows, experts), 1)
    named = [
        (routes_ref[:, route : route + 1] == expert_ids).astype(jnp.float32) for route in range(2)
    ]
    before = (
        lax.broadcasted_iota(jnp.int32, (rows, rows), 1)
        < lax.broadcasted_iota(jnp.int32, (rows, rows), 0)
    ).astype(jnp.bfloat16)
    ranks = jnp.dot(
        before, (named[0] + named[1]).astype(jnp.bfloat16), preferred_element_type=jnp.float32
    )
    slot_ids = lax.broadcasted_iota(jnp.int32, (rows, experts * capacity), 1)
    picks = []
    for route in range(2):
        rank = jnp.sum(named[route] * ranks, axis=1, keepdims=True).astype(jnp.int32)
        target = (routes_ref[:, route : route + 1] ^ place_ref[0]) * capacity + rank
        picks.append((slot_ids == target).astype(jnp.float32).astype(jnp.bfloat16))
    n_tile = 512
    for n in range(width // n_tile):
        cols = slice(n * n_tile, (n + 1) * n_tile)
        mixed = stream_ref[:, cols].astype(jnp.float32)
        for route in range(2):
            result = jnp.dot(picks[route], stack_ref[:, cols], preferred_element_type=jnp.float32)
            mixed = mixed + weights_ref[:, route : route + 1] * result
        mixed_ref[:, cols] = mixed.astype(jnp.bfloat16)


def on_device(
    queries,
    keys,
    values,
    cum_gate,
    documents,
    head_gain,
    out_weight,
    resid,
    norm_gain,
    routes,
    route_weights,
    w_gate,
    w_up,
    w_down,
):
    tokens = queries.shape[0]
    n_sp, n_tp = lax.axis_size("sp"), lax.axis_size("tp")
    place, spot = lax.axis_index("sp"), lax.axis_index("tp")
    blocks = n_tp // 2
    local_rows, model_width = resid.shape
    capacity = 2 * routes.shape[1] * tokens // (n_tp * n_sp)
    each = blocks * capacity
    vmem = pl.BlockSpec(memory_space=pltpu.VMEM)
    smem = pl.BlockSpec(memory_space=pltpu.SMEM)
    places = jnp.stack([place, spot]).astype(jnp.int32)

    route_rows = jnp.concatenate(
        [routes.T.astype(jnp.float32), jnp.zeros((8 - routes.shape[1], local_rows), jnp.float32)],
        axis=0,
    )
    resids = [resid] + [swap(resid, "tp", 2 * j) for j in range(1, blocks)]
    route_blocks = [route_rows] + [swap(route_rows, "tp", 2 * j) for j in range(1, blocks)]

    mine, other = attend(queries, keys, values, cum_gate, documents, head_gain)
    pieces = [mine] + [swap(other if k % 2 else mine, "tp", k) for k in range(1, n_tp)]

    far = far_places(n_sp)
    counts = [capacity if k in far else each for k in range(n_sp)]

    def project(*refs):
        project_kernel(n_sp, capacity, n_tp, far, *refs)

    *outbound, stream = pl.pallas_call(
        project,
        out_shape=[jax.ShapeDtypeStruct((count, model_width), jnp.bfloat16) for count in counts]
        + [jax.ShapeDtypeStruct((local_rows, model_width), jnp.bfloat16)],
        in_specs=[smem] + [vmem] * (n_tp + 2 + 2 * blocks),
        out_specs=[vmem] * (n_sp + 1),
        scratch_shapes=[
            pltpu.VMEM((blocks * local_rows, model_width), jnp.float32),
            pltpu.VMEM((blocks * local_rows, 512), jnp.bfloat16),
            pltpu.VMEM((blocks, n_sp, local_rows), jnp.float32),
            pltpu.VMEM((sum(counts), blocks * local_rows), jnp.bfloat16),
        ],
        compiler_params=pltpu.CompilerParams(vmem_limit_bytes=40 * 2**20),
        name="project",
    )(places, *pieces, out_weight, *resids, *route_blocks, norm_gain[None, :])

    def hop(x, k):
        if k == 0:
            return x
        if k in far and k % 2:
            low, step = k % (n_sp // 2), n_sp // 4
            x = lax.ppermute(x, "sp", [(i, ((i ^ low) - step) % n_sp) for i in range(n_sp)])
            return lax.ppermute(x, "sp", [(i, (i - step) % n_sp) for i in range(n_sp)])
        return swap(x, "sp", k)

    groups = expert_groups(n_sp)
    members = len(groups[0])
    hidden_width = w_gate.shape[2]
    h_tile = 128
    rows = 2 * members * each
    arrived = {k: hop(outbound[k], k) for group in groups for k in group}
    returned = {}
    for group in groups:
        inputs = []
        for k in group:
            inputs.append(arrived[k])
            if k in far:
                inputs += [swap(arrived[k], "tp", 2 * j) for j in range(1, blocks)]
        inputs += [swap(x, "tp", 1) for x in inputs]

        def expert(*refs):
            expert_kernel(len(inputs), *refs)

        part_mine, part_other = pl.pallas_call(
            expert,
            grid=(hidden_width // h_tile,),
            out_shape=[jax.ShapeDtypeStruct((members * each, model_width), jnp.bfloat16)] * 2,
            in_specs=[pl.BlockSpec(x.shape, lambda f: (0, 0)) for x in inputs]
            + [pl.BlockSpec((model_width, h_tile), lambda f: (0, f))] * 2
            + [pl.BlockSpec(memory_space=pl.ANY)],
            out_specs=[pl.BlockSpec((members * each, model_width), lambda f: (0, 0))] * 2,
            scratch_shapes=[
                pltpu.VMEM((rows, model_width), jnp.bfloat16),
                pltpu.VMEM((hidden_width // h_tile, rows, h_tile), jnp.bfloat16),
                pltpu.VMEM((hidden_width, model_width), jnp.bfloat16),
                pltpu.SemaphoreType.DMA,
            ],
            compiler_params=pltpu.CompilerParams(
                dimension_semantics=("arbitrary",), vmem_limit_bytes=40 * 2**20
            ),
            cost_estimate=pl.CostEstimate(
                flops=6 * rows * model_width * hidden_width,
                transcendentals=rows * hidden_width,
                bytes_accessed=6 * model_width * hidden_width + 4 * rows * model_width,
            ),
            name="expert",
        )(*inputs, w_gate[0], w_up[0], w_down[0])
        added = swap(part_other, "tp", 1)
        shape = (members, blocks, capacity, model_width)
        part_mine, added = part_mine.reshape(shape), added.reshape(shape)

        def summed(j):
            return part_mine[:, j].astype(jnp.float32) + added[:, j].astype(jnp.float32)

        result = summed(0)
        for j in range(1, blocks):
            sent = swap(summed(j).astype(jnp.bfloat16), "tp", 2 * j)
            result = result + sent.astype(jnp.float32)
        result = result.astype(jnp.bfloat16)
        for i, k in enumerate(group):
            returned[k] = hop(result[i], k)

    def combine(*refs):
        combine_kernel(n_sp, *refs)

    return pl.pallas_call(
        combine,
        out_shape=jax.ShapeDtypeStruct((local_rows, model_width), jnp.bfloat16),
        in_specs=[smem] + [vmem] * (3 + n_sp),
        out_specs=vmem,
        scratch_shapes=[pltpu.VMEM((n_sp * capacity, model_width), jnp.bfloat16)],
        compiler_params=pltpu.CompilerParams(vmem_limit_bytes=24 * 2**20),
        name="combine",
    )(places, stream, routes, route_weights, *[returned[k] for k in range(n_sp)])


def solution(mesh):
    in_specs = (
        P("sp", "tp"),
        P("sp", "tp"),
        P("sp", "tp"),
        P("sp", "tp"),
        P("sp"),
        P("tp"),
        P(),
        P(("sp", "tp"), None),
        P(),
        P(("sp", "tp"), None),
        P(("sp", "tp"), None),
        P("sp", None, "tp"),
        P("sp", None, "tp"),
        P("sp", "tp", None),
    )
    out_specs = P(("sp", "tp"), None)


    return jax.shard_map(on_device, mesh=mesh, in_specs=in_specs, out_specs=out_specs, check_vma=False)
```

profile of v0, /device:TPU:0, one launch (start us, length us, event | category | flops | bytes accessed | tf_op | source)
XLA Modules:
  0.0 289.6 jit_solution(2549470143420840814)
XLA Ops:
  2.6 5.0 %collective-permute-start.2 = (bf16[544,256]{1,0:T(8,128)(2,1)S(1)}, bf16[544,256]{1,0:T(8,128)(2,1)S(1)}, u32[]{:S(2)}, u32[]{:S(2)}) collective-permute-start(bf16[544,256]{1,0:T(8,128)(2,1)S(1)} %concatenate.10.refs_5_), channel_id=1, source_target_pairs={{0,8},{4,12},{8,16},{12,20},{16,24},{20,28},{1,9},{5,13},{9,17},{1... | collective-permute-start | bytes 835592 | tf_op jit(solution)/shard_map/ppermute | solution.py:159
  7.6 3.5 %collective-permute-start.3 = (bf16[512,256]{1,0:T(8,128)(2,1)}, bf16[512,256]{1,0:T(8,128)(2,1)S(1)}, u32[]{:S(2)}, u32[]{:S(2)}) collective-permute-start(bf16[512,256]{1,0:T(8,128)(2,1)} %refs_6_.2), channel_id=1, source_target_pairs={{0,8},{4,12},{8,16},{12,20},{16,24},{20,28},{1,9},{5,13},{9,17},{1... | collective-permute-start | bytes 786440 | tf_op jit(solution)/shard_map/ppermute | solution.py:159
  11.1 3.5 %collective-permute-done.2.refs_9_ = bf16[544,256]{1,0:T(8,128)(2,1)S(1)} collective-permute-done((bf16[544,256]{1,0:T(8,128)(2,1)S(1)}, bf16[544,256]{1,0:T(8,128)(2,1)S(1)}, u32[]{:S(2)}, u32[]{:S(2)}) %collective-permute-start.2) | collective-permute-done | bytes 278560 | tf_op jit(solution)/shard_map/ppermute | solution.py:159
  14.6 4.4 %collective-permute-start.6 = (bf16[544,256]{1,0:T(8,128)(2,1)S(1)}, bf16[544,256]{1,0:T(8,128)(2,1)S(1)}, u32[]{:S(2)}, u32[]{:S(2)}) collective-permute-start(bf16[544,256]{1,0:T(8,128)(2,1)S(1)} %collective-permute-done.2.refs_9_), channel_id=1, source_target_pairs={{0,8},{4,12},{8,16},{12,20},{16,24},{20,28},{1,9},{5,13},{9,17},{1... | collective-permute-start | bytes 835592 | tf_op jit(solution)/shard_map/ppermute | solution.py:159
  19.0 3.4 %collective-permute-start.1 = (bf16[512,256]{1,0:T(8,128)(2,1)}, bf16[512,256]{1,0:T(8,128)(2,1)S(1)}, u32[]{:S(2)}, u32[]{:S(2)}) collective-permute-start(bf16[512,256]{1,0:T(8,128)(2,1)} %refs_6_.2), channel_id=1, source_target_pairs={{0,4},{8,12},{16,20},{24,28},{1,5},{9,13},{17,21},{25,29},{2,6},{1... | collective-permute-start | bytes 786440 | tf_op jit(solution)/shard_map/ppermute | solution.py:160
  22.5 4.2 %collective-permute-start.7 = (bf16[512,256]{1,0:T(8,128)(2,1)S(1)}, bf16[512,256]{1,0:T(8,128)(2,1)}, u32[]{:S(2)}, u32[]{:S(2)}) collective-permute-start(bf16[512,256]{1,0:T(8,128)(2,1)S(1)} %collective-permute-done.3.refs_10_), channel_id=1, source_target_pairs={{0,8},{4,12},{8,16},{12,20},{16,24},{20,28},{1,9},{5,13},{9,17},{1... | collective-permute-start | bytes 786440 | tf_op jit(solution)/shard_map/ppermute | solution.py:159
  38.1 11.0 %collective-permute-done.5.refs_12_ = bf16[512,256]{1,0:T(8,128)(2,1)} collective-permute-done((bf16[512,256]{1,0:T(8,128)(2,1)S(1)}, bf16[512,256]{1,0:T(8,128)(2,1)}, u32[]{:S(2)}, u32[]{:S(2)}) %collective-permute-start.5) | collective-permute-done | bytes 262176 | tf_op jit(solution)/shard_map/ppermute | solution.py:160
  55.2 9.2 %attention.1 = (bf16[256,256]{1,0:T(8,128)(2,1)S(1)}, bf16[256,256]{1,0:T(8,128)(2,1)S(1)}) custom-call(s32[7]{0:T(128)S(1)} %convert_element_type.136.refs_0_, s32[512]{0:T(512)S(1)} %copy-done.5, bf16[512,256]{1,0:T(8,128)(2,1)S(1)} %copy-done.2, f32[512,8]{1,0:T(8,128)S(1)} %copy.38.refs_3_, f32[1,256]{1,0:T(1,128)S(1)} %bitcast.143, ...), custom_call_target="tpu_custom_call" | custom-call | tf_op jit(solution)/shard_map/attention/pallas_call | solution.py:185
  68.2 5.0 %collective-permute-done.14.refs_9_ = f32[8,128]{1,0:T(8,128)S(1)} collective-permute-done((f32[8,128]{1,0:T(8,128)S(1)}, f32[8,128]{1,0:T(8,128)S(1)}, u32[]{:S(2)}, u32[]{:S(2)}) %collective-permute-start.14) | collective-permute-done | bytes 4128 | tf_op jit(solution)/shard_map/ppermute | solution.py:201
  75.5 3.2 %project.1 = (bf16[128,2048]{1,0:T(8,128)(2,1)S(1)}, bf16[128,2048]{1,0:T(8,128)(2,1)S(1)}, bf16[128,2048]{1,0:T(8,128)(2,1)S(1)}, bf16[128,2048]{1,0:T(8,128)(2...) custom-call(s32[2]{0:T(128)S(1)} %pad_add_fusion.refs_0_, ...), custom_call_target="tpu_custom_call" | custom-call | tf_op jit(solution)/shard_map/project/pallas_call | solution.py:408
  78.7 6.9 %collective-permute-start.43 = (bf16[128,2048]{1,0:T(8,128)(2,1)S(1)}, bf16[128,2048]{1,0:T(8,128)(2,1)S(1)}, u32[]{:S(2)}, u32[]{:S(2)}) collective-permute-start(bf16[128,2048]{1,0:T(8,128)(2,1)S(1)} %get-tuple-element.39), channel_id=1, source_target_pairs={{0,24},{4,28},{8,16},{12,20},{16,8},{20,12},{24,0},{28,4},{1,25},{... | collective-permute-start | bytes 1572872 | tf_op jit(solution)/shard_map/ppermute | solution.py:201
  87.0 3.3 %collective-permute-start.29 = (bf16[64,2048]{1,0:T(8,128)(2,1)S(1)}, bf16[64,2048]{1,0:T(8,128)(2,1)S(1)}, u32[]{:S(2)}, u32[]{:S(2)}) collective-permute-start(bf16[64,2048]{1,0:T(8,128)(2,1)S(1)} %get-tuple-element.35), channel_id=1, source_target_pairs={{0,28},{4,24},{8,4},{12,0},{16,12},{20,8},{24,20},{28,16},{1,29},{... | collective-permute-start | bytes 786440 | tf_op jit(solution)/shard_map/ppermute | solution.py:429
  90.3 5.0 %collective-permute-start.21 = (bf16[128,2048]{1,0:T(8,128)(2,1)S(1)}, bf16[128,2048]{1,0:T(8,128)(2,1)S(1)}, u32[]{:S(2)}, u32[]{:S(2)}) collective-permute-start(bf16[128,2048]{1,0:T(8,128)(2,1)S(1)} %get-tuple-element.31), channel_id=1, source_target_pairs={{0,12},{4,8},{8,4},{12,0},{16,28},{20,24},{24,20},{28,16},{1,13},{... | collective-permute-start | bytes 1572872 | tf_op jit(solution)/shard_map/ppermute | solution.py:201
  95.3 4.2 %collective-permute-start.32 = (bf16[64,2048]{1,0:T(8,128)(2,1)S(1)}, bf16[64,2048]{1,0:T(8,128)(2,1)S(1)}, u32[]{:S(2)}, u32[]{:S(2)}) collective-permute-start(bf16[64,2048]{1,0:T(8,128)(2,1)S(1)} %get-tuple-element.36), channel_id=1, source_target_pairs={{0,16},{4,20},{8,24},{12,28},{16,0},{20,4},{24,8},{28,12},{1,17},{... | collective-permute-start | bytes 786440 | tf_op jit(solution)/shard_map/ppermute | solution.py:201
  99.5 15.8 %collective-permute-done.29 = bf16[64,2048]{1,0:T(8,128)(2,1)S(1)} collective-permute-done((bf16[64,2048]{1,0:T(8,128)(2,1)S(1)}, bf16[64,2048]{1,0:T(8,128)(2,1)S(1)}, u32[]{:S(2)}, u32[]{:S(2)}) %collective-permute-start.29) | collective-permute-done | bytes 262176 | tf_op jit(solution)/shard_map/ppermute | solution.py:429
  115.3 30.2 %collective-permute-start.22 = (bf16[128,2048]{1,0:T(8,128)(2,1)S(1)}, bf16[128,2048]{1,0:T(8,128)(2,1)S(1)}, u32[]{:S(2)}, u32[]{:S(2)}) collective-permute-start(bf16[128,2048]{1,0:T(8,128)(2,1)S(1)} %get-tuple-element.32), channel_id=1, source_target_pairs={{0,8},{4,12},{8,0},{12,4},{16,24},{20,28},{24,16},{28,20},{1,9},{5... | collective-permute-start | bytes 1572872 | tf_op jit(solution)/shard_map/ppermute | solution.py:201
  145.5 4.5 %collective-permute-done.32.refs_2_ = bf16[64,2048]{1,0:T(8,128)(2,1)S(1)} collective-permute-done((bf16[64,2048]{1,0:T(8,128)(2,1)S(1)}, bf16[64,2048]{1,0:T(8,128)(2,1)S(1)}, u32[]{:S(2)}, u32[]{:S(2)}) %collective-permute-start.32) | collective-permute-done | bytes 262176 | tf_op jit(solution)/shard_map/ppermute | solution.py:201
  153.4 13.4 %collective-permute-done.30.refs_0_ = bf16[64,2048]{1,0:T(8,128)(2,1)S(1)} collective-permute-done((bf16[64,2048]{1,0:T(8,128)(2,1)S(1)}, bf16[64,2048]{1,0:T(8,128)(2,1)S(1)}, u32[]{:S(2)}, u32[]{:S(2)}) %collective-permute-start.30) | collective-permute-done | bytes 262176 | tf_op jit(solution)/shard_map/ppermute | solution.py:430
  169.4 5.6 %collective-permute-done.31.refs_1_ = bf16[64,2048]{1,0:T(8,128)(2,1)S(1)} collective-permute-done((bf16[64,2048]{1,0:T(8,128)(2,1)S(1)}, bf16[64,2048]{1,0:T(8,128)(2,1)S(1)}, u32[]{:S(2)}, u32[]{:S(2)}) %collective-permute-start.31) | collective-permute-done | bytes 262176 | tf_op jit(solution)/shard_map/ppermute | solution.py:201
  175.6 9.0 %expert.7 = (bf16[256,2048]{1,0:T(8,128)(2,1)S(1)}, bf16[256,2048]{1,0:T(8,128)(2,1)S(1)}) custom-call(bf16[128,2048]{1,0:T(8,128)(2,1)S(1)} %collective-permute-done.43.refs_0_, bf16[128,2048]{1,0:T(8,128)(2,1)S(1)} %collective-permute-done.44.refs_1_, bf16[128,2048]{1,0:T(8,128)(2,1)S(1)} %collective-permute-done.45.refs_2_, ...), custom_call_target="tpu_custom_call" | custom-call | flops 5637144576 | bytes 15204352 | tf_op jit(solution)/shard_map/expert/pallas_call | solution.py:451
  186.1 9.0 %expert.6 = (bf16[256,2048]{1,0:T(8,128)(2,1)S(1)}, bf16[256,2048]{1,0:T(8,128)(2,1)S(1)}) custom-call(bf16[64,2048]{1,0:T(8,128)(2,1)S(1)} %collective-permute-done.30.refs_0_, bf16[64,2048]{1,0:T(8,128)(2,1)S(1)} %collective-permute-done.31.refs_1_, bf16[64,2048]{1,0:T(8,128)(2,1)S(1)} %collective-permute-done.32.refs_2_, ...), custom_call_target="tpu_custom_call" | custom-call | flops 5637144576 | bytes 15204352 | tf_op jit(solution)/shard_map/expert/pallas_call | solution.py:451
  195.2 9.0 %expert.5 = (bf16[256,2048]{1,0:T(8,128)(2,1)S(1)}, bf16[256,2048]{1,0:T(8,128)(2,1)S(1)}) custom-call(bf16[128,2048]{1,0:T(8,128)(2,1)S(1)} %collective-permute-done.21.refs_0_, bf16[128,2048]{1,0:T(8,128)(2,1)S(1)} %collective-permute-done.22.refs_1_, bf16[128,2048]{1,0:T(8,128)(2,1)S(1)} %collective-permute-done.23.refs_2_, ...), custom_call_target="tpu_custom_call" | custom-call | flops 5637144576 | bytes 15204352 | tf_op jit(solution)/shard_map/expert/pallas_call | solution.py:451
  204.7 9.0 %expert.4 = (bf16[256,2048]{1,0:T(8,128)(2,1)S(1)}, bf16[256,2048]{1,0:T(8,128)(2,1)S(1)}) custom-call(bf16[128,2048]{1,0:T(8,128)(2,1)S(1)} %get-tuple-element.27.refs_0_, bf16[128,2048]{1,0:T(8,128)(2,1)S(1)} %collective-permute-done.15.refs_1_, bf16[128,2048]{1,0:T(8,128)(2,1)S(1)} %collective-permute-done.16.refs_2_, ...), custom_call_target="tpu_custom_call" | custom-call | flops 5637144576 | bytes 15204352 | tf_op jit(solution)/shard_map/expert/pallas_call | solution.py:451
  219.8 10.1 %collective-permute-done.48 = bf16[2,64,2048]{2,1,0:T(8,128)(2,1)S(1)} collective-permute-done((bf16[2,64,2048]{2,1,0:T(8,128)(2,1)S(1)}, bf16[2,64,2048]{2,1,0:T(8,128)(2,1)S(1)}, u32[]{:S(2)}, u32[]{:S(2)}) %collective-permute-start.48) | collective-permute-done | bytes 524320 | tf_op jit(solution)/shard_map/ppermute | solution.py:201
  231.3 4.4 %collective-permute-start.50 = (bf16[64,2048]{1,0:T(8,128)(2,1)S(1)}, bf16[64,2048]{1,0:T(8,128)(2,1)S(1)}, u32[]{:S(2)}, u32[]{:S(2)}) collective-permute-start(bf16[64,2048]{1,0:T(8,128)(2,1)S(1)} %get-tuple-element.43), channel_id=1, source_target_pairs={{0,28},{4,24},{8,20},{12,16},{16,12},{20,8},{24,4},{28,0},{1,29},{... | collective-permute-start | bytes 786440 | tf_op jit(solution)/shard_map/ppermute | solution.py:201
  235.7 5.4 %collective-permute-done.39 = bf16[2,64,2048]{2,1,0:T(8,128)(2,1)S(1)} collective-permute-done((bf16[2,64,2048]{2,1,0:T(8,128)(2,1)S(1)}, bf16[2,64,2048]{2,1,0:T(8,128)(2,1)S(1)}, u32[]{:S(2)}, u32[]{:S(2)}) %collective-permute-start.39) | collective-permute-done | bytes 524320 | tf_op jit(solution)/shard_map/ppermute | solution.py:201
  241.5 10.9 %collective-permute-done.26 = bf16[2,64,2048]{2,1,0:T(8,128)(2,1)S(1)} collective-permute-done((bf16[2,64,2048]{2,1,0:T(8,128)(2,1)S(1)}, bf16[2,64,2048]{2,1,0:T(8,128)(2,1)S(1)}, u32[]{:S(2)}, u32[]{:S(2)}) %collective-permute-start.26) | collective-permute-done | bytes 524320 | tf_op jit(solution)/shard_map/ppermute | solution.py:201
  253.4 9.7 %collective-permute-done.19 = bf16[2,64,2048]{2,1,0:T(8,128)(2,1)S(1)} collective-permute-done((bf16[2,64,2048]{2,1,0:T(8,128)(2,1)S(1)}, bf16[2,64,2048]{2,1,0:T(8,128)(2,1)S(1)}, u32[]{:S(2)}, u32[]{:S(2)}) %collective-permute-start.19) | collective-permute-done | bytes 524320 | tf_op jit(solution)/shard_map/ppermute | solution.py:201
  267.8 5.4 %collective-permute-done.40.refs_8_ = bf16[64,2048]{1,0:T(8,128)(2,1)S(1)} collective-permute-done((bf16[64,2048]{1,0:T(8,128)(2,1)S(1)}, bf16[64,2048]{1,0:T(8,128)(2,1)S(1)}, u32[]{:S(2)}, u32[]{:S(2)}) %collective-permute-start.40) | collective-permute-done | bytes 262176 | tf_op jit(solution)/shard_map/ppermute | solution.py:201
  273.2 3.3 %collective-permute-done.27.refs_6_ = bf16[64,2048]{1,0:T(8,128)(2,1)S(1)} collective-permute-done((bf16[64,2048]{1,0:T(8,128)(2,1)}, bf16[64,2048]{1,0:T(8,128)(2,1)S(1)}, u32[]{:S(2)}, u32[]{:S(2)}) %collective-permute-start.27) | collective-permute-done | bytes 262176 | tf_op jit(solution)/shard_map/ppermute | solution.py:201
  276.5 6.2 %collective-permute-done.28.refs_7_ = bf16[64,2048]{1,0:T(8,128)(2,1)S(1)} collective-permute-done((bf16[64,2048]{1,0:T(8,128)(2,1)S(1)}, bf16[64,2048]{1,0:T(8,128)(2,1)S(1)}, u32[]{:S(2)}, u32[]{:S(2)}) %collective-permute-start.28) | collective-permute-done | bytes 262176 | tf_op jit(solution)/shard_map/ppermute | solution.py:201
  282.7 4.3 %collective-permute-done.42.refs_9_ = bf16[64,2048]{1,0:T(8,128)(2,1)S(1)} collective-permute-done((bf16[64,2048]{1,0:T(8,128)(2,1)}, bf16[64,2048]{1,0:T(8,128)(2,1)S(1)}, u32[]{:S(2)}, u32[]{:S(2)}) %collective-permute-start.42) | collective-permute-done | bytes 262176 | tf_op jit(solution)/shard_map/ppermute | solution.py:430
  (130 shorter events, 52.4 us)
Async XLA Ops:
  7.6 14.9 %collective-permute-start.3 = (bf16[512,256]{1,0:T(8,128)(2,1)}, bf16[512,256]{1,0:T(8,128)(2,1)S(1)}, u32[]{:S(2)}, u32[]{:S(2)}) collective-permute-start(bf16[512,256]{1,0:T(8,128)(2,1)} %refs_6_.2), channel_id=1, source_target_pairs={{0,8},{4,12},{8,16},{12,20},{16,24},{20,28},{1,9},{5,13},{9,17},{1... | collective-permute-start | bytes 786440 | tf_op jit(solution)/shard_map/ppermute | solution.py:159
  28.7 20.4 %collective-permute-start.4 = (bf16[544,256]{1,0:T(8,128)(2,1)S(1)}, bf16[544,256]{1,0:T(8,128)(2,1)S(1)}, u32[]{:S(2)}, u32[]{:S(2)}) collective-permute-start(bf16[544,256]{1,0:T(8,128)(2,1)S(1)} %collective-permute-done.2.refs_9_), channel_id=1, source_target_pairs={{0,4},{8,12},{16,20},{24,28},{4,0},{12,8},{20,16},{28,24},{1,5},{9... | collective-permute-start | bytes 835592 | tf_op jit(solution)/shard_map/ppermute | solution.py:160
  28.8 23.1 %collective-permute-start.8 = (bf16[544,256]{1,0:T(8,128)(2,1)S(1)}, bf16[544,256]{1,0:T(8,128)(2,1)S(1)}, u32[]{:S(2)}, u32[]{:S(2)}) collective-permute-start(bf16[544,256]{1,0:T(8,128)(2,1)S(1)} %collective-permute-done.6.refs_13_), channel_id=1, source_target_pairs={{4,0},{12,8},{20,16},{28,24},{5,1},{13,9},{21,17},{29,25},{6,2},{1... | collective-permute-start | bytes 835592 | tf_op jit(solution)/shard_map/ppermute | solution.py:160
  30.1 19.0 %collective-permute-start.5 = (bf16[512,256]{1,0:T(8,128)(2,1)S(1)}, bf16[512,256]{1,0:T(8,128)(2,1)}, u32[]{:S(2)}, u32[]{:S(2)}) collective-permute-start(bf16[512,256]{1,0:T(8,128)(2,1)S(1)} %collective-permute-done.3.refs_10_), channel_id=1, source_target_pairs={{0,4},{8,12},{16,20},{24,28},{4,0},{12,8},{20,16},{28,24},{1,5},{9... | collective-permute-start | bytes 786440 | tf_op jit(solution)/shard_map/ppermute | solution.py:160
  32.9 19.1 %collective-permute-start.9 = (bf16[512,256]{1,0:T(8,128)(2,1)}, bf16[512,256]{1,0:T(8,128)(2,1)}, u32[]{:S(2)}, u32[]{:S(2)}) collective-permute-start(bf16[512,256]{1,0:T(8,128)(2,1)} %collective-permute-done.7.refs_14_), channel_id=1, source_target_pairs={{4,0},{12,8},{20,16},{28,24},{5,1},{13,9},{21,17},{29,25},{6,2},{1... | collective-permute-start | bytes 786440 | tf_op jit(solution)/shard_map/ppermute | solution.py:160
  35.7 37.5 %collective-permute-start.13 = (bf16[128,2048]{1,0:T(8,128)(2,1)}, bf16[128,2048]{1,0:T(8,128)(2,1)S(1)}, u32[]{:S(2)}, u32[]{:S(2)}) collective-permute-start(bf16[128,2048]{1,0:T(8,128)(2,1)} %refs_6_.3), channel_id=1, source_target_pairs={{0,2},{1,3},{2,0},{3,1},{4,6},{5,7},{6,4},{7,5},{8,10},{9,11},{10,... | collective-permute-start | bytes 1572872 | tf_op jit(solution)/shard_map/ppermute | solution.py:201
  78.7 72.7 %collective-permute-start.43 = (bf16[128,2048]{1,0:T(8,128)(2,1)S(1)}, bf16[128,2048]{1,0:T(8,128)(2,1)S(1)}, u32[]{:S(2)}, u32[]{:S(2)}) collective-permute-start(bf16[128,2048]{1,0:T(8,128)(2,1)S(1)} %get-tuple-element.39), channel_id=1, source_target_pairs={{0,24},{4,28},{8,16},{12,20},{16,8},{20,12},{24,0},{28,4},{1,25},{... | collective-permute-start | bytes 1572872 | tf_op jit(solution)/shard_map/ppermute | solution.py:201
  85.6 65.8 %collective-permute-start.44 = (bf16[128,2048]{1,0:T(8,128)(2,1)S(1)}, bf16[128,2048]{1,0:T(8,128)(2,1)S(1)}, u32[]{:S(2)}, u32[]{:S(2)}) collective-permute-start(bf16[128,2048]{1,0:T(8,128)(2,1)S(1)} %get-tuple-element.40), channel_id=1, source_target_pairs={{0,28},{4,24},{8,20},{12,16},{16,12},{20,8},{24,4},{28,0},{1,29},{... | collective-permute-start | bytes 1572872 | tf_op jit(solution)/shard_map/ppermute | solution.py:201
  87.0 28.2 %collective-permute-start.29 = (bf16[64,2048]{1,0:T(8,128)(2,1)S(1)}, bf16[64,2048]{1,0:T(8,128)(2,1)S(1)}, u32[]{:S(2)}, u32[]{:S(2)}) collective-permute-start(bf16[64,2048]{1,0:T(8,128)(2,1)S(1)} %get-tuple-element.35), channel_id=1, source_target_pairs={{0,28},{4,24},{8,4},{12,0},{16,12},{20,8},{24,20},{28,16},{1,29},{... | collective-permute-start | bytes 786440 | tf_op jit(solution)/shard_map/ppermute | solution.py:429
  90.3 61.6 %collective-permute-start.21 = (bf16[128,2048]{1,0:T(8,128)(2,1)S(1)}, bf16[128,2048]{1,0:T(8,128)(2,1)S(1)}, u32[]{:S(2)}, u32[]{:S(2)}) collective-permute-start(bf16[128,2048]{1,0:T(8,128)(2,1)S(1)} %get-tuple-element.31), channel_id=1, source_target_pairs={{0,12},{4,8},{8,4},{12,0},{16,28},{20,24},{24,20},{28,16},{1,13},{... | collective-permute-start | bytes 1572872 | tf_op jit(solution)/shard_map/ppermute | solution.py:201
  95.3 54.7 %collective-permute-start.32 = (bf16[64,2048]{1,0:T(8,128)(2,1)S(1)}, bf16[64,2048]{1,0:T(8,128)(2,1)S(1)}, u32[]{:S(2)}, u32[]{:S(2)}) collective-permute-start(bf16[64,2048]{1,0:T(8,128)(2,1)S(1)} %get-tuple-element.36), channel_id=1, source_target_pairs={{0,16},{4,20},{8,24},{12,28},{16,0},{20,4},{24,8},{28,12},{1,17},{... | collective-permute-start | bytes 786440 | tf_op jit(solution)/shard_map/ppermute | solution.py:201
  115.3 52.9 %collective-permute-start.22 = (bf16[128,2048]{1,0:T(8,128)(2,1)S(1)}, bf16[128,2048]{1,0:T(8,128)(2,1)S(1)}, u32[]{:S(2)}, u32[]{:S(2)}) collective-permute-start(bf16[128,2048]{1,0:T(8,128)(2,1)S(1)} %get-tuple-element.32), channel_id=1, source_target_pairs={{0,8},{4,12},{8,0},{12,4},{16,24},{20,28},{24,16},{28,20},{1,9},{5... | collective-permute-start | bytes 1572872 | tf_op jit(solution)/shard_map/ppermute | solution.py:201
  150.0 16.8 %collective-permute-start.30 = (bf16[64,2048]{1,0:T(8,128)(2,1)S(1)}, bf16[64,2048]{1,0:T(8,128)(2,1)S(1)}, u32[]{:S(2)}, u32[]{:S(2)}) collective-permute-start(bf16[64,2048]{1,0:T(8,128)(2,1)S(1)} %collective-permute-done.29), channel_id=1, source_target_pairs={{0,24},{4,28},{8,0},{12,4},{16,8},{20,12},{24,16},{28,20},{1,25},{... | collective-permute-start | bytes 786440 | tf_op jit(solution)/shard_map/ppermute | solution.py:430
  151.4 23.6 %collective-permute-start.45 = (bf16[128,2048]{1,0:T(8,128)(2,1)S(1)}, bf16[128,2048]{1,0:T(8,128)(2,1)S(1)}, u32[]{:S(2)}, u32[]{:S(2)}) collective-permute-start(bf16[128,2048]{1,0:T(8,128)(2,1)S(1)} %collective-permute-done.43.refs_0_), channel_id=1, source_target_pairs={{0,1},{1,0},{2,3},{3,2},{4,5},{5,4},{6,7},{7,6},{8,9},{9,8},{10,11... | collective-permute-start | bytes 1572872 | tf_op jit(solution)/shard_map/ppermute | solution.py:201
  151.4 24.1 %collective-permute-start.46 = (bf16[128,2048]{1,0:T(8,128)(2,1)S(1)}, bf16[128,2048]{1,0:T(8,128)(2,1)S(1)}, u32[]{:S(2)}, u32[]{:S(2)}) collective-permute-start(bf16[128,2048]{1,0:T(8,128)(2,1)S(1)} %collective-permute-done.44.refs_1_), channel_id=1, source_target_pairs={{0,1},{1,0},{2,3},{3,2},{4,5},{5,4},{6,7},{7,6},{8,9},{9,8},{10,11... | collective-permute-start | bytes 1572872 | tf_op jit(solution)/shard_map/ppermute | solution.py:201
  151.9 17.5 %collective-permute-start.33 = (bf16[64,2048]{1,0:T(8,128)(2,1)S(1)}, bf16[64,2048]{1,0:T(8,128)(2,1)S(1)}, u32[]{:S(2)}, u32[]{:S(2)}) collective-permute-start(bf16[64,2048]{1,0:T(8,128)(2,1)S(1)} %collective-permute-done.32.refs_2_), channel_id=1, source_target_pairs={{0,2},{1,3},{2,0},{3,1},{4,6},{5,7},{6,4},{7,5},{8,10},{9,11},{10,... | collective-permute-start | bytes 786440 | tf_op jit(solution)/shard_map/ppermute | solution.py:201
  168.2 16.3 %collective-permute-start.15 = (bf16[128,2048]{1,0:T(8,128)(2,1)S(1)}, bf16[128,2048]{1,0:T(8,128)(2,1)S(1)}, u32[]{:S(2)}, u32[]{:S(2)}) collective-permute-start(bf16[128,2048]{1,0:T(8,128)(2,1)S(1)} %get-tuple-element.28), channel_id=1, source_target_pairs={{0,4},{4,0},{8,12},{12,8},{16,20},{20,16},{24,28},{28,24},{1,5},{5... | collective-permute-start | bytes 1572872 | tf_op jit(solution)/shard_map/ppermute | solution.py:201
  169.4 15.7 %collective-permute-start.36 = (bf16[64,2048]{1,0:T(8,128)(2,1)S(1)}, bf16[64,2048]{1,0:T(8,128)(2,1)S(1)}, u32[]{:S(2)}, u32[]{:S(2)}) collective-permute-start(bf16[64,2048]{1,0:T(8,128)(2,1)S(1)} %collective-permute-done.32.refs_2_), channel_id=1, source_target_pairs={{0,1},{1,0},{2,3},{3,2},{4,5},{5,4},{6,7},{7,6},{8,9},{9,8},{10,11... | collective-permute-start | bytes 786440 | tf_op jit(solution)/shard_map/ppermute | solution.py:201
  184.6 20.2 %collective-permute-start.16 = (bf16[128,2048]{1,0:T(8,128)(2,1)S(1)}, bf16[128,2048]{1,0:T(8,128)(2,1)S(1)}, u32[]{:S(2)}, u32[]{:S(2)}) collective-permute-start(bf16[128,2048]{1,0:T(8,128)(2,1)S(1)} %get-tuple-element.27.refs_0_), channel_id=1, source_target_pairs={{0,1},{1,0},{2,3},{3,2},{4,5},{5,4},{6,7},{7,6},{8,9},{9,8},{10,11... | collective-permute-start | bytes 1572872 | tf_op jit(solution)/shard_map/ppermute | solution.py:201
  185.6 19.1 %collective-permute-start.17 = (bf16[128,2048]{1,0:T(8,128)(2,1)S(1)}, bf16[128,2048]{1,0:T(8,128)(2,1)S(1)}, u32[]{:S(2)}, u32[]{:S(2)}) collective-permute-start(bf16[128,2048]{1,0:T(8,128)(2,1)S(1)} %collective-permute-done.15.refs_1_), channel_id=1, source_target_pairs={{0,1},{1,0},{2,3},{3,2},{4,5},{5,4},{6,7},{7,6},{8,9},{9,8},{10,11... | collective-permute-start | bytes 1572872 | tf_op jit(solution)/shard_map/ppermute | solution.py:201
  185.7 28.2 %collective-permute-start.47 = (bf16[256,2048]{1,0:T(8,128)(2,1)S(1)}, bf16[256,2048]{1,0:T(8,128)(2,1)}, u32[]{:S(2)}, u32[]{:S(2)}) collective-permute-start(bf16[256,2048]{1,0:T(8,128)(2,1)S(1)} %get-tuple-element.42), channel_id=1, source_target_pairs={{0,1},{1,0},{2,3},{3,2},{4,5},{5,4},{6,7},{7,6},{8,9},{9,8},{10,11... | collective-permute-start | bytes 3145736 | tf_op jit(solution)/shard_map/ppermute | solution.py:201
  195.1 21.5 %collective-permute-start.38 = (bf16[256,2048]{1,0:T(8,128)(2,1)S(1)}, bf16[256,2048]{1,0:T(8,128)(2,1)S(1)}, u32[]{:S(2)}, u32[]{:S(2)}) collective-permute-start(bf16[256,2048]{1,0:T(8,128)(2,1)S(1)} %get-tuple-element.38), channel_id=1, source_target_pairs={{0,1},{1,0},{2,3},{3,2},{4,5},{5,4},{6,7},{7,6},{8,9},{9,8},{10,11... | collective-permute-start | bytes 3145736 | tf_op jit(solution)/shard_map/ppermute | solution.py:201
  216.7 24.4 %collective-permute-start.39 = (bf16[2,64,2048]{2,1,0:T(8,128)(2,1)S(1)}, bf16[2,64,2048]{2,1,0:T(8,128)(2,1)S(1)}, u32[]{:S(2)}, u32[]{:S(2)}) collective-permute-start(bf16[2,64,2048]{2,1,0:T(8,128)(2,1)S(1)} %fusion.6), channel_id=1, source_target_pairs={{0,2},{1,3},{2,0},{3,1},{4,6},{5,7},{6,4},{7,5},{8,10},{9,11},{10,... | collective-permute-start | bytes 1572872 | tf_op jit(solution)/shard_map/ppermute | solution.py:201
  217.5 34.9 %collective-permute-start.26 = (bf16[2,64,2048]{2,1,0:T(8,128)(2,1)S(1)}, bf16[2,64,2048]{2,1,0:T(8,128)(2,1)S(1)}, u32[]{:S(2)}, u32[]{:S(2)}) collective-permute-start(bf16[2,64,2048]{2,1,0:T(8,128)(2,1)S(1)} %fusion.5), channel_id=1, source_target_pairs={{0,2},{1,3},{2,0},{3,1},{4,6},{5,7},{6,4},{7,5},{8,10},{9,11},{10,... | collective-permute-start | bytes 1572872 | tf_op jit(solution)/shard_map/ppermute | solution.py:201
  219.1 43.9 %collective-permute-start.19 = (bf16[2,64,2048]{2,1,0:T(8,128)(2,1)S(1)}, bf16[2,64,2048]{2,1,0:T(8,128)(2,1)S(1)}, u32[]{:S(2)}, u32[]{:S(2)}) collective-permute-start(bf16[2,64,2048]{2,1,0:T(8,128)(2,1)S(1)} %fusion.4), channel_id=1, source_target_pairs={{0,2},{1,3},{2,0},{3,1},{4,6},{5,7},{6,4},{7,5},{8,10},{9,11},{10,... | collective-permute-start | bytes 1572872 | tf_op jit(solution)/shard_map/ppermute | solution.py:201
  231.2 32.8 %collective-permute-start.49 = (bf16[64,2048]{1,0:T(8,128)(2,1)S(1)}, bf16[64,2048]{1,0:T(8,128)(2,1)S(1)}, u32[]{:S(2)}, u32[]{:S(2)}) collective-permute-start(bf16[64,2048]{1,0:T(8,128)(2,1)S(1)} %get-tuple-element.44), channel_id=1, source_target_pairs={{0,24},{4,28},{8,16},{12,20},{16,8},{20,12},{24,0},{28,4},{1,25},{... | collective-permute-start | bytes 786440 | tf_op jit(solution)/shard_map/ppermute | solution.py:201
  231.3 35.4 %collective-permute-start.50 = (bf16[64,2048]{1,0:T(8,128)(2,1)S(1)}, bf16[64,2048]{1,0:T(8,128)(2,1)S(1)}, u32[]{:S(2)}, u32[]{:S(2)}) collective-permute-start(bf16[64,2048]{1,0:T(8,128)(2,1)S(1)} %get-tuple-element.43), channel_id=1, source_target_pairs={{0,28},{4,24},{8,20},{12,16},{16,12},{20,8},{24,4},{28,0},{1,29},{... | collective-permute-start | bytes 786440 | tf_op jit(solution)/shard_map/ppermute | solution.py:201
  241.5 26.1 %collective-permute-start.41 = (bf16[64,2048]{1,0:T(8,128)(2,1)S(1)}, bf16[64,2048]{1,0:T(8,128)(2,1)}, u32[]{:S(2)}, u32[]{:S(2)}) collective-permute-start(bf16[64,2048]{1,0:T(8,128)(2,1)S(1)} %get-tuple-element.45), channel_id=1, source_target_pairs={{0,28},{4,24},{8,4},{12,0},{16,12},{20,8},{24,20},{28,16},{1,29},{... | collective-permute-start | bytes 786440 | tf_op jit(solution)/shard_map/ppermute | solution.py:429
  252.4 20.8 %collective-permute-start.40 = (bf16[64,2048]{1,0:T(8,128)(2,1)S(1)}, bf16[64,2048]{1,0:T(8,128)(2,1)S(1)}, u32[]{:S(2)}, u32[]{:S(2)}) collective-permute-start(bf16[64,2048]{1,0:T(8,128)(2,1)S(1)} %get-tuple-element.46), channel_id=1, source_target_pairs={{0,16},{4,20},{8,24},{12,28},{16,0},{20,4},{24,8},{28,12},{1,17},{... | collective-permute-start | bytes 786440 | tf_op jit(solution)/shard_map/ppermute | solution.py:201
  264.1 18.6 %collective-permute-start.28 = (bf16[64,2048]{1,0:T(8,128)(2,1)S(1)}, bf16[64,2048]{1,0:T(8,128)(2,1)S(1)}, u32[]{:S(2)}, u32[]{:S(2)}) collective-permute-start(bf16[64,2048]{1,0:T(8,128)(2,1)S(1)} %get-tuple-element.47), channel_id=1, source_target_pairs={{0,12},{4,8},{8,4},{12,0},{16,28},{20,24},{24,20},{28,16},{1,13},{... | collective-permute-start | bytes 786440 | tf_op jit(solution)/shard_map/ppermute | solution.py:201
  266.7 16.0 %collective-permute-start.20 = (bf16[64,2048]{1,0:T(8,128)(2,1)}, bf16[64,2048]{1,0:T(8,128)(2,1)S(1)}, u32[]{:S(2)}, u32[]{:S(2)}) collective-permute-start(bf16[64,2048]{1,0:T(8,128)(2,1)} %get-tuple-element.49), channel_id=1, source_target_pairs={{0,4},{4,0},{8,12},{12,8},{16,20},{20,16},{24,28},{28,24},{1,5},{5... | collective-permute-start | bytes 786440 | tf_op jit(solution)/shard_map/ppermute | solution.py:201
  267.5 19.5 %collective-permute-start.42 = (bf16[64,2048]{1,0:T(8,128)(2,1)}, bf16[64,2048]{1,0:T(8,128)(2,1)S(1)}, u32[]{:S(2)}, u32[]{:S(2)}) collective-permute-start(bf16[64,2048]{1,0:T(8,128)(2,1)} %collective-permute-done.41), channel_id=1, source_target_pairs={{0,24},{4,28},{8,0},{12,4},{16,8},{20,12},{24,16},{28,20},{1,25},{... | collective-permute-start | bytes 786440 | tf_op jit(solution)/shard_map/ppermute | solution.py:430
  (30 other events, 659.6 us)
where the time goes:
time: 290 us
  waiting for transfers between devices  118 us (41%)
  starting transfers between devices  106 us (37%)
  Pallas kernels  50.8 us (18%)
  local copies, waits for them, and re-layouts  8.64 us (3%)
  other arithmetic  5.92 us (2%)
    ppermute x37, starting transfers between devices, swap(): lax.ppermute(x, axis, [(i, i ^ bits) for i in range(lax.axis_size(axis))])  72.9 us
    ppermute x37, waiting for transfers between devices, swap(): lax.ppermute(x, axis, [(i, i ^ bits) for i in range(lax.axis_size(axis))])  66.1 us
    pallas_call x4, Pallas kernels, on_device(): pl.pallas_call(expert, grid=(hidden_width // h_tile,), out_shape=[jax.Sha...  35.9 us
    ppermute x2, waiting for transfers between devices, hop(): return lax.ppermute(x, 'sp', [(i, (i - step) % n_sp) for i in range(n_sp)])  17.7 us
    ppermute x4, starting transfers between devices, chain(): own.append(lax.ppermute(own[-1], 'sp', ahead))  17 us
    ppermute x2, waiting for transfers between devices, hop(): lax.ppermute(x, 'sp', [(i, ((i ^ low) - step) % n_sp) for i in range(n_sp)])  15.8 us
    ppermute x6, waiting for transfers between devices, chain(): other.append(lax.ppermute(own[-1], 'sp', pairs))  15.2 us
    ppermute x6, starting transfers between devices, chain(): other.append(lax.ppermute(own[-1], 'sp', pairs))  10.9 us
  transfers between devices with their start and end apart: 51, of which 17 were waited for; matrix products, arithmetic and copies ran while one was open for 2% of the time, Pallas kernels for 16%

commit v1 on v0

--- a/solution.py
+++ b/solution.py
@@ -201,19 +201,43 @@
     return lax.ppermute(x, axis, [(i, i ^ bits) for i in range(lax.axis_size(axis))])
 
 
-def far_places(n_sp):
-    return [k for k in range(n_sp) if k & (n_sp // 2) and not k & (n_sp // 4)]
+def ways(n_sp):
+    inner = n_sp // 4
+    return [(step, bits) for step in range(4) for bits in range(inner)]
+
+
+def both_blocks(way):
+    return way in ((0, 0), (1, 0), (3, 0))
 
 
 def expert_groups(n_sp):
-    far = far_places(n_sp)
-    near = [k ^ (k >> 1) for k in range(n_sp)]
-    near = [k for k in near if k not in far]
-    size = n_sp // 4
-    return [near[:size], near[size : 2 * size], far[::-1], near[2 * size :]]
-
-
-def project_kernel(experts, capacity, n_tp, far, *refs):
+    inner = n_sp // 4
+    low, high = range(inner // 2), range(inner // 2, inner)
+    return [
+        [(0, bits) for bits in range(inner)],
+        [(step, bits) for bits in low for step in (1, 3)],
+        [(step, bits) for bits in high for step in (1, 3)],
+        [(2, bits) for bits in range(inner)],
+    ]
+
+
+def move(x, way):
+    step, bits = way
+    n_sp = lax.axis_size("sp")
+    inner = n_sp // 4
+    return lax.ppermute(
+        x,
+        "sp",
+        [(i, ((i // inner + step) % 4) * inner + ((i % inner) ^ bits)) for i in range(n_sp)],
+    )
+
+
+def expert_at(place, n_sp, way):
+    inner = n_sp // 4
+    return ((place // inner + way[0]) % 4) * inner + ((place % inner) ^ way[1])
+
+
+def project_kernel(experts, capacity, n_tp, *refs):
     blocks = n_tp // 2
     place_ref = refs[0]
     pieces = refs[1 : 1 + n_tp]
@@ -271,10 +295,11 @@
         slot_ref[j] = jnp.where(chosen > 0.0, ranks, -1.0)
     slot_ids = lax.broadcasted_iota(jnp.int32, (capacity, rows), 0).astype(jnp.float32)
     first, spans = 0, []
-    for k in range(experts):
+    for way in ways(experts):
         spans.append(first)
-        for j in range(1 if k in far else blocks):
-            row_of = slot_ref[j, pl.ds(place ^ k, 1), :]
+        expert = expert_at(place, experts, way)
+        for j in range(blocks if both_blocks(way) else 1):
+            row_of = slot_ref[j, pl.ds(expert, 1), :]
             for i in range(blocks):
                 pick = (slot_ids == row_of) if i == j else jnp.zeros((capacity, rows), jnp.bool_)
                 pick_ref[first : first + capacity, i * rows : (i + 1) * rows] = pick.astype(
@@ -333,6 +358,7 @@
     mixed_ref, stack_ref = refs[experts:]
     rows, width = stream_ref.shape
     capacity = outs[0].shape[0]
+    place, inner = place_ref[0], experts // 4
     for k in range(experts):
         stack_ref[k * capacity : (k + 1) * capacity, :] = outs[k][...]
     expert_ids = lax.broadcasted_iota(jnp.int32, (rows, experts), 1)
@@ -350,7 +376,9 @@
     picks = []
     for route in range(2):
         rank = jnp.sum(named[route] * ranks, axis=1, keepdims=True).astype(jnp.int32)
-        target = (routes_ref[:, route : route + 1] ^ place_ref[0]) * capacity + rank
+        expert = routes_ref[:, route : route + 1]
+        step = (expert // inner + 4 - place // inner) % 4
+        target = (step * inner + ((expert % inner) ^ (place % inner))) * capacity + rank
         picks.append((slot_ids == target).astype(jnp.float32).astype(jnp.bfloat16))
     n_tile = 512
     for n in range(width // n_tile):
@@ -399,11 +427,10 @@
     mine, other = attend(queries, keys, values, cum_gate, documents, head_gain)
     pieces = [mine] + [swap(other if k % 2 else mine, "tp", k) for k in range(1, n_tp)]
 
-    far = far_places(n_sp)
-    counts = [capacity if k in far else each for k in range(n_sp)]
+    counts = [each if both_blocks(way) else capacity for way in ways(n_sp)]
 
     def project(*refs):
-        project_kernel(n_sp, capacity, n_tp, far, *refs)
+        project_kernel(n_sp, capacity, n_tp, *refs)
 
     *outbound, stream = pl.pallas_call(
         project,
@@ -421,28 +448,34 @@
         name="project",
     )(places, *pieces, out_weight, *resids, *route_blocks, norm_gain[None, :])
 
-    def hop(x, k):
-        if k == 0:
+    outbound = dict(zip(ways(n_sp), outbound))
+
+    def dispatch(way):
+        step, bits = way
+        x = outbound[way]
+        if way == (0, 0):
             return x
-        if k in far and k % 2:
-            low, step = k % (n_sp // 2), n_sp // 4
-            x = lax.ppermute(x, "sp", [(i, ((i ^ low) - step) % n_sp) for i in range(n_sp)])
-            return lax.ppermute(x, "sp", [(i, (i - step) % n_sp) for i in range(n_sp)])
-        return swap(x, "sp", k)
+        if step == 0 or bits == 0:
+            return move(x, way)
+        x = move(x, (0, bits))
+        if step == 2:
+            x = move(x, (3, 0))
+            return move(x, (3, 0))
+        return move(x, (step, 0))
 
     groups = expert_groups(n_sp)
     members = len(groups[0])
     hidden_width = w_gate.shape[2]
     h_tile = 128
     rows = 2 * members * each
-    arrived = {k: hop(outbound[k], k) for group in groups for k in group}
+    arrived = {way: dispatch(way) for way in ways(n_sp)}
     returned = {}
     for group in groups:
         inputs = []
-        for k in group:
-            inputs.append(arrived[k])
-            if k in far:
-                inputs += [swap(arrived[k], "tp", 2 * j) for j in range(1, blocks)]
+        for way in group:
+            inputs.append(arrived[way])
+            if not both_blocks(way):
+                inputs += [swap(arrived[way], "tp", 2 * j) for j in range(1, blocks)]
         inputs += [swap(x, "tp", 1) for x in inputs]
 
         def expert(*refs):
@@ -484,8 +517,9 @@
             sent = swap(summed(j).astype(jnp.bfloat16), "tp", 2 * j)
             result = result + sent.astype(jnp.float32)
         result = result.astype(jnp.bfloat16)
-        for i, k in enumerate(group):
-            returned[k] = hop(result[i], k)
+        for i, way in enumerate(group):
+            back = (-way[0] % 4, way[1])
+            returned[way] = result[i] if way == (0, 0) else move(result[i], back)
 
     def combine(*refs):
         combine_kernel(n_sp, *refs)
@@ -498,7 +532,7 @@
         scratch_shapes=[pltpu.VMEM((n_sp * capacity, model_width), jnp.bfloat16)],
         compiler_params=pltpu.CompilerParams(vmem_limit_bytes=24 * 2**20),
         name="combine",
-    )(places, stream, routes, route_weights, *[returned[k] for k in range(n_sp)])
+    )(places, stream, routes, route_weights, *[returned[way] for way in ways(n_sp)])
 
 
 def solution(mesh):

time: 290 us -> 282 us (0.972)
  waiting for transfers between devices: 118 us -> 115 us
    ppermute x37 -> x31, starting transfers between devices: 72.9 us -> 18.9 us  [swap(): lax.ppermute(x, axis, [(i, i ^ bits) for i in range(lax.axis_size(axis))])]
    ppermute x4 -> x18, starting transfers between devices: 4.71 us -> 56.8 us  [move(): lax.ppermute(x, 'sp', [(i, (i // inner + step) % 4 * inner + (i % inner ^...]
    ppermute x37 -> x31, waiting for transfers between devices: 66.1 us -> 40.5 us  [swap(): lax.ppermute(x, axis, [(i, i ^ bits) for i in range(lax.axis_size(axis))])]
    ppermute x4 -> x18, waiting for transfers between devices: 33.4 us -> 55.5 us  [move(): lax.ppermute(x, 'sp', [(i, (i // inner + step) % 4 * inner + (i % inner ^...]
  transfers between devices with their start and end apart: 51 -> 59, of which waited for: 17 -> 15; matrix products, arithmetic and copies ran while one was open for 2% -> 2% of each run, Pallas kernels for 16% -> 16%
where the time goes in v1:
time: 282 us
  waiting for transfers between devices  115 us (41%)
  starting transfers between devices  104 us (37%)
  Pallas kernels  50.6 us (18%)
  local copies, waits for them, and re-layouts  8.76 us (3%)
  other arithmetic  3.77 us (1%)
    ppermute x18, starting transfers between devices, move(): lax.ppermute(x, 'sp', [(i, (i // inner + step) % 4 * inner + (i % inner ^...  56.8 us
    ppermute x18, waiting for transfers between devices, move(): lax.ppermute(x, 'sp', [(i, (i // inner + step) % 4 * inner + (i % inner ^...  55.5 us
    ppermute x31, waiting for transfers between devices, swap(): lax.ppermute(x, axis, [(i, i ^ bits) for i in range(lax.axis_size(axis))])  40.5 us
    pallas_call x4, Pallas kernels, on_device(): pl.pallas_call(expert, grid=(hidden_width // h_tile,), out_shape=[jax.Sha...  35.9 us
    ppermute x31, starting transfers between devices, swap(): lax.ppermute(x, axis, [(i, i ^ bits) for i in range(lax.axis_size(axis))])  18.9 us
    ppermute x4, starting transfers between devices, chain(): own.append(lax.ppermute(own[-1], 'sp', ahead))  17 us
    ppermute x6, waiting for transfers between devices, chain(): other.append(lax.ppermute(own[-1], 'sp', pairs))  15.2 us
    ppermute x6, starting transfers between devices, chain(): other.append(lax.ppermute(own[-1], 'sp', pairs))  10.9 us
  transfers between devices with their start and end apart: 59, of which 15 were waited for; matrix products, arithmetic and copies ran while one was open for 2% of the time, Pallas kernels for 16%

profile of v1, /device:TPU:0, one launch (start us, length us, event | category | flops | bytes accessed | tf_op | source)
XLA Modules:
  0.0 282.0 jit_solution(4252389404186635171)
XLA Ops:
  2.6 5.0 %collective-permute-start.2 = (bf16[544,256]{1,0:T(8,128)(2,1)S(1)}, bf16[544,256]{1,0:T(8,128)(2,1)S(1)}, u32[]{:S(2)}, u32[]{:S(2)}) collective-permute-start(bf16[544,256]{1,0:T(8,128)(2,1)S(1)} %concatenate.10.refs_5_), channel_id=1, source_target_pairs={{0,8},{4,12},{8,16},{12,20},{16,24},{20,28},{1,9},{5,13},{9,17},{1... | collective-permute-start | bytes 835592 | tf_op jit(solution)/shard_map/ppermute | solution.py:159
  7.5 3.5 %collective-permute-start.3 = (bf16[512,256]{1,0:T(8,128)(2,1)}, bf16[512,256]{1,0:T(8,128)(2,1)S(1)}, u32[]{:S(2)}, u32[]{:S(2)}) collective-permute-start(bf16[512,256]{1,0:T(8,128)(2,1)} %refs_6_.2), channel_id=1, source_target_pairs={{0,8},{4,12},{8,16},{12,20},{16,24},{20,28},{1,9},{5,13},{9,17},{1... | collective-permute-start | bytes 786440 | tf_op jit(solution)/shard_map/ppermute | solution.py:159
  11.0 3.5 %collective-permute-done.2.refs_9_ = bf16[544,256]{1,0:T(8,128)(2,1)S(1)} collective-permute-done((bf16[544,256]{1,0:T(8,128)(2,1)S(1)}, bf16[544,256]{1,0:T(8,128)(2,1)S(1)}, u32[]{:S(2)}, u32[]{:S(2)}) %collective-permute-start.2) | collective-permute-done | bytes 278560 | tf_op jit(solution)/shard_map/ppermute | solution.py:159
  14.5 4.4 %collective-permute-start.6 = (bf16[544,256]{1,0:T(8,128)(2,1)S(1)}, bf16[544,256]{1,0:T(8,128)(2,1)S(1)}, u32[]{:S(2)}, u32[]{:S(2)}) collective-permute-start(bf16[544,256]{1,0:T(8,128)(2,1)S(1)} %collective-permute-done.2.refs_9_), channel_id=1, source_target_pairs={{0,8},{4,12},{8,16},{12,20},{16,24},{20,28},{1,9},{5,13},{9,17},{1... | collective-permute-start | bytes 835592 | tf_op jit(solution)/shard_map/ppermute | solution.py:159
  18.9 3.4 %collective-permute-start.1 = (bf16[512,256]{1,0:T(8,128)(2,1)}, bf16[512,256]{1,0:T(8,128)(2,1)S(1)}, u32[]{:S(2)}, u32[]{:S(2)}) collective-permute-start(bf16[512,256]{1,0:T(8,128)(2,1)} %refs_6_.2), channel_id=1, source_target_pairs={{0,4},{8,12},{16,20},{24,28},{1,5},{9,13},{17,21},{25,29},{2,6},{1... | collective-permute-start | bytes 786440 | tf_op jit(solution)/shard_map/ppermute | solution.py:160
  22.4 4.2 %collective-permute-start.7 = (bf16[512,256]{1,0:T(8,128)(2,1)S(1)}, bf16[512,256]{1,0:T(8,128)(2,1)}, u32[]{:S(2)}, u32[]{:S(2)}) collective-permute-start(bf16[512,256]{1,0:T(8,128)(2,1)S(1)} %collective-permute-done.3.refs_10_), channel_id=1, source_target_pairs={{0,8},{4,12},{8,16},{12,20},{16,24},{20,28},{1,9},{5,13},{9,17},{1... | collective-permute-start | bytes 786440 | tf_op jit(solution)/shard_map/ppermute | solution.py:159
  38.1 11.0 %collective-permute-done.5.refs_12_ = bf16[512,256]{1,0:T(8,128)(2,1)} collective-permute-done((bf16[512,256]{1,0:T(8,128)(2,1)S(1)}, bf16[512,256]{1,0:T(8,128)(2,1)}, u32[]{:S(2)}, u32[]{:S(2)}) %collective-permute-start.5) | collective-permute-done | bytes 262176 | tf_op jit(solution)/shard_map/ppermute | solution.py:160
  55.2 9.2 %attention.1 = (bf16[256,256]{1,0:T(8,128)(2,1)S(1)}, bf16[256,256]{1,0:T(8,128)(2,1)S(1)}) custom-call(s32[7]{0:T(128)S(1)} %convert_element_type.136.refs_0_, s32[512]{0:T(512)S(1)} %copy-done.5, bf16[512,256]{1,0:T(8,128)(2,1)S(1)} %copy-done.2, f32[512,8]{1,0:T(8,128)S(1)} %copy.38.refs_3_, f32[1,256]{1,0:T(1,128)S(1)} %bitcast.143, ...), custom_call_target="tpu_custom_call" | custom-call | tf_op jit(solution)/shard_map/attention/pallas_call | solution.py:185
  68.2 5.0 %collective-permute-done.14.refs_9_ = f32[8,128]{1,0:T(8,128)S(1)} collective-permute-done((f32[8,128]{1,0:T(8,128)S(1)}, f32[8,128]{1,0:T(8,128)S(1)}, u32[]{:S(2)}, u32[]{:S(2)}) %collective-permute-start.14) | collective-permute-done | bytes 4128 | tf_op jit(solution)/shard_map/ppermute | solution.py:201
  75.4 3.0 %project.1 = (bf16[128,2048]{1,0:T(8,128)(2,1)S(1)}, bf16[64,2048]{1,0:T(8,128)(2,1)S(1)}, bf16[128,2048]{1,0:T(8,128)(2,1)S(1)}, bf16[64,2048]{1,0:T(8,128)(2,1...) custom-call(s32[2]{0:T(128)S(1)} %pad_add_fusion.refs_0_, ...), custom_call_target="tpu_custom_call" | custom-call | tf_op jit(solution)/shard_map/project/pallas_call | solution.py:435
  78.4 5.1 %collective-permute-start.15 = (bf16[64,2048]{1,0:T(8,128)(2,1)S(1)}, bf16[64,2048]{1,0:T(8,128)(2,1)S(1)}, u32[]{:S(2)}, u32[]{:S(2)}) collective-permute-start(bf16[64,2048]{1,0:T(8,128)(2,1)S(1)} %get-tuple-element.28), channel_id=1, source_target_pairs={{0,4},{4,0},{8,12},{12,8},{16,20},{20,16},{24,28},{28,24},{1,5},{5... | collective-permute-start | bytes 786440 | tf_op jit(solution)/shard_map/ppermute | solution.py:228
  85.5 11.9 %collective-permute-start.23 = (bf16[128,2048]{1,0:T(8,128)(2,1)S(1)}, bf16[128,2048]{1,0:T(8,128)(2,1)S(1)}, u32[]{:S(2)}, u32[]{:S(2)}) collective-permute-start(bf16[128,2048]{1,0:T(8,128)(2,1)S(1)} %get-tuple-element.31), channel_id=1, source_target_pairs={{0,8},{4,12},{8,16},{12,20},{16,24},{20,28},{24,0},{28,4},{1,9},{5... | collective-permute-start | bytes 1572872 | tf_op jit(solution)/shard_map/ppermute | solution.py:228
  97.4 6.6 %collective-permute-start.43 = (bf16[64,2048]{1,0:T(8,128)(2,1)S(1)}, bf16[64,2048]{1,0:T(8,128)(2,1)S(1)}, u32[]{:S(2)}, u32[]{:S(2)}) collective-permute-start(bf16[64,2048]{1,0:T(8,128)(2,1)S(1)} %get-tuple-element.39), channel_id=1, source_target_pairs={{0,16},{4,20},{8,24},{12,28},{16,0},{20,4},{24,8},{28,12},{1,17},{... | collective-permute-start | bytes 786440 | tf_op jit(solution)/shard_map/ppermute | solution.py:228
  106.0 20.1 %collective-permute-done.43.refs_0_ = bf16[64,2048]{1,0:T(8,128)(2,1)S(1)} collective-permute-done((bf16[64,2048]{1,0:T(8,128)(2,1)S(1)}, bf16[64,2048]{1,0:T(8,128)(2,1)S(1)}, u32[]{:S(2)}, u32[]{:S(2)}) %collective-permute-start.43) | collective-permute-done | bytes 262176 | tf_op jit(solution)/shard_map/ppermute | solution.py:228
  127.6 5.9 %collective-permute-start.31 = (bf16[64,2048]{1,0:T(8,128)(2,1)S(1)}, bf16[64,2048]{1,0:T(8,128)(2,1)S(1)}, u32[]{:S(2)}, u32[]{:S(2)}) collective-permute-start(bf16[64,2048]{1,0:T(8,128)(2,1)S(1)} %collective-permute-done.30), channel_id=1, source_target_pairs={{0,8},{4,12},{8,16},{12,20},{16,24},{20,28},{24,0},{28,4},{1,9},{5... | collective-permute-start | bytes 786440 | tf_op jit(solution)/shard_map/ppermute | solution.py:228
  133.6 2.9 %collective-permute-start.34 = (bf16[64,2048]{1,0:T(8,128)(2,1)S(1)}, bf16[64,2048]{1,0:T(8,128)(2,1)S(1)}, u32[]{:S(2)}, u32[]{:S(2)}) collective-permute-start(bf16[64,2048]{1,0:T(8,128)(2,1)S(1)} %collective-permute-done.33), channel_id=1, source_target_pairs={{0,24},{4,28},{8,0},{12,4},{16,8},{20,12},{24,16},{28,20},{1,25},{... | collective-permute-start | bytes 786440 | tf_op jit(solution)/shard_map/ppermute | solution.py:228
  137.0 7.0 %collective-permute-start.46 = (bf16[64,2048]{1,0:T(8,128)(2,1)S(1)}, bf16[64,2048]{1,0:T(8,128)(2,1)S(1)}, u32[]{:S(2)}, u32[]{:S(2)}) collective-permute-start(bf16[64,2048]{1,0:T(8,128)(2,1)S(1)} %collective-permute-done.45), channel_id=1, source_target_pairs={{0,24},{4,28},{8,0},{12,4},{16,8},{20,12},{24,16},{28,20},{1,25},{... | collective-permute-start | bytes 786440 | tf_op jit(solution)/shard_map/ppermute | solution.py:228
  144.5 3.9 %collective-permute-done.34.refs_2_ = bf16[64,2048]{1,0:T(8,128)(2,1)S(1)} collective-permute-done((bf16[64,2048]{1,0:T(8,128)(2,1)S(1)}, bf16[64,2048]{1,0:T(8,128)(2,1)S(1)}, u32[]{:S(2)}, u32[]{:S(2)}) %collective-permute-start.34) | collective-permute-done | bytes 262176 | tf_op jit(solution)/shard_map/ppermute | solution.py:228
  148.9 4.3 %collective-permute-done.46 = bf16[64,2048]{1,0:T(8,128)(2,1)S(1)} collective-permute-done((bf16[64,2048]{1,0:T(8,128)(2,1)S(1)}, bf16[64,2048]{1,0:T(8,128)(2,1)S(1)}, u32[]{:S(2)}, u32[]{:S(2)}) %collective-permute-start.46) | collective-permute-done | bytes 262176 | tf_op jit(solution)/shard_map/ppermute | solution.py:228
  155.2 3.7 %collective-permute-start.47 = (bf16[64,2048]{1,0:T(8,128)(2,1)S(1)}, bf16[64,2048]{1,0:T(8,128)(2,1)S(1)}, u32[]{:S(2)}, u32[]{:S(2)}) collective-permute-start(bf16[64,2048]{1,0:T(8,128)(2,1)S(1)} %collective-permute-done.46), channel_id=1, source_target_pairs={{0,24},{4,28},{8,0},{12,4},{16,8},{20,12},{24,16},{28,20},{1,25},{... | collective-permute-start | bytes 786440 | tf_op jit(solution)/shard_map/ppermute | solution.py:228
  158.9 9.0 %expert.4 = (bf16[256,2048]{1,0:T(8,128)(2,1)S(1)}, bf16[256,2048]{1,0:T(8,128)(2,1)S(1)}) custom-call(bf16[128,2048]{1,0:T(8,128)(2,1)S(1)} %get-tuple-element.27.refs_0_, bf16[64,2048]{1,0:T(8,128)(2,1)S(1)} %collective-permute-done.15.refs_1_, bf16[64,2048]{1,0:T(8,128)(2,1)S(1)} %collective-permute-done.16.refs_2_, ...), custom_call_target="tpu_custom_call" | custom-call | flops 5637144576 | bytes 15204352 | tf_op jit(solution)/shard_map/expert/pallas_call | solution.py:484
  169.5 9.0 %expert.5 = (bf16[256,2048]{1,0:T(8,128)(2,1)S(1)}, bf16[256,2048]{1,0:T(8,128)(2,1)S(1)}) custom-call(bf16[128,2048]{1,0:T(8,128)(2,1)S(1)} %collective-permute-done.23.refs_0_, bf16[128,2048]{1,0:T(8,128)(2,1)S(1)} %collective-permute-done.24.refs_1_, bf16[128,2048]{1,0:T(8,128)(2,1)S(1)} %collective-permute-done.25.refs_2_, ...), custom_call_target="tpu_custom_call" | custom-call | flops 5637144576 | bytes 15204352 | tf_op jit(solution)/shard_map/expert/pallas_call | solution.py:484
  179.7 9.0 %expert.6 = (bf16[256,2048]{1,0:T(8,128)(2,1)S(1)}, bf16[256,2048]{1,0:T(8,128)(2,1)S(1)}) custom-call(bf16[64,2048]{1,0:T(8,128)(2,1)S(1)} %collective-permute-done.31.refs_0_, bf16[64,2048]{1,0:T(8,128)(2,1)S(1)} %collective-permute-done.32.refs_1_, bf16[64,2048]{1,0:T(8,128)(2,1)S(1)} %collective-permute-done.34.refs_2_, ...), custom_call_target="tpu_custom_call" | custom-call | flops 5637144576 | bytes 15204352 | tf_op jit(solution)/shard_map/expert/pallas_call | solution.py:484
  189.2 9.0 %expert.7 = (bf16[256,2048]{1,0:T(8,128)(2,1)S(1)}, bf16[256,2048]{1,0:T(8,128)(2,1)S(1)}) custom-call(bf16[64,2048]{1,0:T(8,128)(2,1)S(1)} %collective-permute-done.43.refs_0_, bf16[64,2048]{1,0:T(8,128)(2,1)S(1)} %collective-permute-done.44.refs_1_, bf16[64,2048]{1,0:T(8,128)(2,1)S(1)} %collective-permute-done.47.refs_2_, ...), custom_call_target="tpu_custom_call" | custom-call | flops 5637144576 | bytes 15204352 | tf_op jit(solution)/shard_map/expert/pallas_call | solution.py:484
  202.4 10.9 %collective-permute-done.21 = bf16[2,64,2048]{2,1,0:T(8,128)(2,1)S(1)} collective-permute-done((bf16[2,64,2048]{2,1,0:T(8,128)(2,1)S(1)}, bf16[2,64,2048]{2,1,0:T(8,128)(2,1)S(1)}, u32[]{:S(2)}, u32[]{:S(2)}) %collective-permute-start.21) | collective-permute-done | bytes 524320 | tf_op jit(solution)/shard_map/ppermute | solution.py:201
  215.4 9.1 %collective-permute-done.28 = bf16[2,64,2048]{2,1,0:T(8,128)(2,1)S(1)} collective-permute-done((bf16[2,64,2048]{2,1,0:T(8,128)(2,1)S(1)}, bf16[2,64,2048]{2,1,0:T(8,128)(2,1)S(1)}, u32[]{:S(2)}, u32[]{:S(2)}) %collective-permute-start.28) | collective-permute-done | bytes 524320 | tf_op jit(solution)/shard_map/ppermute | solution.py:201
  224.9 2.9 %collective-permute-start.29 = (bf16[64,2048]{1,0:T(8,128)(2,1)S(1)}, bf16[64,2048]{1,0:T(8,128)(2,1)S(1)}, u32[]{:S(2)}, u32[]{:S(2)}) collective-permute-start(bf16[64,2048]{1,0:T(8,128)(2,1)S(1)} %get-tuple-element.46), channel_id=1, source_target_pairs={{0,24},{4,28},{8,0},{12,4},{16,8},{20,12},{24,16},{28,20},{1,25},{... | collective-permute-start | bytes 786440 | tf_op jit(solution)/shard_map/ppermute | solution.py:228
  227.7 8.1 %collective-permute-done.41 = bf16[2,64,2048]{2,1,0:T(8,128)(2,1)S(1)} collective-permute-done((bf16[2,64,2048]{2,1,0:T(8,128)(2,1)S(1)}, bf16[2,64,2048]{2,1,0:T(8,128)(2,1)S(1)}, u32[]{:S(2)}, u32[]{:S(2)}) %collective-permute-start.41) | collective-permute-done | bytes 524320 | tf_op jit(solution)/shard_map/ppermute | solution.py:201
  239.1 7.4 %collective-permute-done.54 = bf16[2,64,2048]{2,1,0:T(8,128)(2,1)S(1)} collective-permute-done((bf16[2,64,2048]{2,1,0:T(8,128)(2,1)S(1)}, bf16[2,64,2048]{2,1,0:T(8,128)(2,1)S(1)}, u32[]{:S(2)}, u32[]{:S(2)}) %collective-permute-start.54) | collective-permute-done | bytes 524320 | tf_op jit(solution)/shard_map/ppermute | solution.py:201
  252.2 6.2 %collective-permute-done.58.refs_11_ = bf16[64,2048]{1,0:T(8,128)(2,1)S(1)} collective-permute-done((bf16[64,2048]{1,0:T(8,128)(2,1)S(1)}, bf16[64,2048]{1,0:T(8,128)(2,1)S(1)}, u32[]{:S(2)}, u32[]{:S(2)}) %collective-permute-start.58) | collective-permute-done | bytes 262176 | tf_op jit(solution)/shard_map/ppermute | solution.py:228
  258.5 14.8 %collective-permute-done.55.refs_8_ = bf16[64,2048]{1,0:T(8,128)(2,1)S(1)} collective-permute-done((bf16[64,2048]{1,0:T(8,128)(2,1)}, bf16[64,2048]{1,0:T(8,128)(2,1)S(1)}, u32[]{:S(2)}, u32[]{:S(2)}) %collective-permute-start.55) | collective-permute-done | bytes 262176 | tf_op jit(solution)/shard_map/ppermute | solution.py:228
  273.3 6.1 %collective-permute-done.56.refs_9_ = bf16[64,2048]{1,0:T(8,128)(2,1)S(1)} collective-permute-done((bf16[64,2048]{1,0:T(8,128)(2,1)}, bf16[64,2048]{1,0:T(8,128)(2,1)S(1)}, u32[]{:S(2)}, u32[]{:S(2)}) %collective-permute-start.56) | collective-permute-done | bytes 262176 | tf_op jit(solution)/shard_map/ppermute | solution.py:228
  (146 shorter events, 56.7 us)
Async XLA Ops:
  7.5 14.9 %collective-permute-start.3 = (bf16[512,256]{1,0:T(8,128)(2,1)}, bf16[512,256]{1,0:T(8,128)(2,1)S(1)}, u32[]{:S(2)}, u32[]{:S(2)}) collective-permute-start(bf16[512,256]{1,0:T(8,128)(2,1)} %refs_6_.2), channel_id=1, source_target_pairs={{0,8},{4,12},{8,16},{12,20},{16,24},{20,28},{1,9},{5,13},{9,17},{1... | collective-permute-start | bytes 786440 | tf_op jit(solution)/shard_map/ppermute | solution.py:159
  28.7 20.4 %collective-permute-start.4 = (bf16[544,256]{1,0:T(8,128)(2,1)S(1)}, bf16[544,256]{1,0:T(8,128)(2,1)S(1)}, u32[]{:S(2)}, u32[]{:S(2)}) collective-permute-start(bf16[544,256]{1,0:T(8,128)(2,1)S(1)} %collective-permute-done.2.refs_9_), channel_id=1, source_target_pairs={{0,4},{8,12},{16,20},{24,28},{4,0},{12,8},{20,16},{28,24},{1,5},{9... | collective-permute-start | bytes 835592 | tf_op jit(solution)/shard_map/ppermute | solution.py:160
  28.8 23.1 %collective-permute-start.8 = (bf16[544,256]{1,0:T(8,128)(2,1)S(1)}, bf16[544,256]{1,0:T(8,128)(2,1)S(1)}, u32[]{:S(2)}, u32[]{:S(2)}) collective-permute-start(bf16[544,256]{1,0:T(8,128)(2,1)S(1)} %collective-permute-done.6.refs_13_), channel_id=1, source_target_pairs={{4,0},{12,8},{20,16},{28,24},{5,1},{13,9},{21,17},{29,25},{6,2},{1... | collective-permute-start | bytes 835592 | tf_op jit(solution)/shard_map/ppermute | solution.py:160
  30.1 19.0 %collective-permute-start.5 = (bf16[512,256]{1,0:T(8,128)(2,1)S(1)}, bf16[512,256]{1,0:T(8,128)(2,1)}, u32[]{:S(2)}, u32[]{:S(2)}) collective-permute-start(bf16[512,256]{1,0:T(8,128)(2,1)S(1)} %collective-permute-done.3.refs_10_), channel_id=1, source_target_pairs={{0,4},{8,12},{16,20},{24,28},{4,0},{12,8},{20,16},{28,24},{1,5},{9... | collective-permute-start | bytes 786440 | tf_op jit(solution)/shard_map/ppermute | solution.py:160
  32.8 19.1 %collective-permute-start.9 = (bf16[512,256]{1,0:T(8,128)(2,1)}, bf16[512,256]{1,0:T(8,128)(2,1)}, u32[]{:S(2)}, u32[]{:S(2)}) collective-permute-start(bf16[512,256]{1,0:T(8,128)(2,1)} %collective-permute-done.7.refs_14_), channel_id=1, source_target_pairs={{4,0},{12,8},{20,16},{28,24},{5,1},{13,9},{21,17},{29,25},{6,2},{1... | collective-permute-start | bytes 786440 | tf_op jit(solution)/shard_map/ppermute | solution.py:160
  35.7 37.5 %collective-permute-start.13 = (bf16[128,2048]{1,0:T(8,128)(2,1)}, bf16[128,2048]{1,0:T(8,128)(2,1)S(1)}, u32[]{:S(2)}, u32[]{:S(2)}) collective-permute-start(bf16[128,2048]{1,0:T(8,128)(2,1)} %refs_6_.3), channel_id=1, source_target_pairs={{0,2},{1,3},{2,0},{3,1},{4,6},{5,7},{6,4},{7,5},{8,10},{9,11},{10,... | collective-permute-start | bytes 1572872 | tf_op jit(solution)/shard_map/ppermute | solution.py:201
  78.4 19.0 %collective-permute-start.15 = (bf16[64,2048]{1,0:T(8,128)(2,1)S(1)}, bf16[64,2048]{1,0:T(8,128)(2,1)S(1)}, u32[]{:S(2)}, u32[]{:S(2)}) collective-permute-start(bf16[64,2048]{1,0:T(8,128)(2,1)S(1)} %get-tuple-element.28), channel_id=1, source_target_pairs={{0,4},{4,0},{8,12},{12,8},{16,20},{20,16},{24,28},{28,24},{1,5},{5... | collective-permute-start | bytes 786440 | tf_op jit(solution)/shard_map/ppermute | solution.py:228
  83.6 20.4 %collective-permute-start.33 = (bf16[64,2048]{1,0:T(8,128)(2,1)S(1)}, bf16[64,2048]{1,0:T(8,128)(2,1)S(1)}, u32[]{:S(2)}, u32[]{:S(2)}) collective-permute-start(bf16[64,2048]{1,0:T(8,128)(2,1)S(1)} %get-tuple-element.36), channel_id=1, source_target_pairs={{0,4},{4,0},{8,12},{12,8},{16,20},{20,16},{24,28},{28,24},{1,5},{5... | collective-permute-start | bytes 786440 | tf_op jit(solution)/shard_map/ppermute | solution.py:228
  85.5 42.1 %collective-permute-start.17 = (bf16[128,2048]{1,0:T(8,128)(2,1)S(1)}, bf16[128,2048]{1,0:T(8,128)(2,1)S(1)}, u32[]{:S(2)}, u32[]{:S(2)}) collective-permute-start(bf16[128,2048]{1,0:T(8,128)(2,1)S(1)} %get-tuple-element.27.refs_0_), channel_id=1, source_target_pairs={{0,1},{1,0},{2,3},{3,2},{4,5},{5,4},{6,7},{7,6},{8,9},{9,8},{10,11... | collective-permute-start | bytes 1572872 | tf_op jit(solution)/shard_map/ppermute | solution.py:201
  85.5 48.0 %collective-permute-start.23 = (bf16[128,2048]{1,0:T(8,128)(2,1)S(1)}, bf16[128,2048]{1,0:T(8,128)(2,1)S(1)}, u32[]{:S(2)}, u32[]{:S(2)}) collective-permute-start(bf16[128,2048]{1,0:T(8,128)(2,1)S(1)} %get-tuple-element.31), channel_id=1, source_target_pairs={{0,8},{4,12},{8,16},{12,20},{16,24},{20,28},{24,0},{28,4},{1,9},{5... | collective-permute-start | bytes 1572872 | tf_op jit(solution)/shard_map/ppermute | solution.py:228
  97.4 39.1 %collective-permute-start.24 = (bf16[128,2048]{1,0:T(8,128)(2,1)S(1)}, bf16[128,2048]{1,0:T(8,128)(2,1)S(1)}, u32[]{:S(2)}, u32[]{:S(2)}) collective-permute-start(bf16[128,2048]{1,0:T(8,128)(2,1)S(1)} %get-tuple-element.32), channel_id=1, source_target_pairs={{0,24},{4,28},{8,0},{12,4},{16,8},{20,12},{24,16},{28,20},{1,25},{... | collective-permute-start | bytes 1572872 | tf_op jit(solution)/shard_map/ppermute | solution.py:228
  97.4 28.7 %collective-permute-start.43 = (bf16[64,2048]{1,0:T(8,128)(2,1)S(1)}, bf16[64,2048]{1,0:T(8,128)(2,1)S(1)}, u32[]{:S(2)}, u32[]{:S(2)}) collective-permute-start(bf16[64,2048]{1,0:T(8,128)(2,1)S(1)} %get-tuple-element.39), channel_id=1, source_target_pairs={{0,16},{4,20},{8,24},{12,28},{16,0},{20,4},{24,8},{28,12},{1,17},{... | collective-permute-start | bytes 786440 | tf_op jit(solution)/shard_map/ppermute | solution.py:228
  104.0 23.7 %collective-permute-start.45 = (bf16[64,2048]{1,0:T(8,128)(2,1)S(1)}, bf16[64,2048]{1,0:T(8,128)(2,1)S(1)}, u32[]{:S(2)}, u32[]{:S(2)}) collective-permute-start(bf16[64,2048]{1,0:T(8,128)(2,1)S(1)} %get-tuple-element.40), channel_id=1, source_target_pairs={{0,4},{4,0},{8,12},{12,8},{16,20},{20,16},{24,28},{28,24},{1,5},{5... | collective-permute-start | bytes 786440 | tf_op jit(solution)/shard_map/ppermute | solution.py:228
  127.6 16.3 %collective-permute-start.18 = (bf16[64,2048]{1,0:T(8,128)(2,1)S(1)}, bf16[64,2048]{1,0:T(8,128)(2,1)S(1)}, u32[]{:S(2)}, u32[]{:S(2)}) collective-permute-start(bf16[64,2048]{1,0:T(8,128)(2,1)S(1)} %collective-permute-done.15.refs_1_), channel_id=1, source_target_pairs={{0,1},{1,0},{2,3},{3,2},{4,5},{5,4},{6,7},{7,6},{8,9},{9,8},{10,11... | collective-permute-start | bytes 786440 | tf_op jit(solution)/shard_map/ppermute | solution.py:201
  127.6 16.3 %collective-permute-start.31 = (bf16[64,2048]{1,0:T(8,128)(2,1)S(1)}, bf16[64,2048]{1,0:T(8,128)(2,1)S(1)}, u32[]{:S(2)}, u32[]{:S(2)}) collective-permute-start(bf16[64,2048]{1,0:T(8,128)(2,1)S(1)} %collective-permute-done.30), channel_id=1, source_target_pairs={{0,8},{4,12},{8,16},{12,20},{16,24},{20,28},{24,0},{28,4},{1,9},{5... | collective-permute-start | bytes 786440 | tf_op jit(solution)/shard_map/ppermute | solution.py:228
  133.6 14.8 %collective-permute-start.34 = (bf16[64,2048]{1,0:T(8,128)(2,1)S(1)}, bf16[64,2048]{1,0:T(8,128)(2,1)S(1)}, u32[]{:S(2)}, u32[]{:S(2)}) collective-permute-start(bf16[64,2048]{1,0:T(8,128)(2,1)S(1)} %collective-permute-done.33), channel_id=1, source_target_pairs={{0,24},{4,28},{8,0},{12,4},{16,8},{20,12},{24,16},{28,20},{1,25},{... | collective-permute-start | bytes 786440 | tf_op jit(solution)/shard_map/ppermute | solution.py:228
  137.0 16.2 %collective-permute-start.46 = (bf16[64,2048]{1,0:T(8,128)(2,1)S(1)}, bf16[64,2048]{1,0:T(8,128)(2,1)S(1)}, u32[]{:S(2)}, u32[]{:S(2)}) collective-permute-start(bf16[64,2048]{1,0:T(8,128)(2,1)S(1)} %collective-permute-done.45), channel_id=1, source_target_pairs={{0,24},{4,28},{8,0},{12,4},{16,8},{20,12},{24,16},{28,20},{1,25},{... | collective-permute-start | bytes 786440 | tf_op jit(solution)/shard_map/ppermute | solution.py:228
  148.4 20.2 %collective-permute-start.25 = (bf16[128,2048]{1,0:T(8,128)(2,1)S(1)}, bf16[128,2048]{1,0:T(8,128)(2,1)S(1)}, u32[]{:S(2)}, u32[]{:S(2)}) collective-permute-start(bf16[128,2048]{1,0:T(8,128)(2,1)S(1)} %collective-permute-done.23.refs_0_), channel_id=1, source_target_pairs={{0,1},{1,0},{2,3},{3,2},{4,5},{5,4},{6,7},{7,6},{8,9},{9,8},{10,11... | collective-permute-start | bytes 1572872 | tf_op jit(solution)/shard_map/ppermute | solution.py:201
  148.4 20.6 %collective-permute-start.26 = (bf16[128,2048]{1,0:T(8,128)(2,1)S(1)}, bf16[128,2048]{1,0:T(8,128)(2,1)S(1)}, u32[]{:S(2)}, u32[]{:S(2)}) collective-permute-start(bf16[128,2048]{1,0:T(8,128)(2,1)S(1)} %collective-permute-done.24.refs_1_), channel_id=1, source_target_pairs={{0,1},{1,0},{2,3},{3,2},{4,5},{5,4},{6,7},{7,6},{8,9},{9,8},{10,11... | collective-permute-start | bytes 1572872 | tf_op jit(solution)/shard_map/ppermute | solution.py:201
  153.2 14.7 %collective-permute-start.32 = (bf16[64,2048]{1,0:T(8,128)(2,1)S(1)}, bf16[64,2048]{1,0:T(8,128)(2,1)S(1)}, u32[]{:S(2)}, u32[]{:S(2)}) collective-permute-start(bf16[64,2048]{1,0:T(8,128)(2,1)S(1)} %collective-permute-done.31.refs_0_), channel_id=1, source_target_pairs={{0,2},{1,3},{2,0},{3,1},{4,6},{5,7},{6,4},{7,5},{8,10},{9,11},{10,... | collective-permute-start | bytes 786440 | tf_op jit(solution)/shard_map/ppermute | solution.py:201
  178.6 19.7 %collective-permute-start.20 = (bf16[256,2048]{1,0:T(8,128)(2,1)S(1)}, bf16[256,2048]{1,0:T(8,128)(2,1)S(1)}, u32[]{:S(2)}, u32[]{:S(2)}) collective-permute-start(bf16[256,2048]{1,0:T(8,128)(2,1)S(1)} %get-tuple-element.30), channel_id=1, source_target_pairs={{0,1},{1,0},{2,3},{3,2},{4,5},{5,4},{6,7},{7,6},{8,9},{9,8},{10,11... | collective-permute-start | bytes 3145736 | tf_op jit(solution)/shard_map/ppermute | solution.py:201
  179.2 20.8 %collective-permute-start.27 = (bf16[256,2048]{1,0:T(8,128)(2,1)S(1)}, bf16[256,2048]{1,0:T(8,128)(2,1)S(1)}, u32[]{:S(2)}, u32[]{:S(2)}) collective-permute-start(bf16[256,2048]{1,0:T(8,128)(2,1)S(1)} %get-tuple-element.34), channel_id=1, source_target_pairs={{0,1},{1,0},{2,3},{3,2},{4,5},{5,4},{6,7},{7,6},{8,9},{9,8},{10,11... | collective-permute-start | bytes 3145736 | tf_op jit(solution)/shard_map/ppermute | solution.py:201
  198.2 15.6 %collective-permute-start.53 = (bf16[256,2048]{1,0:T(8,128)(2,1)S(1)}, bf16[256,2048]{1,0:T(8,128)(2,1)S(1)}, u32[]{:S(2)}, u32[]{:S(2)}) collective-permute-start(bf16[256,2048]{1,0:T(8,128)(2,1)S(1)} %get-tuple-element.42), channel_id=1, source_target_pairs={{0,1},{1,0},{2,3},{3,2},{4,5},{5,4},{6,7},{7,6},{8,9},{9,8},{10,11... | collective-permute-start | bytes 3145736 | tf_op jit(solution)/shard_map/ppermute | solution.py:201
  198.5 14.9 %collective-permute-start.21 = (bf16[2,64,2048]{2,1,0:T(8,128)(2,1)S(1)}, bf16[2,64,2048]{2,1,0:T(8,128)(2,1)S(1)}, u32[]{:S(2)}, u32[]{:S(2)}) collective-permute-start(bf16[2,64,2048]{2,1,0:T(8,128)(2,1)S(1)} %fusion.4), channel_id=1, source_target_pairs={{0,2},{1,3},{2,0},{3,1},{4,6},{5,7},{6,4},{7,5},{8,10},{9,11},{10,... | collective-permute-start | bytes 1572872 | tf_op jit(solution)/shard_map/ppermute | solution.py:201
  200.1 24.4 %collective-permute-start.28 = (bf16[2,64,2048]{2,1,0:T(8,128)(2,1)S(1)}, bf16[2,64,2048]{2,1,0:T(8,128)(2,1)S(1)}, u32[]{:S(2)}, u32[]{:S(2)}) collective-permute-start(bf16[2,64,2048]{2,1,0:T(8,128)(2,1)S(1)} %fusion.5), channel_id=1, source_target_pairs={{0,2},{1,3},{2,0},{3,1},{4,6},{5,7},{6,4},{7,5},{8,10},{9,11},{10,... | collective-permute-start | bytes 1572872 | tf_op jit(solution)/shard_map/ppermute | solution.py:201
  200.9 34.9 %collective-permute-start.41 = (bf16[2,64,2048]{2,1,0:T(8,128)(2,1)S(1)}, bf16[2,64,2048]{2,1,0:T(8,128)(2,1)S(1)}, u32[]{:S(2)}, u32[]{:S(2)}) collective-permute-start(bf16[2,64,2048]{2,1,0:T(8,128)(2,1)S(1)} %fusion.6), channel_id=1, source_target_pairs={{0,2},{1,3},{2,0},{3,1},{4,6},{5,7},{6,4},{7,5},{8,10},{9,11},{10,... | collective-permute-start | bytes 1572872 | tf_op jit(solution)/shard_map/ppermute | solution.py:201
  213.6 34.1 %collective-permute-start.22 = (bf16[64,2048]{1,0:T(8,128)(2,1)S(1)}, bf16[64,2048]{1,0:T(8,128)(2,1)S(1)}, u32[]{:S(2)}, u32[]{:S(2)}) collective-permute-start(bf16[64,2048]{1,0:T(8,128)(2,1)S(1)} %get-tuple-element.49), channel_id=1, source_target_pairs={{0,4},{4,0},{8,12},{12,8},{16,20},{20,16},{24,28},{28,24},{1,5},{5... | collective-permute-start | bytes 786440 | tf_op jit(solution)/shard_map/ppermute | solution.py:228
  213.9 32.6 %collective-permute-start.54 = (bf16[2,64,2048]{2,1,0:T(8,128)(2,1)S(1)}, bf16[2,64,2048]{2,1,0:T(8,128)(2,1)S(1)}, u32[]{:S(2)}, u32[]{:S(2)}) collective-permute-start(bf16[2,64,2048]{2,1,0:T(8,128)(2,1)S(1)} %fusion.7), channel_id=1, source_target_pairs={{0,2},{1,3},{2,0},{3,1},{4,6},{5,7},{6,4},{7,5},{8,10},{9,11},{10,... | collective-permute-start | bytes 1572872 | tf_op jit(solution)/shard_map/ppermute | solution.py:201
  224.9 25.5 %collective-permute-start.29 = (bf16[64,2048]{1,0:T(8,128)(2,1)S(1)}, bf16[64,2048]{1,0:T(8,128)(2,1)S(1)}, u32[]{:S(2)}, u32[]{:S(2)}) collective-permute-start(bf16[64,2048]{1,0:T(8,128)(2,1)S(1)} %get-tuple-element.46), channel_id=1, source_target_pairs={{0,24},{4,28},{8,0},{12,4},{16,8},{20,12},{24,16},{28,20},{1,25},{... | collective-permute-start | bytes 786440 | tf_op jit(solution)/shard_map/ppermute | solution.py:228
  236.8 15.5 %collective-permute-start.42 = (bf16[64,2048]{1,0:T(8,128)(2,1)}, bf16[64,2048]{1,0:T(8,128)(2,1)S(1)}, u32[]{:S(2)}, u32[]{:S(2)}) collective-permute-start(bf16[64,2048]{1,0:T(8,128)(2,1)} %get-tuple-element.44), channel_id=1, source_target_pairs={{0,28},{4,24},{8,4},{12,0},{16,12},{20,8},{24,20},{28,16},{1,29},{... | collective-permute-start | bytes 786440 | tf_op jit(solution)/shard_map/ppermute | solution.py:228
  247.7 25.6 %collective-permute-start.55 = (bf16[64,2048]{1,0:T(8,128)(2,1)}, bf16[64,2048]{1,0:T(8,128)(2,1)S(1)}, u32[]{:S(2)}, u32[]{:S(2)}) collective-permute-start(bf16[64,2048]{1,0:T(8,128)(2,1)} %get-tuple-element.48), channel_id=1, source_target_pairs={{0,16},{4,20},{8,24},{12,28},{16,0},{20,4},{24,8},{28,12},{1,17},{... | collective-permute-start | bytes 786440 | tf_op jit(solution)/shard_map/ppermute | solution.py:228
  250.4 29.0 %collective-permute-start.56 = (bf16[64,2048]{1,0:T(8,128)(2,1)}, bf16[64,2048]{1,0:T(8,128)(2,1)S(1)}, u32[]{:S(2)}, u32[]{:S(2)}) collective-permute-start(bf16[64,2048]{1,0:T(8,128)(2,1)} %get-tuple-element.47), channel_id=1, source_target_pairs={{0,20},{4,16},{8,28},{12,24},{16,4},{20,0},{24,12},{28,8},{1,21},{... | collective-permute-start | bytes 786440 | tf_op jit(solution)/shard_map/ppermute | solution.py:228
  (38 other events, 726.4 us)

commit v2 on v1

--- a/solution.py
+++ b/solution.py
@@ -18,7 +18,7 @@
     return [part.astype(jnp.bfloat16) for part in (hi, mid, low)]
 
 
-def attention_kernel(tokens, heads, head_size, tile, sources, *refs):
+def attention_kernel(tokens, heads, head_size, tile, n_tp, sources, *refs):
     valid_ref, docs_ref, q_ref, meta_ref, gain_ref = refs[:5]
     kv_refs = refs[5 : 5 + 2 * sources]
     mine_ref, other_ref = refs[5 + 2 * sources : 7 + 2 * sources]
@@ -109,15 +109,19 @@
         ]
         scale = spread([lax.rsqrt(mean + EPS) for mean in means])
         normed = (attended * scale * gain_ref[...]).astype(jnp.bfloat16)
-        here = pl.ds(pl.multiple_of((step // 2) * tile, tile), tile)
-
-        @pl.when(step % 2 == valid_ref[sources])
-        def _():
-            mine_ref[here, :] = normed
-
-        @pl.when(step % 2 != valid_ref[sources])
-        def _():
-            other_ref[here, :] = normed
+        piece = docs_ref.shape[0] // n_tp
+        for part in range(tile // piece):
+            index = step * (tile // piece) + part
+            here = pl.ds(pl.multiple_of((index // 2) * piece, piece), piece)
+            value = normed[part * piece : (part + 1) * piece]
+
+            @pl.when(index % 2 == valid_ref[sources])
+            def _():
+                mine_ref[here, :] = value
+
+            @pl.when(index % 2 != valid_ref[sources])
+            def _():
+                other_ref[here, :] = value
 
         return carry
 
@@ -130,7 +134,7 @@
     head_size = width // heads
     n_sp = lax.axis_size("sp")
     place = lax.axis_index("sp")
-    tile = tokens // lax.axis_size("tp")
+    tile = tokens // 2
 
     gate_rows = [part.T.reshape(-1, width) for part in bf16_parts(cum_gate)]
     doc_rows = documents.astype(jnp.bfloat16).reshape(-1, width)
@@ -178,7 +182,7 @@
     valid = jnp.stack(valid + [lax.axis_index("tp") % 2 == 1]).astype(jnp.int32)
 
     def kernel(*refs):
-        attention_kernel(tokens, heads, head_size, tile, sources, *refs)
+        attention_kernel(tokens, heads, head_size, tile, lax.axis_size("tp"), sources, *refs)
 
     vmem = pl.BlockSpec(memory_space=pltpu.VMEM)
     smem = pl.BlockSpec(memory_space=pltpu.SMEM)
@@ -214,8 +218,7 @@
     inner = n_sp // 4
     low, high = range(inner // 2), range(inner // 2, inner)
     return [
-        [(0, bits) for bits in range(inner)],
-        [(step, bits) for bits in low for step in (1, 3)],
+        [(0, bits) for bits in range(inner)] + [(step, bits) for bits in low for step in (1, 3)],
         [(step, bits) for bits in high for step in (1, 3)],
         [(2, bits) for bits in range(inner)],
     ]
@@ -317,7 +320,7 @@
             outs[k][:, cols] = picked[spans[k] : spans[k + 1]]
 
 
-def expert_kernel(count, *refs):
+def expert_kernel(count, moves, *refs):
     inputs = refs[:count]
     gate_ref, up_ref, down_hbm = refs[count : count + 3]
     mine_ref, other_ref, x_ref, hidden_ref, down_ref, sem = refs[count + 3 :]
@@ -349,8 +352,10 @@
             out = jnp.dot(
                 hidden, down_ref[:, cols], preferred_element_type=jnp.float32
             ).astype(jnp.bfloat16)
-            mine_ref[:, cols] = out[:mine_rows]
-            other_ref[:, cols] = out[mine_rows:]
+            for source, target, span in moves:
+                mine_ref[target : target + span, cols] = out[source : source + span]
+                source += mine_rows
+                other_ref[target : target + span, cols] = out[source : source + span]
 
 
 def combine_kernel(experts, place_ref, stream_ref, routes_ref, weights_ref, *refs):
@@ -464,22 +469,35 @@
         return move(x, (step, 0))
 
     groups = expert_groups(n_sp)
-    members = len(groups[0])
     hidden_width = w_gate.shape[2]
     h_tile = 128
-    rows = 2 * members * each
     arrived = {way: dispatch(way) for way in ways(n_sp)}
     returned = {}
     for group in groups:
-        inputs = []
-        for way in group:
-            inputs.append(arrived[way])
-            if not both_blocks(way):
-                inputs += [swap(arrived[way], "tp", 2 * j) for j in range(1, blocks)]
+        members = len(group)
+        rows = 2 * members * each
+        single = [way for way in group if not both_blocks(way)]
+        both = [way for way in group if both_blocks(way)]
+        inputs = [arrived[way] for way in both]
+        moves = [
+            (i * each + j * capacity, (j * members + i) * capacity, capacity)
+            for i in range(len(both))
+            for j in range(blocks)
+        ]
+        cut, count = len(both) * each, len(single) * capacity
+        moves += [
+            (cut + j * count, (j * members + len(both)) * capacity, count) for j in range(blocks)
+        ]
+        if len(single) > 1:
+            joined = jnp.concatenate([arrived[way] for way in single], axis=0)
+        else:
+            joined = arrived[single[0]]
+        crossed = [swap(joined, "tp", 2 * j) for j in range(1, blocks)]
+        inputs += [joined, *crossed]
         inputs += [swap(x, "tp", 1) for x in inputs]
 
         def expert(*refs):
-            expert_kernel(len(inputs), *refs)
+            expert_kernel(len(inputs), moves, *refs)
 
         part_mine, part_other = pl.pallas_call(
             expert,
@@ -506,18 +524,18 @@
             name="expert",
         )(*inputs, w_gate[0], w_up[0], w_down[0])
         added = swap(part_other, "tp", 1)
-        shape = (members, blocks, capacity, model_width)
-        part_mine, added = part_mine.reshape(shape), added.reshape(shape)
+        span = members * capacity
 
         def summed(j):
-            return part_mine[:, j].astype(jnp.float32) + added[:, j].astype(jnp.float32)
+            here = slice(j * span, (j + 1) * span)
+            return part_mine[here].astype(jnp.float32) + added[here].astype(jnp.float32)
 
         result = summed(0)
         for j in range(1, blocks):
             sent = swap(summed(j).astype(jnp.bfloat16), "tp", 2 * j)
             result = result + sent.astype(jnp.float32)
-        result = result.astype(jnp.bfloat16)
-        for i, way in enumerate(group):
+        result = result.astype(jnp.bfloat16).reshape(members, capacity, model_width)
+        for i, way in enumerate(both + single):
             back = (-way[0] % 4, way[1])
             returned[way] = result[i] if way == (0, 0) else move(result[i], back)
 

time: 282 us -> 252 us (0.89)
  starting transfers between devices: 104 us -> 83 us
  Pallas kernels: 50.6 us -> 45.6 us
  waiting for transfers between devices: 115 us -> 110 us
    ppermute x18, starting transfers between devices: 56.8 us -> 38.6 us  [move(): lax.ppermute(x, 'sp', [(i, (i // inner + step) % 4 * inner + (i % inner ^...]
    ppermute x18, waiting for transfers between devices: 55.5 us -> 48.1 us  [move(): lax.ppermute(x, 'sp', [(i, (i // inner + step) % 4 * inner + (i % inner ^...]
    ppermute x31 -> x23, waiting for transfers between devices: 40.5 us -> 43.7 us  [swap(): lax.ppermute(x, axis, [(i, i ^ bits) for i in range(lax.axis_size(axis))])]
    ppermute x31 -> x23, starting transfers between devices: 18.9 us -> 16.5 us  [swap(): lax.ppermute(x, axis, [(i, i ^ bits) for i in range(lax.axis_size(axis))])]
    pallas_call x4 -> x3, Pallas kernels: 35.9 us -> 33.5 us  [on_device(): pl.pallas_call(expert, grid=(hidden_width // h_tile,), out_shape=[jax.Sha...]
    unnamed x24 -> x26, local copies, waits for them, and re-layouts: 5.69 us -> 5.74 us
  transfers between devices with their start and end apart: 59 -> 51, of which waited for: 15 -> 19; matrix products, arithmetic and copies ran while one was open for 2% -> 2% of each run, Pallas kernels for 16% -> 16%
where the time goes in v2:
time: 252 us
  waiting for transfers between devices  110 us (44%)
  starting transfers between devices  83 us (33%)
  Pallas kernels  45.6 us (18%)
  local copies, waits for them, and re-layouts  8.12 us (3%)
  other arithmetic  4 us (2%)
    ppermute x18, waiting for transfers between devices, move(): lax.ppermute(x, 'sp', [(i, (i // inner + step) % 4 * inner + (i % inner ^...  48.1 us
    ppermute x23, waiting for transfers between devices, swap(): lax.ppermute(x, axis, [(i, i ^ bits) for i in range(lax.axis_size(axis))])  43.7 us
    ppermute x18, starting transfers between devices, move(): lax.ppermute(x, 'sp', [(i, (i // inner + step) % 4 * inner + (i % inner ^...  38.6 us
    pallas_call x3, Pallas kernels, on_device(): pl.pallas_call(expert, grid=(hidden_width // h_tile,), out_shape=[jax.Sha...  33.5 us
    ppermute x4, starting transfers between devices, chain(): own.append(lax.ppermute(own[-1], 'sp', ahead))  17 us
    ppermute x23, starting transfers between devices, swap(): lax.ppermute(x, axis, [(i, i ^ bits) for i in range(lax.axis_size(axis))])  16.5 us
    ppermute x6, waiting for transfers between devices, chain(): other.append(lax.ppermute(own[-1], 'sp', pairs))  15.2 us
    ppermute x6, starting transfers between devices, chain(): other.append(lax.ppermute(own[-1], 'sp', pairs))  10.9 us
  transfers between devices with their start and end apart: 51, of which 19 were waited for; matrix products, arithmetic and copies ran while one was open for 2% of the time, Pallas kernels for 16%

profile of v2, /device:TPU:0, one launch (start us, length us, event | category | flops | bytes accessed | tf_op | source)
XLA Modules:
  0.0 251.6 jit_solution(1591115582818060691)
XLA Ops:
  2.5 5.0 %collective-permute-start.2 = (bf16[544,256]{1,0:T(8,128)(2,1)S(1)}, bf16[544,256]{1,0:T(8,128)(2,1)S(1)}, u32[]{:S(2)}, u32[]{:S(2)}) collective-permute-start(bf16[544,256]{1,0:T(8,128)(2,1)S(1)} %concatenate.16.refs_5_), channel_id=1, source_target_pairs={{0,8},{4,12},{8,16},{12,20},{16,24},{20,28},{1,9},{5,13},{9,17},{1... | collective-permute-start | bytes 835592 | tf_op jit(solution)/shard_map/ppermute | solution.py:163
  7.5 3.5 %collective-permute-start.3 = (bf16[512,256]{1,0:T(8,128)(2,1)}, bf16[512,256]{1,0:T(8,128)(2,1)S(1)}, u32[]{:S(2)}, u32[]{:S(2)}) collective-permute-start(bf16[512,256]{1,0:T(8,128)(2,1)} %refs_6_.2), channel_id=1, source_target_pairs={{0,8},{4,12},{8,16},{12,20},{16,24},{20,28},{1,9},{5,13},{9,17},{1... | collective-permute-start | bytes 786440 | tf_op jit(solution)/shard_map/ppermute | solution.py:163
  11.0 3.5 %collective-permute-done.2.refs_9_ = bf16[544,256]{1,0:T(8,128)(2,1)S(1)} collective-permute-done((bf16[544,256]{1,0:T(8,128)(2,1)S(1)}, bf16[544,256]{1,0:T(8,128)(2,1)S(1)}, u32[]{:S(2)}, u32[]{:S(2)}) %collective-permute-start.2) | collective-permute-done | bytes 278560 | tf_op jit(solution)/shard_map/ppermute | solution.py:163
  14.5 4.4 %collective-permute-start.6 = (bf16[544,256]{1,0:T(8,128)(2,1)S(1)}, bf16[544,256]{1,0:T(8,128)(2,1)S(1)}, u32[]{:S(2)}, u32[]{:S(2)}) collective-permute-start(bf16[544,256]{1,0:T(8,128)(2,1)S(1)} %collective-permute-done.2.refs_9_), channel_id=1, source_target_pairs={{0,8},{4,12},{8,16},{12,20},{16,24},{20,28},{1,9},{5,13},{9,17},{1... | collective-permute-start | bytes 835592 | tf_op jit(solution)/shard_map/ppermute | solution.py:163
  18.9 3.4 %collective-permute-start.1 = (bf16[512,256]{1,0:T(8,128)(2,1)}, bf16[512,256]{1,0:T(8,128)(2,1)S(1)}, u32[]{:S(2)}, u32[]{:S(2)}) collective-permute-start(bf16[512,256]{1,0:T(8,128)(2,1)} %refs_6_.2), channel_id=1, source_target_pairs={{0,4},{8,12},{16,20},{24,28},{1,5},{9,13},{17,21},{25,29},{2,6},{1... | collective-permute-start | bytes 786440 | tf_op jit(solution)/shard_map/ppermute | solution.py:164
  22.4 4.2 %collective-permute-start.7 = (bf16[512,256]{1,0:T(8,128)(2,1)S(1)}, bf16[512,256]{1,0:T(8,128)(2,1)}, u32[]{:S(2)}, u32[]{:S(2)}) collective-permute-start(bf16[512,256]{1,0:T(8,128)(2,1)S(1)} %collective-permute-done.3.refs_10_), channel_id=1, source_target_pairs={{0,8},{4,12},{8,16},{12,20},{16,24},{20,28},{1,9},{5,13},{9,17},{1... | collective-permute-start | bytes 786440 | tf_op jit(solution)/shard_map/ppermute | solution.py:163
  30.1 2.7 %collective-permute-start.5 = (bf16[512,256]{1,0:T(8,128)(2,1)S(1)}, bf16[512,256]{1,0:T(8,128)(2,1)}, u32[]{:S(2)}, u32[]{:S(2)}) collective-permute-start(bf16[512,256]{1,0:T(8,128)(2,1)S(1)} %collective-permute-done.3.refs_10_), channel_id=1, source_target_pairs={{0,4},{8,12},{16,20},{24,28},{4,0},{12,8},{20,16},{28,24},{1,5},{9... | collective-permute-start | bytes 786440 | tf_op jit(solution)/shard_map/ppermute | solution.py:164
  38.1 11.0 %collective-permute-done.5.refs_12_ = bf16[512,256]{1,0:T(8,128)(2,1)} collective-permute-done((bf16[512,256]{1,0:T(8,128)(2,1)S(1)}, bf16[512,256]{1,0:T(8,128)(2,1)}, u32[]{:S(2)}, u32[]{:S(2)}) %collective-permute-start.5) | collective-permute-done | bytes 262176 | tf_op jit(solution)/shard_map/ppermute | solution.py:164
  49.1 2.8 %collective-permute-done.9.refs_16_ = bf16[512,256]{1,0:T(8,128)(2,1)} collective-permute-done((bf16[512,256]{1,0:T(8,128)(2,1)}, bf16[512,256]{1,0:T(8,128)(2,1)}, u32[]{:S(2)}, u32[]{:S(2)}) %collective-permute-start.9) | collective-permute-done | bytes 262176 | tf_op jit(solution)/shard_map/ppermute | solution.py:164
  55.1 6.6 %attention.1 = (bf16[256,256]{1,0:T(8,128)(2,1)S(1)}, bf16[256,256]{1,0:T(8,128)(2,1)S(1)}) custom-call(s32[7]{0:T(128)S(1)} %convert_element_type.87.refs_0_, s32[512]{0:T(512)S(1)} %copy-done.5, bf16[512,256]{1,0:T(8,128)(2,1)S(1)} %copy-done.2, f32[512,8]{1,0:T(8,128)S(1)} %copy.22.refs_3_, f32[1,256]{1,0:T(1,128)S(1)} %bitcast.23, ...), custom_call_target="tpu_custom_call" | custom-call | tf_op jit(solution)/shard_map/attention/pallas_call | solution.py:189
  65.6 5.0 %collective-permute-done.14.refs_9_ = f32[8,128]{1,0:T(8,128)S(1)} collective-permute-done((f32[8,128]{1,0:T(8,128)S(1)}, f32[8,128]{1,0:T(8,128)S(1)}, u32[]{:S(2)}, u32[]{:S(2)}) %collective-permute-start.14) | collective-permute-done | bytes 4128 | tf_op jit(solution)/shard_map/ppermute | solution.py:205
  72.8 3.0 %project.1 = (bf16[128,2048]{1,0:T(8,128)(2,1)S(1)}, bf16[64,2048]{1,0:T(8,128)(2,1)S(1)}, bf16[128,2048]{1,0:T(8,128)(2,1)S(1)}, bf16[64,2048]{1,0:T(8,128)(2,1...) custom-call(s32[2]{0:T(128)S(1)} %pad_add_fusion.refs_0_, ...), custom_call_target="tpu_custom_call" | custom-call | tf_op jit(solution)/shard_map/project/pallas_call | solution.py:440
  81.8 3.6 %collective-permute-done.28 = bf16[64,2048]{1,0:T(8,128)(2,1)S(1)} collective-permute-done((bf16[64,2048]{1,0:T(8,128)(2,1)S(1)}, bf16[64,2048]{1,0:T(8,128)(2,1)S(1)}, u32[]{:S(2)}, u32[]{:S(2)}) %collective-permute-start.28) | collective-permute-done | bytes 262176 | tf_op jit(solution)/shard_map/ppermute | solution.py:231
  85.4 6.7 %collective-permute-start.29 = (bf16[64,2048]{1,0:T(8,128)(2,1)S(1)}, bf16[64,2048]{1,0:T(8,128)(2,1)S(1)}, u32[]{:S(2)}, u32[]{:S(2)}) collective-permute-start(bf16[64,2048]{1,0:T(8,128)(2,1)S(1)} %collective-permute-done.28), channel_id=1, source_target_pairs={{0,8},{4,12},{8,16},{12,20},{16,24},{20,28},{24,0},{28,4},{1,9},{5... | collective-permute-start | bytes 786440 | tf_op jit(solution)/shard_map/ppermute | solution.py:231
  92.2 5.6 %collective-permute-start.15 = (bf16[128,2048]{1,0:T(8,128)(2,1)S(1)}, bf16[128,2048]{1,0:T(8,128)(2,1)S(1)}, u32[]{:S(2)}, u32[]{:S(2)}) collective-permute-start(bf16[128,2048]{1,0:T(8,128)(2,1)S(1)} %get-tuple-element.26), channel_id=1, source_target_pairs={{0,8},{4,12},{8,16},{12,20},{16,24},{20,28},{24,0},{28,4},{1,9},{5... | collective-permute-start | bytes 1572872 | tf_op jit(solution)/shard_map/ppermute | solution.py:231
  97.9 3.2 %collective-permute-done.17.refs_3_ = bf16[64,2048]{1,0:T(8,128)(2,1)S(1)} collective-permute-done((bf16[64,2048]{1,0:T(8,128)(2,1)S(1)}, bf16[64,2048]{1,0:T(8,128)(2,1)S(1)}, u32[]{:S(2)}, u32[]{:S(2)}) %collective-permute-start.17) | collective-permute-done | bytes 262176 | tf_op jit(solution)/shard_map/ppermute | solution.py:231
  101.1 3.5 %collective-permute-start.40 = (bf16[64,2048]{1,0:T(8,128)(2,1)S(1)}, bf16[64,2048]{1,0:T(8,128)(2,1)S(1)}, u32[]{:S(2)}, u32[]{:S(2)}) collective-permute-start(bf16[64,2048]{1,0:T(8,128)(2,1)S(1)} %collective-permute-done.39), channel_id=1, source_target_pairs={{0,24},{4,28},{8,0},{12,4},{16,8},{20,12},{24,16},{28,20},{1,25},{... | collective-permute-start | bytes 786440 | tf_op jit(solution)/shard_map/ppermute | solution.py:231
  104.7 22.2 %collective-permute-done.40 = bf16[64,2048]{1,0:T(8,128)(2,1)S(1)} collective-permute-done((bf16[64,2048]{1,0:T(8,128)(2,1)S(1)}, bf16[64,2048]{1,0:T(8,128)(2,1)S(1)}, u32[]{:S(2)}, u32[]{:S(2)}) %collective-permute-start.40) | collective-permute-done | bytes 262176 | tf_op jit(solution)/shard_map/ppermute | solution.py:231
  128.4 3.7 %collective-permute-done.31 = bf16[64,2048]{1,0:T(8,128)(2,1)S(1)} collective-permute-done((bf16[64,2048]{1,0:T(8,128)(2,1)S(1)}, bf16[64,2048]{1,0:T(8,128)(2,1)S(1)}, u32[]{:S(2)}, u32[]{:S(2)}) %collective-permute-start.31) | collective-permute-done | bytes 262176 | tf_op jit(solution)/shard_map/ppermute | solution.py:231
  136.2 4.2 %collective-permute-done.41 = bf16[64,2048]{1,0:T(8,128)(2,1)S(1)} collective-permute-done((bf16[64,2048]{1,0:T(8,128)(2,1)S(1)}, bf16[64,2048]{1,0:T(8,128)(2,1)S(1)}, u32[]{:S(2)}, u32[]{:S(2)}) %collective-permute-start.41) | collective-permute-done | bytes 262176 | tf_op jit(solution)/shard_map/ppermute | solution.py:231
  143.5 4.1 %collective-permute-done.32.refs_1_ = bf16[128,2048]{1,0:T(8,128)(2,1)S(1)} collective-permute-done((bf16[128,2048]{1,0:T(8,128)(2,1)S(1)}, bf16[128,2048]{1,0:T(8,128)(2,1)S(1)}, u32[]{:S(2)}, u32[]{:S(2)}) %collective-permute-start.32) | collective-permute-done | bytes 524320 | tf_op jit(solution)/shard_map/ppermute | solution.py:205
  148.1 15.6 %expert.3 = (bf16[512,2048]{1,0:T(8,128)(2,1)S(1)}, bf16[512,2048]{1,0:T(8,128)(2,1)S(1)}) custom-call(bf16[128,2048]{1,0:T(8,128)(2,1)S(1)} %get-tuple-element.25.refs_0_, bf16[128,2048]{1,0:T(8,128)(2,1)S(1)} %collective-permute-done.15.refs_1_, bf16[128,2048]{1,0:T(8,128)(2,1)S(1)} %collective-permute-done.16.refs_2_, ...), custom_call_target="tpu_custom_call" | custom-call | flops 11274289152 | bytes 19398656 | tf_op jit(solution)/shard_map/expert/pallas_call | solution.py:502
  164.3 9.0 %expert.4 = (bf16[256,2048]{1,0:T(8,128)(2,1)S(1)}, bf16[256,2048]{1,0:T(8,128)(2,1)S(1)}) custom-call(bf16[128,2048]{1,0:T(8,128)(2,1)S(1)} %constant_dynamic-update-slice_fusion.refs_0_, bf16[128,2048]{1,0:T(8,128)(2,1)S(1)} %collective-permute-done.32.refs_1_, bf16[128,2048]{1,0:T(8,128)(2,1)S(1)} %collective-permute-done.33.refs_2_, ...), custom_call_target="tpu_custom_call" | custom-call | flops 5637144576 | bytes 15204352 | tf_op jit(solution)/shard_map/expert/pallas_call | solution.py:502
  173.4 9.0 %expert.5 = (bf16[256,2048]{1,0:T(8,128)(2,1)S(1)}, bf16[256,2048]{1,0:T(8,128)(2,1)S(1)}) custom-call(bf16[128,2048]{1,0:T(8,128)(2,1)S(1)} %constant_dynamic-update-slice_fusion.2.refs_0_, bf16[128,2048]{1,0:T(8,128)(2,1)S(1)} %collective-permute-done.42.refs_1_, bf16[128,2048]{1,0:T(8,128)(2,1)S(1)} %collective-permute-done.43.refs_2_, ...), custom_call_target="tpu_custom_call" | custom-call | flops 5637144576 | bytes 15204352 | tf_op jit(solution)/shard_map/expert/pallas_call | solution.py:502
  187.9 10.0 %collective-permute-done.36 = bf16[128,2048]{1,0:T(8,128)(2,1)S(1)} collective-permute-done((bf16[128,2048]{1,0:T(8,128)(2,1)S(1)}, bf16[128,2048]{1,0:T(8,128)(2,1)S(1)}, u32[]{:S(2)}, u32[]{:S(2)}) %collective-permute-start.36) | collective-permute-done | bytes 524320 | tf_op jit(solution)/shard_map/ppermute | solution.py:205
  198.2 5.1 %collective-permute-start.37 = (bf16[64,2048]{1,0:T(8,128)(2,1)S(1)}, bf16[64,2048]{1,0:T(8,128)(2,1)S(1)}, u32[]{:S(2)}, u32[]{:S(2)}) collective-permute-start(bf16[64,2048]{1,0:T(8,128)(2,1)S(1)} %get-tuple-element.44), channel_id=1, source_target_pairs={{0,28},{4,24},{8,4},{12,0},{16,12},{20,8},{24,20},{28,16},{1,29},{... | collective-permute-start | bytes 786440 | tf_op jit(solution)/shard_map/ppermute | solution.py:231
  203.3 5.8 %collective-permute-done.46 = bf16[128,2048]{1,0:T(8,128)(2,1)S(1)} collective-permute-done((bf16[128,2048]{1,0:T(8,128)(2,1)S(1)}, bf16[128,2048]{1,0:T(8,128)(2,1)S(1)}, u32[]{:S(2)}, u32[]{:S(2)}) %collective-permute-start.46) | collective-permute-done | bytes 524320 | tf_op jit(solution)/shard_map/ppermute | solution.py:205
  213.5 17.2 %collective-permute-done.25 = bf16[256,2048]{1,0:T(8,128)(2,1)S(1)} collective-permute-done((bf16[256,2048]{1,0:T(8,128)(2,1)S(1)}, bf16[256,2048]{1,0:T(8,128)(2,1)S(1)}, u32[]{:S(2)}, u32[]{:S(2)}) %collective-permute-start.25) | collective-permute-done | bytes 1048608 | tf_op jit(solution)/shard_map/ppermute | solution.py:205
  233.8 4.0 %collective-permute-start.27 = (bf16[64,2048]{1,0:T(8,128)(2,1)}, bf16[64,2048]{1,0:T(8,128)(2,1)S(1)}, u32[]{:S(2)}, u32[]{:S(2)}) collective-permute-start(bf16[64,2048]{1,0:T(8,128)(2,1)} %get-tuple-element.40), channel_id=1, source_target_pairs={{0,24},{4,28},{8,0},{12,4},{16,8},{20,12},{24,16},{28,20},{1,25},{... | collective-permute-start | bytes 786440 | tf_op jit(solution)/shard_map/ppermute | solution.py:231
  238.1 4.1 %collective-permute-done.26.refs_5_ = bf16[64,2048]{1,0:T(8,128)(2,1)S(1)} collective-permute-done((bf16[64,2048]{1,0:T(8,128)(2,1)}, bf16[64,2048]{1,0:T(8,128)(2,1)S(1)}, u32[]{:S(2)}, u32[]{:S(2)}) %collective-permute-start.26) | collective-permute-done | bytes 262176 | tf_op jit(solution)/shard_map/ppermute | solution.py:231
  242.2 2.6 %collective-permute-done.27.refs_6_ = bf16[64,2048]{1,0:T(8,128)(2,1)S(1)} collective-permute-done((bf16[64,2048]{1,0:T(8,128)(2,1)}, bf16[64,2048]{1,0:T(8,128)(2,1)S(1)}, u32[]{:S(2)}, u32[]{:S(2)}) %collective-permute-start.27) | collective-permute-done | bytes 262176 | tf_op jit(solution)/shard_map/ppermute | solution.py:231
  244.8 4.2 %collective-permute-done.49.refs_10_ = bf16[64,2048]{1,0:T(8,128)(2,1)S(1)} collective-permute-done((bf16[64,2048]{1,0:T(8,128)(2,1)}, bf16[64,2048]{1,0:T(8,128)(2,1)S(1)}, u32[]{:S(2)}, u32[]{:S(2)}) %collective-permute-start.49) | collective-permute-done | bytes 262176 | tf_op jit(solution)/shard_map/ppermute | solution.py:231
  (130 shorter events, 52.4 us)
Async XLA Ops:
  2.5 12.0 %collective-permute-start.2 = (bf16[544,256]{1,0:T(8,128)(2,1)S(1)}, bf16[544,256]{1,0:T(8,128)(2,1)S(1)}, u32[]{:S(2)}, u32[]{:S(2)}) collective-permute-start(bf16[544,256]{1,0:T(8,128)(2,1)S(1)} %concatenate.16.refs_5_), channel_id=1, source_target_pairs={{0,8},{4,12},{8,16},{12,20},{16,24},{20,28},{1,9},{5,13},{9,17},{1... | collective-permute-start | bytes 835592 | tf_op jit(solution)/shard_map/ppermute | solution.py:163
  7.5 14.9 %collective-permute-start.3 = (bf16[512,256]{1,0:T(8,128)(2,1)}, bf16[512,256]{1,0:T(8,128)(2,1)S(1)}, u32[]{:S(2)}, u32[]{:S(2)}) collective-permute-start(bf16[512,256]{1,0:T(8,128)(2,1)} %refs_6_.2), channel_id=1, source_target_pairs={{0,8},{4,12},{8,16},{12,20},{16,24},{20,28},{1,9},{5,13},{9,17},{1... | collective-permute-start | bytes 786440 | tf_op jit(solution)/shard_map/ppermute | solution.py:163
  14.5 14.2 %collective-permute-start.6 = (bf16[544,256]{1,0:T(8,128)(2,1)S(1)}, bf16[544,256]{1,0:T(8,128)(2,1)S(1)}, u32[]{:S(2)}, u32[]{:S(2)}) collective-permute-start(bf16[544,256]{1,0:T(8,128)(2,1)S(1)} %collective-permute-done.2.refs_9_), channel_id=1, source_target_pairs={{0,8},{4,12},{8,16},{12,20},{16,24},{20,28},{1,9},{5,13},{9,17},{1... | collective-permute-start | bytes 835592 | tf_op jit(solution)/shard_map/ppermute | solution.py:163
  28.7 20.4 %collective-permute-start.4 = (bf16[544,256]{1,0:T(8,128)(2,1)S(1)}, bf16[544,256]{1,0:T(8,128)(2,1)S(1)}, u32[]{:S(2)}, u32[]{:S(2)}) collective-permute-start(bf16[544,256]{1,0:T(8,128)(2,1)S(1)} %collective-permute-done.2.refs_9_), channel_id=1, source_target_pairs={{0,4},{8,12},{16,20},{24,28},{4,0},{12,8},{20,16},{28,24},{1,5},{9... | collective-permute-start | bytes 835592 | tf_op jit(solution)/shard_map/ppermute | solution.py:164
  28.7 23.1 %collective-permute-start.8 = (bf16[544,256]{1,0:T(8,128)(2,1)S(1)}, bf16[544,256]{1,0:T(8,128)(2,1)S(1)}, u32[]{:S(2)}, u32[]{:S(2)}) collective-permute-start(bf16[544,256]{1,0:T(8,128)(2,1)S(1)} %collective-permute-done.6.refs_13_), channel_id=1, source_target_pairs={{4,0},{12,8},{20,16},{28,24},{5,1},{13,9},{21,17},{29,25},{6,2},{1... | collective-permute-start | bytes 835592 | tf_op jit(solution)/shard_map/ppermute | solution.py:164
  30.1 19.0 %collective-permute-start.5 = (bf16[512,256]{1,0:T(8,128)(2,1)S(1)}, bf16[512,256]{1,0:T(8,128)(2,1)}, u32[]{:S(2)}, u32[]{:S(2)}) collective-permute-start(bf16[512,256]{1,0:T(8,128)(2,1)S(1)} %collective-permute-done.3.refs_10_), channel_id=1, source_target_pairs={{0,4},{8,12},{16,20},{24,28},{4,0},{12,8},{20,16},{28,24},{1,5},{9... | collective-permute-start | bytes 786440 | tf_op jit(solution)/shard_map/ppermute | solution.py:164
  32.8 19.1 %collective-permute-start.9 = (bf16[512,256]{1,0:T(8,128)(2,1)}, bf16[512,256]{1,0:T(8,128)(2,1)}, u32[]{:S(2)}, u32[]{:S(2)}) collective-permute-start(bf16[512,256]{1,0:T(8,128)(2,1)} %collective-permute-done.7.refs_14_), channel_id=1, source_target_pairs={{4,0},{12,8},{20,16},{28,24},{5,1},{13,9},{21,17},{29,25},{6,2},{1... | collective-permute-start | bytes 786440 | tf_op jit(solution)/shard_map/ppermute | solution.py:164
  35.7 34.9 %collective-permute-start.13 = (bf16[128,2048]{1,0:T(8,128)(2,1)}, bf16[128,2048]{1,0:T(8,128)(2,1)S(1)}, u32[]{:S(2)}, u32[]{:S(2)}) collective-permute-start(bf16[128,2048]{1,0:T(8,128)(2,1)} %refs_6_.3), channel_id=1, source_target_pairs={{0,2},{1,3},{2,0},{3,1},{4,6},{5,7},{6,4},{7,5},{8,10},{9,11},{10,... | collective-permute-start | bytes 1572872 | tf_op jit(solution)/shard_map/ppermute | solution.py:205
  78.3 13.9 %collective-permute-start.39 = (bf16[64,2048]{1,0:T(8,128)(2,1)S(1)}, bf16[64,2048]{1,0:T(8,128)(2,1)S(1)}, u32[]{:S(2)}, u32[]{:S(2)}) collective-permute-start(bf16[64,2048]{1,0:T(8,128)(2,1)S(1)} %get-tuple-element.36), channel_id=1, source_target_pairs={{0,4},{4,0},{8,12},{12,8},{16,20},{20,16},{24,28},{28,24},{1,5},{5... | collective-permute-start | bytes 786440 | tf_op jit(solution)/shard_map/ppermute | solution.py:231
  78.4 19.4 %collective-permute-start.38 = (bf16[64,2048]{1,0:T(8,128)(2,1)S(1)}, bf16[64,2048]{1,0:T(8,128)(2,1)S(1)}, u32[]{:S(2)}, u32[]{:S(2)}) collective-permute-start(bf16[64,2048]{1,0:T(8,128)(2,1)S(1)} %get-tuple-element.35), channel_id=1, source_target_pairs={{0,16},{4,20},{8,24},{12,28},{16,0},{20,4},{24,8},{28,12},{1,17},{... | collective-permute-start | bytes 786440 | tf_op jit(solution)/shard_map/ppermute | solution.py:231
  79.8 18.0 %collective-permute-start.30 = (bf16[64,2048]{1,0:T(8,128)(2,1)S(1)}, bf16[64,2048]{1,0:T(8,128)(2,1)S(1)}, u32[]{:S(2)}, u32[]{:S(2)}) collective-permute-start(bf16[64,2048]{1,0:T(8,128)(2,1)S(1)} %get-tuple-element.32), channel_id=1, source_target_pairs={{0,4},{4,0},{8,12},{12,8},{16,20},{20,16},{24,28},{28,24},{1,5},{5... | collective-permute-start | bytes 786440 | tf_op jit(solution)/shard_map/ppermute | solution.py:231
  80.8 20.3 %collective-permute-start.17 = (bf16[64,2048]{1,0:T(8,128)(2,1)S(1)}, bf16[64,2048]{1,0:T(8,128)(2,1)S(1)}, u32[]{:S(2)}, u32[]{:S(2)}) collective-permute-start(bf16[64,2048]{1,0:T(8,128)(2,1)S(1)} %get-tuple-element.28), channel_id=1, source_target_pairs={{0,4},{4,0},{8,12},{12,8},{16,20},{20,16},{24,28},{28,24},{1,5},{5... | collective-permute-start | bytes 786440 | tf_op jit(solution)/shard_map/ppermute | solution.py:231
  85.4 19.2 %collective-permute-start.29 = (bf16[64,2048]{1,0:T(8,128)(2,1)S(1)}, bf16[64,2048]{1,0:T(8,128)(2,1)S(1)}, u32[]{:S(2)}, u32[]{:S(2)}) collective-permute-start(bf16[64,2048]{1,0:T(8,128)(2,1)S(1)} %collective-permute-done.28), channel_id=1, source_target_pairs={{0,8},{4,12},{8,16},{12,20},{16,24},{20,28},{24,0},{28,4},{1,9},{5... | collective-permute-start | bytes 786440 | tf_op jit(solution)/shard_map/ppermute | solution.py:231
  92.2 41.9 %collective-permute-start.15 = (bf16[128,2048]{1,0:T(8,128)(2,1)S(1)}, bf16[128,2048]{1,0:T(8,128)(2,1)S(1)}, u32[]{:S(2)}, u32[]{:S(2)}) collective-permute-start(bf16[128,2048]{1,0:T(8,128)(2,1)S(1)} %get-tuple-element.26), channel_id=1, source_target_pairs={{0,8},{4,12},{8,16},{12,20},{16,24},{20,28},{24,0},{28,4},{1,9},{5... | collective-permute-start | bytes 1572872 | tf_op jit(solution)/shard_map/ppermute | solution.py:231
  97.8 37.9 %collective-permute-start.16 = (bf16[128,2048]{1,0:T(8,128)(2,1)S(1)}, bf16[128,2048]{1,0:T(8,128)(2,1)S(1)}, u32[]{:S(2)}, u32[]{:S(2)}) collective-permute-start(bf16[128,2048]{1,0:T(8,128)(2,1)S(1)} %get-tuple-element.27), channel_id=1, source_target_pairs={{0,24},{4,28},{8,0},{12,4},{16,8},{20,12},{24,16},{28,20},{1,25},{... | collective-permute-start | bytes 1572872 | tf_op jit(solution)/shard_map/ppermute | solution.py:231
  97.8 37.8 %collective-permute-start.19 = (bf16[128,2048]{1,0:T(8,128)(2,1)S(1)}, bf16[128,2048]{1,0:T(8,128)(2,1)S(1)}, u32[]{:S(2)}, u32[]{:S(2)}) collective-permute-start(bf16[128,2048]{1,0:T(8,128)(2,1)S(1)} %get-tuple-element.25.refs_0_), channel_id=1, source_target_pairs={{0,1},{1,0},{2,3},{3,2},{4,5},{5,4},{6,7},{7,6},{8,9},{9,8},{10,11... | collective-permute-start | bytes 1572872 | tf_op jit(solution)/shard_map/ppermute | solution.py:205
  101.1 25.8 %collective-permute-start.40 = (bf16[64,2048]{1,0:T(8,128)(2,1)S(1)}, bf16[64,2048]{1,0:T(8,128)(2,1)S(1)}, u32[]{:S(2)}, u32[]{:S(2)}) collective-permute-start(bf16[64,2048]{1,0:T(8,128)(2,1)S(1)} %collective-permute-done.39), channel_id=1, source_target_pairs={{0,24},{4,28},{8,0},{12,4},{16,8},{20,12},{24,16},{28,20},{1,25},{... | collective-permute-start | bytes 786440 | tf_op jit(solution)/shard_map/ppermute | solution.py:231
  104.7 27.5 %collective-permute-start.31 = (bf16[64,2048]{1,0:T(8,128)(2,1)S(1)}, bf16[64,2048]{1,0:T(8,128)(2,1)S(1)}, u32[]{:S(2)}, u32[]{:S(2)}) collective-permute-start(bf16[64,2048]{1,0:T(8,128)(2,1)S(1)} %collective-permute-done.30), channel_id=1, source_target_pairs={{0,24},{4,28},{8,0},{12,4},{16,8},{20,12},{24,16},{28,20},{1,25},{... | collective-permute-start | bytes 786440 | tf_op jit(solution)/shard_map/ppermute | solution.py:231
  134.1 13.5 %collective-permute-start.32 = (bf16[128,2048]{1,0:T(8,128)(2,1)S(1)}, bf16[128,2048]{1,0:T(8,128)(2,1)S(1)}, u32[]{:S(2)}, u32[]{:S(2)}) collective-permute-start(bf16[128,2048]{1,0:T(8,128)(2,1)S(1)} %constant_dynamic-update-slice_fusion.refs_0_), channel_id=1, source_target_pairs={{0,2},{1,3},{2,0},{3,1},{4,6},{5,7},{6,4},{7,5},{8,10},{9,11},{10,... | collective-permute-start | bytes 1572872 | tf_op jit(solution)/shard_map/ppermute | solution.py:205
  135.6 12.5 %collective-permute-start.21 = (bf16[128,2048]{1,0:T(8,128)(2,1)S(1)}, bf16[128,2048]{1,0:T(8,128)(2,1)S(1)}, u32[]{:S(2)}, u32[]{:S(2)}) collective-permute-start(bf16[128,2048]{1,0:T(8,128)(2,1)S(1)} %collective-permute-done.16.refs_2_), channel_id=1, source_target_pairs={{0,1},{1,0},{2,3},{3,2},{4,5},{5,4},{6,7},{7,6},{8,9},{9,8},{10,11... | collective-permute-start | bytes 1572872 | tf_op jit(solution)/shard_map/ppermute | solution.py:205
  140.5 23.8 %collective-permute-start.33 = (bf16[128,2048]{1,0:T(8,128)(2,1)S(1)}, bf16[128,2048]{1,0:T(8,128)(2,1)S(1)}, u32[]{:S(2)}, u32[]{:S(2)}) collective-permute-start(bf16[128,2048]{1,0:T(8,128)(2,1)S(1)} %constant_dynamic-update-slice_fusion.refs_0_), channel_id=1, source_target_pairs={{0,1},{1,0},{2,3},{3,2},{4,5},{5,4},{6,7},{7,6},{8,9},{9,8},{10,11... | collective-permute-start | bytes 1572872 | tf_op jit(solution)/shard_map/ppermute | solution.py:205
  141.9 21.8 %collective-permute-start.42 = (bf16[128,2048]{1,0:T(8,128)(2,1)S(1)}, bf16[128,2048]{1,0:T(8,128)(2,1)S(1)}, u32[]{:S(2)}, u32[]{:S(2)}) collective-permute-start(bf16[128,2048]{1,0:T(8,128)(2,1)S(1)} %constant_dynamic-update-slice_fusion.2.refs_0_), channel_id=1, source_target_pairs={{0,2},{1,3},{2,0},{3,1},{4,6},{5,7},{6,4},{7,5},{8,10},{9,11},{10,... | collective-permute-start | bytes 1572872 | tf_op jit(solution)/shard_map/ppermute | solution.py:205
  147.6 25.8 %collective-permute-start.43 = (bf16[128,2048]{1,0:T(8,128)(2,1)S(1)}, bf16[128,2048]{1,0:T(8,128)(2,1)S(1)}, u32[]{:S(2)}, u32[]{:S(2)}) collective-permute-start(bf16[128,2048]{1,0:T(8,128)(2,1)S(1)} %constant_dynamic-update-slice_fusion.2.refs_0_), channel_id=1, source_target_pairs={{0,1},{1,0},{2,3},{3,2},{4,5},{5,4},{6,7},{7,6},{8,9},{9,8},{10,11... | collective-permute-start | bytes 1572872 | tf_op jit(solution)/shard_map/ppermute | solution.py:205
  147.6 16.7 %collective-permute-start.34 = (bf16[128,2048]{1,0:T(8,128)(2,1)S(1)}, bf16[128,2048]{1,0:T(8,128)(2,1)S(1)}, u32[]{:S(2)}, u32[]{:S(2)}) collective-permute-start(bf16[128,2048]{1,0:T(8,128)(2,1)S(1)} %collective-permute-done.32.refs_1_), channel_id=1, source_target_pairs={{0,1},{1,0},{2,3},{3,2},{4,5},{5,4},{6,7},{7,6},{8,9},{9,8},{10,11... | collective-permute-start | bytes 1572872 | tf_op jit(solution)/shard_map/ppermute | solution.py:205
  163.7 23.2 %collective-permute-start.24 = (bf16[512,2048]{1,0:T(8,128)(2,1)S(1)}, bf16[512,2048]{1,0:T(8,128)(2,1)S(1)}, u32[]{:S(2)}, u32[]{:S(2)}) collective-permute-start(bf16[512,2048]{1,0:T(8,128)(2,1)S(1)} %get-tuple-element.30), channel_id=1, source_target_pairs={{0,1},{1,0},{2,3},{3,2},{4,5},{5,4},{6,7},{7,6},{8,9},{9,8},{10,11... | collective-permute-start | bytes 6291464 | tf_op jit(solution)/shard_map/ppermute | solution.py:205
  183.0 14.9 %collective-permute-start.36 = (bf16[128,2048]{1,0:T(8,128)(2,1)S(1)}, bf16[128,2048]{1,0:T(8,128)(2,1)S(1)}, u32[]{:S(2)}, u32[]{:S(2)}) collective-permute-start(bf16[128,2048]{1,0:T(8,128)(2,1)S(1)} %add_convert_fusion.5), channel_id=1, source_target_pairs={{0,2},{1,3},{2,0},{3,1},{4,6},{5,7},{6,4},{7,5},{8,10},{9,11},{10,... | collective-permute-start | bytes 1572872 | tf_op jit(solution)/shard_map/ppermute | solution.py:205
  185.3 23.8 %collective-permute-start.46 = (bf16[128,2048]{1,0:T(8,128)(2,1)S(1)}, bf16[128,2048]{1,0:T(8,128)(2,1)S(1)}, u32[]{:S(2)}, u32[]{:S(2)}) collective-permute-start(bf16[128,2048]{1,0:T(8,128)(2,1)S(1)} %add_convert_fusion.3), channel_id=1, source_target_pairs={{0,2},{1,3},{2,0},{3,1},{4,6},{5,7},{6,4},{7,5},{8,10},{9,11},{10,... | collective-permute-start | bytes 1572872 | tf_op jit(solution)/shard_map/ppermute | solution.py:205
  187.3 43.4 %collective-permute-start.25 = (bf16[256,2048]{1,0:T(8,128)(2,1)S(1)}, bf16[256,2048]{1,0:T(8,128)(2,1)S(1)}, u32[]{:S(2)}, u32[]{:S(2)}) collective-permute-start(bf16[256,2048]{1,0:T(8,128)(2,1)S(1)} %add_convert_fusion.1), channel_id=1, source_target_pairs={{0,2},{1,3},{2,0},{3,1},{4,6},{5,7},{6,4},{7,5},{8,10},{9,11},{10,... | collective-permute-start | bytes 3145736 | tf_op jit(solution)/shard_map/ppermute | solution.py:205
  198.2 35.7 %collective-permute-start.37 = (bf16[64,2048]{1,0:T(8,128)(2,1)S(1)}, bf16[64,2048]{1,0:T(8,128)(2,1)S(1)}, u32[]{:S(2)}, u32[]{:S(2)}) collective-permute-start(bf16[64,2048]{1,0:T(8,128)(2,1)S(1)} %get-tuple-element.44), channel_id=1, source_target_pairs={{0,28},{4,24},{8,4},{12,0},{16,12},{20,8},{24,20},{28,16},{1,29},{... | collective-permute-start | bytes 786440 | tf_op jit(solution)/shard_map/ppermute | solution.py:231
  203.3 34.5 %collective-permute-start.50 = (bf16[64,2048]{1,0:T(8,128)(2,1)S(1)}, bf16[64,2048]{1,0:T(8,128)(2,1)S(1)}, u32[]{:S(2)}, u32[]{:S(2)}) collective-permute-start(bf16[64,2048]{1,0:T(8,128)(2,1)S(1)} %get-tuple-element.43), channel_id=1, source_target_pairs={{0,12},{4,8},{8,20},{12,16},{16,28},{20,24},{24,4},{28,0},{1,13},{... | collective-permute-start | bytes 786440 | tf_op jit(solution)/shard_map/ppermute | solution.py:231
  209.4 28.6 %collective-permute-start.47 = (bf16[64,2048]{1,0:T(8,128)(2,1)S(1)}, bf16[64,2048]{1,0:T(8,128)(2,1)S(1)}, u32[]{:S(2)}, u32[]{:S(2)}) collective-permute-start(bf16[64,2048]{1,0:T(8,128)(2,1)S(1)} %get-tuple-element.46), channel_id=1, source_target_pairs={{0,16},{4,20},{8,24},{12,28},{16,0},{20,4},{24,8},{28,12},{1,17},{... | collective-permute-start | bytes 786440 | tf_op jit(solution)/shard_map/ppermute | solution.py:231
  211.0 27.1 %collective-permute-start.48 = (bf16[64,2048]{1,0:T(8,128)(2,1)S(1)}, bf16[64,2048]{1,0:T(8,128)(2,1)S(1)}, u32[]{:S(2)}, u32[]{:S(2)}) collective-permute-start(bf16[64,2048]{1,0:T(8,128)(2,1)S(1)} %get-tuple-element.45), channel_id=1, source_target_pairs={{0,20},{4,16},{8,28},{12,24},{16,4},{20,0},{24,12},{28,8},{1,21},{... | collective-permute-start | bytes 786440 | tf_op jit(solution)/shard_map/ppermute | solution.py:231
  (30 other events, 367.7 us)

commit v3 on v0

--- a/solution.py
+++ b/solution.py
@@ -21,8 +21,7 @@
 def attention_kernel(tokens, heads, head_size, tile, sources, *refs):
     valid_ref, docs_ref, q_ref, meta_ref, gain_ref = refs[:5]
     kv_refs = refs[5 : 5 + 2 * sources]
-    mine_ref, other_ref = refs[5 + 2 * sources : 7 + 2 * sources]
-    m_ref, l_ref, acc_ref = refs[7 + 2 * sources :]
+    out_ref, m_ref, l_ref, acc_ref = refs[5 + 2 * sources :]
     width = heads * head_size
     halves = tokens // width
     rows = tokens // head_size
@@ -108,17 +107,7 @@
             for h in range(heads)
         ]
         scale = spread([lax.rsqrt(mean + EPS) for mean in means])
-        normed = (attended * scale * gain_ref[...]).astype(jnp.bfloat16)
-        here = pl.ds(pl.multiple_of((step // 2) * tile, tile), tile)
-
-        @pl.when(step % 2 == valid_ref[sources])
-        def _():
-            mine_ref[here, :] = normed
-
-        @pl.when(step % 2 != valid_ref[sources])
-        def _():
-            other_ref[here, :] = normed
-
+        out_ref[pl.ds(row0, tile), :] = (attended * scale * gain_ref[...]).astype(jnp.bfloat16)
         return carry
 
     lax.fori_loop(0, tokens // tile, q_tile, 0)
@@ -130,7 +119,7 @@
     head_size = width // heads
     n_sp = lax.axis_size("sp")
     place = lax.axis_index("sp")
-    tile = tokens // lax.axis_size("tp")
+    tile = tokens // 2
 
     gate_rows = [part.T.reshape(-1, width) for part in bf16_parts(cum_gate)]
     doc_rows = documents.astype(jnp.bfloat16).reshape(-1, width)
@@ -175,7 +164,7 @@
             exists = exists & (member == 0)
         valid.append(exists)
     sources = len(valid)
-    valid = jnp.stack(valid + [lax.axis_index("tp") % 2 == 1]).astype(jnp.int32)
+    valid = jnp.stack(valid).astype(jnp.int32)
 
     def kernel(*refs):
         attention_kernel(tokens, heads, head_size, tile, sources, *refs)
@@ -184,9 +173,9 @@
     smem = pl.BlockSpec(memory_space=pltpu.SMEM)
     return pl.pallas_call(
         kernel,
-        out_shape=[jax.ShapeDtypeStruct((tokens // 2, width), jnp.bfloat16)] * 2,
+        out_shape=jax.ShapeDtypeStruct((tokens, width), jnp.bfloat16),
         in_specs=[smem, smem] + [vmem] * (3 + len(blocks)),
-        out_specs=[vmem, vmem],
+        out_specs=vmem,
         scratch_shapes=[
             pltpu.VMEM((heads, tile, 1), jnp.float32),
             pltpu.VMEM((heads, tile, 1), jnp.float32),
@@ -201,58 +190,20 @@
     return lax.ppermute(x, axis, [(i, i ^ bits) for i in range(lax.axis_size(axis))])
 
 
-def far_places(n_sp):
-    return [k for k in range(n_sp) if k & (n_sp // 2) and not k & (n_sp // 4)]
-
-
-def expert_groups(n_sp):
-    far = far_places(n_sp)
-    near = [k ^ (k >> 1) for k in range(n_sp)]
-    near = [k for k in near if k not in far]
-    size = n_sp // 4
-    return [near[:size], near[size : 2 * size], far[::-1], near[2 * size :]]
-
-
-def project_kernel(experts, capacity, n_tp, far, *refs):
-    blocks = n_tp // 2
-    place_ref = refs[0]
-    pieces = refs[1 : 1 + n_tp]
-    weight_ref = refs[1 + n_tp]
-    resids = refs[2 + n_tp : 2 + n_tp + blocks]
-    routes = refs[2 + n_tp + blocks : 2 + n_tp + 2 * blocks]
-    gain_ref = refs[2 + n_tp + 2 * blocks]
-    outs = refs[3 + n_tp + 2 * blocks : 3 + n_tp + 2 * blocks + experts]
-    stream_ref, wide_ref, packed_ref, slot_ref, pick_ref = refs[3 + n_tp + 2 * blocks + experts :]
-    rows, width = resids[0].shape
-    part = pieces[0].shape[1]
-    place, spot = place_ref[0], place_ref[1]
-    across = spot // 2
+CHUNKS = 2
+
+
+def project_kernel(experts, capacity, x_ref, weight_ref, resid_ref, routes_ref, gain_ref, *refs):
+    outs = refs[:CHUNKS]
+    stream_ref, wide_ref, pick_ref = refs[CHUNKS:]
+    rows, width = resid_ref.shape
     n_tile = 512
-
-    inputs = [
-        jnp.concatenate(
-            [
-                piece[pl.ds(pl.multiple_of((across ^ j) * rows, rows), rows), :]
-                for j in range(blocks)
-            ],
-            axis=0,
-        )
-        for piece in pieces
-    ]
-    total = jnp.zeros((blocks * rows, 1), jnp.float32)
+    total = jnp.zeros((rows, 1), jnp.float32)
     for n in range(width // n_tile):
         cols = slice(n * n_tile, (n + 1) * n_tile)
-        projected = jnp.zeros((blocks * rows, n_tile), jnp.float32)
-        for k in range(n_tp):
-            from_row = pl.multiple_of((spot ^ k) * part, part)
-            projected = projected + jnp.dot(
-                inputs[k],
-                weight_ref[pl.ds(from_row, part), cols],
-                preferred_element_type=jnp.float32,
-            )
-        resid = jnp.concatenate([resid_ref[:, cols] for resid_ref in resids], axis=0)
-        stream = (resid.astype(jnp.float32) + projected).astype(jnp.bfloat16)
-        stream_ref[:, cols] = stream[:rows]
+        projected = jnp.dot(x_ref[...], weight_ref[:, cols], preferred_element_type=jnp.float32)
+        stream = (resid_ref[:, cols].astype(jnp.float32) + projected).astype(jnp.bfloat16)
+        stream_ref[:, cols] = stream
         wide = stream.astype(jnp.float32)
         wide_ref[:, cols] = wide
         total = total + jnp.sum(wide * wide, axis=1, keepdims=True)
@@ -263,33 +214,26 @@
         < lax.broadcasted_iota(jnp.int32, (rows, rows), 1)
     ).astype(jnp.bfloat16)
     expert_ids = lax.broadcasted_iota(jnp.int32, (experts, rows), 0).astype(jnp.float32)
-    for j in range(blocks):
-        chosen = jnp.zeros((experts, rows), jnp.float32)
-        for route in range(2):
-            chosen = chosen + (routes[j][route : route + 1, :] == expert_ids).astype(jnp.float32)
-        ranks = jnp.dot(chosen.astype(jnp.bfloat16), before, preferred_element_type=jnp.float32)
-        slot_ref[j] = jnp.where(chosen > 0.0, ranks, -1.0)
-    slot_ids = lax.broadcasted_iota(jnp.int32, (capacity, rows), 0).astype(jnp.float32)
-    first, spans = 0, []
-    for k in range(experts):
-        spans.append(first)
-        for j in range(1 if k in far else blocks):
-            row_of = slot_ref[j, pl.ds(place ^ k, 1), :]
-            for i in range(blocks):
-                pick = (slot_ids == row_of) if i == j else jnp.zeros((capacity, rows), jnp.bool_)
-                pick_ref[first : first + capacity, i * rows : (i + 1) * rows] = pick.astype(
-                    jnp.float32
-                ).astype(jnp.bfloat16)
-            first += capacity
-    spans.append(first)
+    chosen = jnp.zeros((experts, rows), jnp.float32)
+    for route in range(2):
+        chosen = chosen + (routes_ref[route : route + 1, :] == expert_ids).astype(jnp.float32)
+    ranks = jnp.dot(chosen.astype(jnp.bfloat16), before, preferred_element_type=jnp.float32)
+    slots = jnp.where(chosen > 0.0, ranks, -1.0)
+    span = capacity // CHUNKS
+    for c in range(CHUNKS):
+        slot_ids = lax.broadcasted_iota(jnp.int32, (span, rows), 0) + c * span
+        for e in range(experts):
+            pick = (slot_ids.astype(jnp.float32) == slots[e : e + 1, :]).astype(jnp.float32)
+            first = (c * experts + e) * span
+            pick_ref[first : first + span, :] = pick
+    each = experts * span
+    picks = pick_ref[...].astype(jnp.bfloat16)
     for n in range(width // n_tile):
         cols = slice(n * n_tile, (n + 1) * n_tile)
-        packed_ref[...] = (wide_ref[:, cols] * scale * gain_ref[:, cols]).astype(jnp.bfloat16)
-        picked = jnp.dot(
-            pick_ref[...], packed_ref[...], preferred_element_type=jnp.float32
-        ).astype(jnp.bfloat16)
-        for k in range(experts):
-            outs[k][:, cols] = picked[spans[k] : spans[k + 1]]
+        normed = (wide_ref[:, cols] * scale * gain_ref[:, cols]).astype(jnp.bfloat16)
+        picked = jnp.dot(picks, normed, preferred_element_type=jnp.float32).astype(jnp.bfloat16)
+        for c in range(CHUNKS):
+            outs[c][:, cols] = picked[c * each : (c + 1) * each]
 
 
 def expert_kernel(count, *refs):
@@ -328,13 +272,14 @@
             other_ref[:, cols] = out[mine_rows:]
 
 
-def combine_kernel(experts, place_ref, stream_ref, routes_ref, weights_ref, *refs):
-    outs = refs[:experts]
-    mixed_ref, stack_ref = refs[experts:]
+def combine_kernel(experts, stream_ref, routes_ref, weights_ref, *refs):
+    outs = refs[:CHUNKS]
+    mixed_ref, stack_ref = refs[CHUNKS:]
     rows, width = stream_ref.shape
-    capacity = outs[0].shape[0]
-    for k in range(experts):
-        stack_ref[k * capacity : (k + 1) * capacity, :] = outs[k][...]
+    each = outs[0].shape[0]
+    span = each // experts
+    for c in range(CHUNKS):
+        stack_ref[c * each : (c + 1) * each, :] = outs[c][...]
     expert_ids = lax.broadcasted_iota(jnp.int32, (rows, experts), 1)
     named = [
         (routes_ref[:, route : route + 1] == expert_ids).astype(jnp.float32) for route in range(2)
@@ -346,11 +291,12 @@
     ranks = jnp.dot(
         before, (named[0] + named[1]).astype(jnp.bfloat16), preferred_element_type=jnp.float32
     )
-    slot_ids = lax.broadcasted_iota(jnp.int32, (rows, experts * capacity), 1)
+    slot_ids = lax.broadcasted_iota(jnp.int32, (rows, CHUNKS * each), 1)
     picks = []
     for route in range(2):
         rank = jnp.sum(named[route] * ranks, axis=1, keepdims=True).astype(jnp.int32)
-        target = (routes_ref[:, route : route + 1] ^ place_ref[0]) * capacity + rank
+        chunk = rank // span
+        target = chunk * each + routes_ref[:, route : route + 1] * span + (rank - chunk * span)
         picks.append((slot_ids == target).astype(jnp.float32).astype(jnp.bfloat16))
     n_tile = 512
     for n in range(width // n_tile):
@@ -380,82 +326,57 @@
 ):
     tokens = queries.shape[0]
     n_sp, n_tp = lax.axis_size("sp"), lax.axis_size("tp")
-    place, spot = lax.axis_index("sp"), lax.axis_index("tp")
     blocks = n_tp // 2
     local_rows, model_width = resid.shape
     capacity = 2 * routes.shape[1] * tokens // (n_tp * n_sp)
-    each = blocks * capacity
+    span = capacity // CHUNKS
     vmem = pl.BlockSpec(memory_space=pltpu.VMEM)
-    smem = pl.BlockSpec(memory_space=pltpu.SMEM)
-    places = jnp.stack([place, spot]).astype(jnp.int32)
-
-    route_rows = jnp.concatenate(
-        [routes.T.astype(jnp.float32), jnp.zeros((8 - routes.shape[1], local_rows), jnp.float32)],
-        axis=0,
-    )
-    resids = [resid] + [swap(resid, "tp", 2 * j) for j in range(1, blocks)]
-    route_blocks = [route_rows] + [swap(route_rows, "tp", 2 * j) for j in range(1, blocks)]
-
-    mine, other = attend(queries, keys, values, cum_gate, documents, head_gain)
-    pieces = [mine] + [swap(other if k % 2 else mine, "tp", k) for k in range(1, n_tp)]
-
-    far = far_places(n_sp)
-    counts = [capacity if k in far else each for k in range(n_sp)]
+    route_rows = routes.T.astype(jnp.float32)
+
+    head_normed = attend(queries, keys, values, cum_gate, documents, head_gain)
+    regrouped = lax.all_to_all(head_normed, "tp", split_axis=0, concat_axis=1, tiled=True)
 
     def project(*refs):
-        project_kernel(n_sp, capacity, n_tp, far, *refs)
+        project_kernel(n_sp, capacity, *refs)
 
     *outbound, stream = pl.pallas_call(
         project,
-        out_shape=[jax.ShapeDtypeStruct((count, model_width), jnp.bfloat16) for count in counts]
+        out_shape=[jax.ShapeDtypeStruct((n_sp * span, model_width), jnp.bfloat16)] * CHUNKS
         + [jax.ShapeDtypeStruct((local_rows, model_width), jnp.bfloat16)],
-        in_specs=[smem] + [vmem] * (n_tp + 2 + 2 * blocks),
-        out_specs=[vmem] * (n_sp + 1),
+        in_specs=[vmem] * 5,
+        out_specs=[vmem] * (CHUNKS + 1),
         scratch_shapes=[
-            pltpu.VMEM((blocks * local_rows, model_width), jnp.float32),
-            pltpu.VMEM((blocks * local_rows, 512), jnp.bfloat16),
-            pltpu.VMEM((blocks, n_sp, local_rows), jnp.float32),
-            pltpu.VMEM((sum(counts), blocks * local_rows), jnp.bfloat16),
+            pltpu.VMEM((local_rows, model_width), jnp.float32),
+            pltpu.VMEM((n_sp * capacity, local_rows), jnp.float32),
         ],
         compiler_params=pltpu.CompilerParams(vmem_limit_bytes=40 * 2**20),
         name="project",
-    )(places, *pieces, out_weight, *resids, *route_blocks, norm_gain[None, :])
-
-    def hop(x, k):
-        if k == 0:
-            return x
-        if k in far and k % 2:
-            low, step = k % (n_sp // 2), n_sp // 4
-            x = lax.ppermute(x, "sp", [(i, ((i ^ low) - step) % n_sp) for i in range(n_sp)])
-            return lax.ppermute(x, "sp", [(i, (i - step) % n_sp) for i in range(n_sp)])
-        return swap(x, "sp", k)
-
-    groups = expert_groups(n_sp)
-    members = len(groups[0])
+    )(regrouped, out_weight, resid, route_rows, norm_gain[None, :])
+
     hidden_width = w_gate.shape[2]
     h_tile = 128
-    rows = 2 * members * each
-    arrived = {k: hop(outbound[k], k) for group in groups for k in group}
-    returned = {}
-    for group in groups:
-        inputs = []
-        for k in group:
-            inputs.append(arrived[k])
-            if k in far:
-                inputs += [swap(arrived[k], "tp", 2 * j) for j in range(1, blocks)]
+    each = n_sp * span
+    rows = n_tp * each
+    arrived, crossed = [], []
+    for c in range(CHUNKS):
+        arrived.append(lax.all_to_all(outbound[c], "sp", 0, 0, tiled=True))
+        crossed.append([swap(arrived[c], "tp", 2 * j) for j in range(1, blocks)])
+    returned = []
+    for c in range(CHUNKS):
+        inputs = [arrived[c], *crossed[c]]
         inputs += [swap(x, "tp", 1) for x in inputs]
 
         def expert(*refs):
-            expert_kernel(len(inputs), *refs)
+            expert_kernel(n_tp, *refs)
 
         part_mine, part_other = pl.pallas_call(
             expert,
             grid=(hidden_width // h_tile,),
-            out_shape=[jax.ShapeDtypeStruct((members * each, model_width), jnp.bfloat16)] * 2,
+            out_shape=[jax.ShapeDtypeStruct((rows // 2, model_width), jnp.bfloat16)] * 2,
             in_specs=[pl.BlockSpec(x.shape, lambda f: (0, 0)) for x in inputs]
             + [pl.BlockSpec((model_width, h_tile), lambda f: (0, f))] * 2
             + [pl.BlockSpec(memory_space=pl.ANY)],
-            out_specs=[pl.BlockSpec((members * each, model_width), lambda f: (0, 0))] * 2,
+            out_specs=[pl.BlockSpec((rows // 2, model_width), lambda f: (0, 0))] * 2,
             scratch_shapes=[
                 pltpu.VMEM((rows, model_width), jnp.bfloat16),
                 pltpu.VMEM((hidden_width // h_tile, rows, h_tile), jnp.bfloat16),
@@ -473,19 +394,18 @@
             name="expert",
         )(*inputs, w_gate[0], w_up[0], w_down[0])
         added = swap(part_other, "tp", 1)
-        shape = (members, blocks, capacity, model_width)
-        part_mine, added = part_mine.reshape(shape), added.reshape(shape)
 
         def summed(j):
-            return part_mine[:, j].astype(jnp.float32) + added[:, j].astype(jnp.float32)
+            here = slice(j * each, (j + 1) * each)
+            return part_mine[here].astype(jnp.float32) + added[here].astype(jnp.float32)
 
         result = summed(0)
         for j in range(1, blocks):
             sent = swap(summed(j).astype(jnp.bfloat16), "tp", 2 * j)
             result = result + sent.astype(jnp.float32)
-        result = result.astype(jnp.bfloat16)
-        for i, k in enumerate(group):
-            returned[k] = hop(result[i], k)
+        returned.append(
+            lax.all_to_all(result.astype(jnp.bfloat16), "sp", 0, 0, tiled=True)
+        )
 
     def combine(*refs):
         combine_kernel(n_sp, *refs)
@@ -493,12 +413,12 @@
     return pl.pallas_call(
         combine,
         out_shape=jax.ShapeDtypeStruct((local_rows, model_width), jnp.bfloat16),
-        in_specs=[smem] + [vmem] * (3 + n_sp),
+        in_specs=[vmem] * (3 + CHUNKS),
         out_specs=vmem,
         scratch_shapes=[pltpu.VMEM((n_sp * capacity, model_width), jnp.bfloat16)],
         compiler_params=pltpu.CompilerParams(vmem_limit_bytes=24 * 2**20),
         name="combine",
-    )(places, stream, routes, route_weights, *[returned[k] for k in range(n_sp)])
+    )(stream, routes, route_weights, *returned)
 
 
 def solution(mesh):

time: 290 us -> 295 us (1.017)
  starting transfers between devices: 106 us -> 49.8 us
  blocking collectives: 0 us -> 35.8 us
  waiting for transfers between devices: 118 us -> 145 us
  Pallas kernels: 50.8 us -> 43.4 us
    ppermute x37 -> x10, starting transfers between devices: 72.9 us -> 4.45 us  [swap(): lax.ppermute(x, axis, [(i, i ^ bits) for i in range(lax.axis_size(axis))])]
    all_to_all x0 -> x4, waiting for transfers between devices: none -> 54.7 us  [the longest x1 24.6 us: on_device(): arrived.append(lax.all_to_all(outbound[c], 'sp', 0, 0, tiled=True))]
    all_to_all x0 -> x1, blocking collectives: none -> 35.8 us  [on_device(): arrived.append(lax.all_to_all(outbound[c], 'sp', 0, 0, tiled=True))]
    ppermute x4 -> x0, waiting for transfers between devices: 33.4 us -> none  [the longest x2 17.7 us: hop(): return lax.ppermute(x, 'sp', [(i, (i - step) % n_sp) for i in range(n_sp)])]
    all_to_all x0 -> x4, starting transfers between devices: none -> 18.1 us  [the longest x2 11 us: on_device(): lax.all_to_all(result.astype(jnp.bfloat16), 'sp', 0, 0, tiled=True)]
    ppermute x4 -> x0, starting transfers between devices: 4.71 us -> none  [the longest x2 3.33 us: hop(): lax.ppermute(x, 'sp', [(i, ((i ^ low) - step) % n_sp) for i in range(n_sp)])]
    ppermute x37 -> x10, waiting for transfers between devices: 66.1 us -> 70.4 us  [swap(): lax.ppermute(x, axis, [(i, i ^ bits) for i in range(lax.axis_size(axis))])]
    unnamed x24 -> x32, local copies, waits for them, and re-layouts: 5.69 us -> 9.38 us
  transfers between devices with their start and end apart: 51 -> 24, of which waited for: 17 -> 10; matrix products, arithmetic and copies ran while one was open for 2% -> 3% of each run, Pallas kernels for 16% -> 11%
where the time goes in v3:
time: 295 us; the launch traced here: 294 us
  waiting for transfers between devices  145 us (49%)
  starting transfers between devices  49.8 us (17%)
  Pallas kernels  43.4 us (15%)
  blocking collectives  35.8 us (12%)
  local copies, waits for them, and re-layouts  10.8 us (4%)
  other arithmetic  8.54 us (3%)
    ppermute x10, waiting for transfers between devices, swap(): lax.ppermute(x, axis, [(i, i ^ bits) for i in range(lax.axis_size(axis))])  70.4 us
    all_to_all x1, blocking collectives, on_device(): arrived.append(lax.all_to_all(outbound[c], 'sp', 0, 0, tiled=True))  35.8 us
    pallas_call x2, Pallas kernels, on_device(): pl.pallas_call(expert, grid=(hidden_width // h_tile,), out_shape=[jax.Sha...  32.2 us
    all_to_all x1, waiting for transfers between devices, on_device(): arrived.append(lax.all_to_all(outbound[c], 'sp', 0, 0, tiled=True))  24.6 us
    all_to_all x2, waiting for transfers between devices, on_device(): lax.all_to_all(result.astype(jnp.bfloat16), 'sp', 0, 0, tiled=True)  24.1 us
    ppermute x6, waiting for transfers between devices, chain(): other.append(lax.ppermute(own[-1], 'sp', pairs))  16.6 us
    ppermute x4, starting transfers between devices, chain(): own.append(lax.ppermute(own[-1], 'sp', ahead))  16.3 us
    all_to_all x2, starting transfers between devices, on_device(): lax.all_to_all(result.astype(jnp.bfloat16), 'sp', 0, 0, tiled=True)  11 us
  transfers between devices with their start and end apart: 24, of which 10 were waited for; matrix products, arithmetic and copies ran while one was open for 3% of the time, Pallas kernels for 11%

profile of v3, /device:TPU:0, one launch (start us, length us, event | category | flops | bytes accessed | tf_op | source)
XLA Modules:
  0.0 293.9 jit_solution(12668357288929030250)
XLA Ops:
  2.5 5.0 %collective-permute-start.2 = (bf16[544,256]{1,0:T(8,128)(2,1)S(1)}, bf16[544,256]{1,0:T(8,128)(2,1)S(1)}, u32[]{:S(2)}, u32[]{:S(2)}) collective-permute-start(bf16[544,256]{1,0:T(8,128)(2,1)S(1)} %concatenate.7.refs_5_), channel_id=1, source_target_pairs={{0,8},{4,12},{8,16},{12,20},{16,24},{20,28},{1,9},{5,13},{9,17},{1... | collective-permute-start | bytes 835592 | tf_op jit(solution)/shard_map/ppermute | solution.py:148
  7.5 3.5 %collective-permute-start.3 = (bf16[512,256]{1,0:T(8,128)(2,1)}, bf16[512,256]{1,0:T(8,128)(2,1)S(1)}, u32[]{:S(2)}, u32[]{:S(2)}) collective-permute-start(bf16[512,256]{1,0:T(8,128)(2,1)} %refs_6_.1), channel_id=1, source_target_pairs={{0,8},{4,12},{8,16},{12,20},{16,24},{20,28},{1,9},{5,13},{9,17},{1... | collective-permute-start | bytes 786440 | tf_op jit(solution)/shard_map/ppermute | solution.py:148
  11.0 3.5 %collective-permute-done.2.refs_9_ = bf16[544,256]{1,0:T(8,128)(2,1)S(1)} collective-permute-done((bf16[544,256]{1,0:T(8,128)(2,1)S(1)}, bf16[544,256]{1,0:T(8,128)(2,1)S(1)}, u32[]{:S(2)}, u32[]{:S(2)}) %collective-permute-start.2) | collective-permute-done | bytes 278560 | tf_op jit(solution)/shard_map/ppermute | solution.py:148
  14.5 4.4 %collective-permute-start.6 = (bf16[544,256]{1,0:T(8,128)(2,1)S(1)}, bf16[544,256]{1,0:T(8,128)(2,1)S(1)}, u32[]{:S(2)}, u32[]{:S(2)}) collective-permute-start(bf16[544,256]{1,0:T(8,128)(2,1)S(1)} %collective-permute-done.2.refs_9_), channel_id=1, source_target_pairs={{0,8},{4,12},{8,16},{12,20},{16,24},{20,28},{1,9},{5,13},{9,17},{1... | collective-permute-start | bytes 835592 | tf_op jit(solution)/shard_map/ppermute | solution.py:148
  18.9 3.4 %collective-permute-start.1 = (bf16[512,256]{1,0:T(8,128)(2,1)}, bf16[512,256]{1,0:T(8,128)(2,1)S(1)}, u32[]{:S(2)}, u32[]{:S(2)}) collective-permute-start(bf16[512,256]{1,0:T(8,128)(2,1)} %refs_6_.1), channel_id=1, source_target_pairs={{0,4},{8,12},{16,20},{24,28},{1,5},{9,13},{17,21},{25,29},{2,6},{1... | collective-permute-start | bytes 786440 | tf_op jit(solution)/shard_map/ppermute | solution.py:149
  22.4 3.5 %collective-permute-start.7 = (bf16[512,256]{1,0:T(8,128)(2,1)S(1)}, bf16[512,256]{1,0:T(8,128)(2,1)S(1)}, u32[]{:S(2)}, u32[]{:S(2)}) collective-permute-start(bf16[512,256]{1,0:T(8,128)(2,1)S(1)} %collective-permute-done.3.refs_10_), channel_id=1, source_target_pairs={{0,8},{4,12},{8,16},{12,20},{16,24},{20,28},{1,9},{5,13},{9,17},{1... | collective-permute-start | bytes 786440 | tf_op jit(solution)/shard_map/ppermute | solution.py:148
  25.9 2.1 collective-permute-start
  28.1 1.3 collective-permute-start.8
  29.4 2.7 collective-permute-start.5
  35.0 13.3 %collective-permute-done.5.refs_12_ = bf16[512,256]{1,0:T(8,128)(2,1)S(1)} collective-permute-done((bf16[512,256]{1,0:T(8,128)(2,1)S(1)}, bf16[512,256]{1,0:T(8,128)(2,1)S(1)}, u32[]{:S(2)}, u32[]{:S(2)}) %collective-permute-start.5) | collective-permute-done | bytes 262176 | tf_op jit(solution)/shard_map/ppermute | solution.py:149
  48.3 2.8 collective-permute-done.9.refs_16_
  56.0 6.6 %attention.1 = bf16[512,256]{1,0:T(8,128)(2,1)} custom-call(s32[6]{0:T(128)S(1)} %convert_element_type.65.refs_0_, s32[512]{0:T(512)S(1)} %copy-done.9, bf16[512,256]{1,0:T(8,128)(2,1)S(1)} %copy-done.4, f32[512,8]{1,0:T(8,128)S(1)} %copy.24.refs_3_, f32[1,256]{1,0:T(1,128)S(1)} %bitcast.42, bf16[544,256]{1,0:T(8,128)(2,1)S(1)} %concatenate.7.refs_5_, ...), custom_call_target="tpu_custom_call" | custom-call | tf_op jit(solution)/shard_map/attention/pallas_call | solution.py:174
  62.7 3.4 %all-to-all-start = ((bf16[4,128,256]{2,1,0:T(8,128)(2,1)}), bf16[4,128,256]{2,1,0:T(8,128)(2,1)S(1)}, u32[]{:S(2)}, u32[]{:S(2)}) async-start(bf16[4,128,256]{2,1,0:T(8,128)(2,1)} %bitcast.10), calls=%async_computation | async-start | bytes 524288 | tf_op jit(solution)/shard_map/all_to_all | solution.py:337
  66.1 6.0 %all-to-all-done = bf16[4,128,256]{2,1,0:T(8,128)(2,1)S(1)} async-done(((bf16[4,128,256]{2,1,0:T(8,128)(2,1)}), bf16[4,128,256]{2,1,0:T(8,128)(2,1)S(1)}, u32[]{:S(2)}, u32[]{:S(2)}) %all-to-all-start) | async-done | bytes 262176 | tf_op jit(solution)/shard_map/all_to_all | solution.py:337
  72.1 2.2 copy-done
  74.3 2.5 project.1
  76.8 35.8 %all_to_all.63 = bf16[8,32,2048]{2,1,0:T(8,128)(2,1)S(1)} all-to-all(bf16[8,32,2048]{2,1,0:T(8,128)(2,1)S(1)} %bitcast.40), channel_id=1, replica_groups=mesh['sp'=8,'tp'=4] {'sp'}, dimensions={0} | all-to-all | bytes 2097152 | tf_op jit(solution)/shard_map/all_to_all | solution.py:362
  112.7 3.7 %all-to-all-start.1 = ((bf16[8,32,2048]{2,1,0:T(8,128)(2,1)}), bf16[8,32,2048]{2,1,0:T(8,128)(2,1)S(1)}, u32[]{:S(2)}, u32[]{:S(2)}) async-start(bf16[8,32,2048]{2,1,0:T(8,128)(2,1)} %bitcast.14), calls=%async_computation.1 | async-start | bytes 2097152 | tf_op jit(solution)/shard_map/all_to_all | solution.py:362
  117.2 24.6 %all-to-all-done.1 = bf16[8,32,2048]{2,1,0:T(8,128)(2,1)S(1)} async-done(((bf16[8,32,2048]{2,1,0:T(8,128)(2,1)}), bf16[8,32,2048]{2,1,0:T(8,128)(2,1)S(1)}, u32[]{:S(2)}, u32[]{:S(2)}) %all-to-all-start.1) | async-done | bytes 1048608 | tf_op jit(solution)/shard_map/all_to_all | solution.py:362
  143.1 22.0 %collective-permute-done.10.refs_1_ = bf16[256,2048]{1,0:T(8,128)(2,1)S(1)} collective-permute-done((bf16[256,2048]{1,0:T(8,128)(2,1)S(1)}, bf16[256,2048]{1,0:T(8,128)(2,1)S(1)}, u32[]{:S(2)}, u32[]{:S(2)}) %collective-permute-start.10) | collective-permute-done | bytes 1048608 | tf_op jit(solution)/shard_map/ppermute | solution.py:190
  165.2 2.0 copy-done.11
  167.2 15.5 %expert.3 = (bf16[512,2048]{1,0:T(8,128)(2,1)S(1)}, bf16[512,2048]{1,0:T(8,128)(2,1)S(1)}) custom-call(bf16[256,2048]{1,0:T(8,128)(2,1)S(1)} %bitcast.39, bf16[256,2048]{1,0:T(8,128)(2,1)S(1)} %collective-permute-done.15.refs_1_, bf16[256,2048]{1,0:T(8,128)(2,1)S(1)} %collective-permute-done.16.refs_2_, ...), custom_call_target="tpu_custom_call" | custom-call | flops 11274289152 | bytes 19398656 | tf_op jit(solution)/shard_map/expert/pallas_call | solution.py:372
  183.3 16.7 %expert.2 = (bf16[512,2048]{1,0:T(8,128)(2,1)S(1)}, bf16[512,2048]{1,0:T(8,128)(2,1)}) custom-call(bf16[256,2048]{1,0:T(8,128)(2,1)S(1)} %bitcast.36, bf16[256,2048]{1,0:T(8,128)(2,1)S(1)} %collective-permute-done.10.refs_1_, bf16[256,2048]{1,0:T(8,128)(2,1)S(1)} %collective-permute-done.11.refs_2_, bf16[256,2048]{1,0:T(8,128)(2,1)S(1)} %collective-permute-done.12.refs_3_, ...), custom_call_target="tpu_custom_call" | custom-call | flops 11274289152 | bytes 19398656 | tf_op jit(solution)/shard_map/expert/pallas_call | solution.py:372
  201.4 24.8 %collective-permute-done.19 = bf16[256,2048]{1,0:T(8,128)(2,1)S(1)} collective-permute-done((bf16[256,2048]{1,0:T(8,128)(2,1)S(1)}, bf16[256,2048]{1,0:T(8,128)(2,1)S(1)}, u32[]{:S(2)}, u32[]{:S(2)}) %collective-permute-start.19) | collective-permute-done | bytes 1048608 | tf_op jit(solution)/shard_map/ppermute | solution.py:190
  226.1 1.6 add_convert_fusion
  227.7 5.1 %all-to-all-start.4 = ((bf16[8,32,2048]{2,1,0:T(8,128)(2,1)}), bf16[8,32,2048]{2,1,0:T(8,128)(2,1)S(1)}, u32[]{:S(2)}, u32[]{:S(2)}) async-start(bf16[8,32,2048]{2,1,0:T(8,128)(2,1)} %bitcast.45), calls=%async_computation.4 | async-start | bytes 2097152 | tf_op jit(solution)/shard_map/all_to_all | solution.py:407
  232.8 1.6 add_convert_fusion.3
  235.3 23.6 %collective-permute-done.14 = bf16[256,2048]{1,0:T(8,128)(2,1)S(1)} collective-permute-done((bf16[256,2048]{1,0:T(8,128)(2,1)S(1)}, bf16[256,2048]{1,0:T(8,128)(2,1)S(1)}, u32[]{:S(2)}, u32[]{:S(2)}) %collective-permute-start.14) | collective-permute-done | bytes 1048608 | tf_op jit(solution)/shard_map/ppermute | solution.py:190
  258.9 2.7 add_convert_fusion.2
  261.6 5.9 %all-to-all-start.2 = ((bf16[8,32,2048]{2,1,0:T(8,128)(2,1)}), bf16[8,32,2048]{2,1,0:T(8,128)(2,1)S(1)}, u32[]{:S(2)}, u32[]{:S(2)}) async-start(bf16[8,32,2048]{2,1,0:T(8,128)(2,1)} %bitcast.46), calls=%async_computation.2 | async-start | bytes 2097152 | tf_op jit(solution)/shard_map/all_to_all | solution.py:407
  267.7 24.1 %all-to-all-done.2 = bf16[8,32,2048]{2,1,0:T(8,128)(2,1)S(1)} async-done(((bf16[8,32,2048]{2,1,0:T(8,128)(2,1)}), bf16[8,32,2048]{2,1,0:T(8,128)(2,1)S(1)}, u32[]{:S(2)}, u32[]{:S(2)}) %all-to-all-start.2) | async-done | bytes 1048608 | tf_op jit(solution)/shard_map/all_to_all | solution.py:407
  291.8 2.0 combine.1
  (74 shorter events, 15.5 us)
Async XLA Ops:
  2.5 12.0 %collective-permute-start.2 = (bf16[544,256]{1,0:T(8,128)(2,1)S(1)}, bf16[544,256]{1,0:T(8,128)(2,1)S(1)}, u32[]{:S(2)}, u32[]{:S(2)}) collective-permute-start(bf16[544,256]{1,0:T(8,128)(2,1)S(1)} %concatenate.7.refs_5_), channel_id=1, source_target_pairs={{0,8},{4,12},{8,16},{12,20},{16,24},{20,28},{1,9},{5,13},{9,17},{1... | collective-permute-start | bytes 835592 | tf_op jit(solution)/shard_map/ppermute | solution.py:148
  7.5 14.9 %collective-permute-start.3 = (bf16[512,256]{1,0:T(8,128)(2,1)}, bf16[512,256]{1,0:T(8,128)(2,1)S(1)}, u32[]{:S(2)}, u32[]{:S(2)}) collective-permute-start(bf16[512,256]{1,0:T(8,128)(2,1)} %refs_6_.1), channel_id=1, source_target_pairs={{0,8},{4,12},{8,16},{12,20},{16,24},{20,28},{1,9},{5,13},{9,17},{1... | collective-permute-start | bytes 786440 | tf_op jit(solution)/shard_map/ppermute | solution.py:148
  14.5 13.5 %collective-permute-start.6 = (bf16[544,256]{1,0:T(8,128)(2,1)S(1)}, bf16[544,256]{1,0:T(8,128)(2,1)S(1)}, u32[]{:S(2)}, u32[]{:S(2)}) collective-permute-start(bf16[544,256]{1,0:T(8,128)(2,1)S(1)} %collective-permute-done.2.refs_9_), channel_id=1, source_target_pairs={{0,8},{4,12},{8,16},{12,20},{16,24},{20,28},{1,9},{5,13},{9,17},{1... | collective-permute-start | bytes 835592 | tf_op jit(solution)/shard_map/ppermute | solution.py:148
  18.9 10.5 %collective-permute-start.1 = (bf16[512,256]{1,0:T(8,128)(2,1)}, bf16[512,256]{1,0:T(8,128)(2,1)S(1)}, u32[]{:S(2)}, u32[]{:S(2)}) collective-permute-start(bf16[512,256]{1,0:T(8,128)(2,1)} %refs_6_.1), channel_id=1, source_target_pairs={{0,4},{8,12},{16,20},{24,28},{1,5},{9,13},{17,21},{25,29},{2,6},{1... | collective-permute-start | bytes 786440 | tf_op jit(solution)/shard_map/ppermute | solution.py:149
  22.4 9.7 %collective-permute-start.7 = (bf16[512,256]{1,0:T(8,128)(2,1)S(1)}, bf16[512,256]{1,0:T(8,128)(2,1)S(1)}, u32[]{:S(2)}, u32[]{:S(2)}) collective-permute-start(bf16[512,256]{1,0:T(8,128)(2,1)S(1)} %collective-permute-done.3.refs_10_), channel_id=1, source_target_pairs={{0,8},{4,12},{8,16},{12,20},{16,24},{20,28},{1,9},{5,13},{9,17},{1... | collective-permute-start | bytes 786440 | tf_op jit(solution)/shard_map/ppermute | solution.py:148
  25.9 9.1 %collective-permute-start = (bf16[544,256]{1,0:T(8,128)(2,1)S(1)}, bf16[544,256]{1,0:T(8,128)(2,1)S(1)}, u32[]{:S(2)}, u32[]{:S(2)}) collective-permute-start(bf16[544,256]{1,0:T(8,128)(2,1)S(1)} %concatenate.7.refs_5_), channel_id=1, source_target_pairs={{0,4},{8,12},{16,20},{24,28},{1,5},{9,13},{17,21},{25,29},{2,6},{1... | collective-permute-start | bytes 835592 | tf_op jit(solution)/shard_map/ppermute | solution.py:149
  28.0 20.3 %collective-permute-start.4 = (bf16[544,256]{1,0:T(8,128)(2,1)S(1)}, bf16[544,256]{1,0:T(8,128)(2,1)S(1)}, u32[]{:S(2)}, u32[]{:S(2)}) collective-permute-start(bf16[544,256]{1,0:T(8,128)(2,1)S(1)} %collective-permute-done.2.refs_9_), channel_id=1, source_target_pairs={{0,4},{8,12},{16,20},{24,28},{4,0},{12,8},{20,16},{28,24},{1,5},{9... | collective-permute-start | bytes 835592 | tf_op jit(solution)/shard_map/ppermute | solution.py:149
  28.1 23.7 %collective-permute-start.8 = (bf16[544,256]{1,0:T(8,128)(2,1)S(1)}, bf16[544,256]{1,0:T(8,128)(2,1)S(1)}, u32[]{:S(2)}, u32[]{:S(2)}) collective-permute-start(bf16[544,256]{1,0:T(8,128)(2,1)S(1)} %collective-permute-done.6.refs_13_), channel_id=1, source_target_pairs={{4,0},{12,8},{20,16},{28,24},{5,1},{13,9},{21,17},{29,25},{6,2},{1... | collective-permute-start | bytes 835592 | tf_op jit(solution)/shard_map/ppermute | solution.py:149
  29.4 18.9 %collective-permute-start.5 = (bf16[512,256]{1,0:T(8,128)(2,1)S(1)}, bf16[512,256]{1,0:T(8,128)(2,1)S(1)}, u32[]{:S(2)}, u32[]{:S(2)}) collective-permute-start(bf16[512,256]{1,0:T(8,128)(2,1)S(1)} %collective-permute-done.3.refs_10_), channel_id=1, source_target_pairs={{0,4},{8,12},{16,20},{24,28},{4,0},{12,8},{20,16},{28,24},{1,5},{9... | collective-permute-start | bytes 786440 | tf_op jit(solution)/shard_map/ppermute | solution.py:149
  32.1 19.0 %collective-permute-start.9 = (bf16[512,256]{1,0:T(8,128)(2,1)S(1)}, bf16[512,256]{1,0:T(8,128)(2,1)S(1)}, u32[]{:S(2)}, u32[]{:S(2)}) collective-permute-start(bf16[512,256]{1,0:T(8,128)(2,1)S(1)} %collective-permute-done.7.refs_14_), channel_id=1, source_target_pairs={{4,0},{12,8},{20,16},{28,24},{5,1},{13,9},{21,17},{29,25},{6,2},{1... | collective-permute-start | bytes 786440 | tf_op jit(solution)/shard_map/ppermute | solution.py:149
  56.0 10.1 %copy-start.13 = (s32[128,2]{0,1:T(2,128)S(1)}, s32[128,2]{0,1:T(2,128)}, u32[]{:S(2)}) copy-start(s32[128,2]{0,1:T(2,128)} %param.23) | copy-start | bytes 3076
  56.0 16.1 %copy-start.3 = (bf16[128,2048]{1,0:T(8,128)(2,1)S(1)}, bf16[128,2048]{1,0:T(8,128)(2,1)}, u32[]{:S(2)}) copy-start(bf16[128,2048]{1,0:T(8,128)(2,1)} %refs_2_.4) | copy-start | bytes 1572868
  56.0 16.1 %copy-start.8 = (f32[2048]{0:T(1024)S(1)}, f32[2048]{0:T(1024)}, u32[]{:S(2)}) copy-start(f32[2048]{0:T(1024)} %param.22) | copy-start | bytes 24580
  62.7 9.4 %all-to-all-start = ((bf16[4,128,256]{2,1,0:T(8,128)(2,1)}), bf16[4,128,256]{2,1,0:T(8,128)(2,1)S(1)}, u32[]{:S(2)}, u32[]{:S(2)}) async-start(bf16[4,128,256]{2,1,0:T(8,128)(2,1)} %bitcast.10), calls=%async_computation | async-start | bytes 524288 | tf_op jit(solution)/shard_map/all_to_all | solution.py:337
  72.1 2.2 copy-start
  76.8 35.9 %copy-start.1 = (bf16[128,2048]{1,0:T(8,128)(2,1)}, bf16[128,2048]{1,0:T(8,128)(2,1)S(1)}, u32[]{:S(2)}) copy-start(bf16[128,2048]{1,0:T(8,128)(2,1)S(1)} %get-tuple-element.12.refs_0_) | copy-start | bytes 1572868
  112.7 29.1 %all-to-all-start.1 = ((bf16[8,32,2048]{2,1,0:T(8,128)(2,1)}), bf16[8,32,2048]{2,1,0:T(8,128)(2,1)S(1)}, u32[]{:S(2)}, u32[]{:S(2)}) async-start(bf16[8,32,2048]{2,1,0:T(8,128)(2,1)} %bitcast.14), calls=%async_computation.1 | async-start | bytes 2097152 | tf_op jit(solution)/shard_map/all_to_all | solution.py:362
  116.4 26.2 %collective-permute-start.15 = (bf16[256,2048]{1,0:T(8,128)(2,1)S(1)}, bf16[256,2048]{1,0:T(8,128)(2,1)S(1)}, u32[]{:S(2)}, u32[]{:S(2)}) collective-permute-start(bf16[256,2048]{1,0:T(8,128)(2,1)S(1)} %bitcast.37), channel_id=1, source_target_pairs={{0,2},{1,3},{2,0},{3,1},{4,6},{5,7},{6,4},{7,5},{8,10},{9,11},{10,... | collective-permute-start | bytes 3145736 | tf_op jit(solution)/shard_map/ppermute | solution.py:190
  141.8 23.3 %collective-permute-start.10 = (bf16[256,2048]{1,0:T(8,128)(2,1)S(1)}, bf16[256,2048]{1,0:T(8,128)(2,1)S(1)}, u32[]{:S(2)}, u32[]{:S(2)}) collective-permute-start(bf16[256,2048]{1,0:T(8,128)(2,1)S(1)} %bitcast.34), channel_id=1, source_target_pairs={{0,2},{1,3},{2,0},{3,1},{4,6},{5,7},{6,4},{7,5},{8,10},{9,11},{10,... | collective-permute-start | bytes 3145736 | tf_op jit(solution)/shard_map/ppermute | solution.py:190
  142.6 22.6 %collective-permute-start.16 = (bf16[256,2048]{1,0:T(8,128)(2,1)S(1)}, bf16[256,2048]{1,0:T(8,128)(2,1)S(1)}, u32[]{:S(2)}, u32[]{:S(2)}) collective-permute-start(bf16[256,2048]{1,0:T(8,128)(2,1)S(1)} %bitcast.38), channel_id=1, source_target_pairs={{0,1},{1,0},{2,3},{3,2},{4,5},{5,4},{6,7},{7,6},{8,9},{9,8},{10,11... | collective-permute-start | bytes 3145736 | tf_op jit(solution)/shard_map/ppermute | solution.py:190
  142.6 22.6 %collective-permute-start.17 = (bf16[256,2048]{1,0:T(8,128)(2,1)S(1)}, bf16[256,2048]{1,0:T(8,128)(2,1)S(1)}, u32[]{:S(2)}, u32[]{:S(2)}) collective-permute-start(bf16[256,2048]{1,0:T(8,128)(2,1)S(1)} %collective-permute-done.15.refs_1_), channel_id=1, source_target_pairs={{0,1},{1,0},{2,3},{3,2},{4,5},{5,4},{6,7},{7,6},{8,9},{9,8},{10,11... | collective-permute-start | bytes 3145736 | tf_op jit(solution)/shard_map/ppermute | solution.py:190
  143.1 40.2 %collective-permute-start.11 = (bf16[256,2048]{1,0:T(8,128)(2,1)S(1)}, bf16[256,2048]{1,0:T(8,128)(2,1)S(1)}, u32[]{:S(2)}, u32[]{:S(2)}) collective-permute-start(bf16[256,2048]{1,0:T(8,128)(2,1)S(1)} %bitcast.35), channel_id=1, source_target_pairs={{0,1},{1,0},{2,3},{3,2},{4,5},{5,4},{6,7},{7,6},{8,9},{9,8},{10,11... | collective-permute-start | bytes 3145736 | tf_op jit(solution)/shard_map/ppermute | solution.py:190
  165.2 18.1 %collective-permute-start.12 = (bf16[256,2048]{1,0:T(8,128)(2,1)S(1)}, bf16[256,2048]{1,0:T(8,128)(2,1)S(1)}, u32[]{:S(2)}, u32[]{:S(2)}) collective-permute-start(bf16[256,2048]{1,0:T(8,128)(2,1)S(1)} %collective-permute-done.10.refs_1_), channel_id=1, source_target_pairs={{0,1},{1,0},{2,3},{3,2},{4,5},{5,4},{6,7},{7,6},{8,9},{9,8},{10,11... | collective-permute-start | bytes 3145736 | tf_op jit(solution)/shard_map/ppermute | solution.py:190
  167.2 16.1 %copy-start.12 = (bf16[1,2048,896]{2,1,0:T(8,128)(2,1)S(1)}, bf16[1,2048,896]{2,1,0:T(8,128)(2,1)}, u32[]{:S(2)}) copy-start(bf16[1,2048,896]{2,1,0:T(8,128)(2,1)} %param.25) | copy-start | bytes 11010052
  182.7 17.4 %collective-permute-start.18 = (bf16[512,2048]{1,0:T(8,128)(2,1)S(1)}, bf16[512,2048]{1,0:T(8,128)(2,1)S(1)}, u32[]{:S(2)}, u32[]{:S(2)}) collective-permute-start(bf16[512,2048]{1,0:T(8,128)(2,1)S(1)} %get-tuple-element.18), channel_id=1, source_target_pairs={{0,1},{1,0},{2,3},{3,2},{4,5},{5,4},{6,7},{7,6},{8,9},{9,8},{10,11... | collective-permute-start | bytes 6291464 | tf_op jit(solution)/shard_map/ppermute | solution.py:190
  200.0 32.8 %collective-permute-start.13 = (bf16[512,2048]{1,0:T(8,128)(2,1)}, bf16[512,2048]{1,0:T(8,128)(2,1)}, u32[]{:S(2)}, u32[]{:S(2)}) collective-permute-start(bf16[512,2048]{1,0:T(8,128)(2,1)} %get-tuple-element.15), channel_id=1, source_target_pairs={{0,1},{1,0},{2,3},{3,2},{4,5},{5,4},{6,7},{7,6},{8,9},{9,8},{10,11... | collective-permute-start | bytes 6291464 | tf_op jit(solution)/shard_map/ppermute | solution.py:190
  200.5 25.6 %collective-permute-start.19 = (bf16[256,2048]{1,0:T(8,128)(2,1)S(1)}, bf16[256,2048]{1,0:T(8,128)(2,1)S(1)}, u32[]{:S(2)}, u32[]{:S(2)}) collective-permute-start(bf16[256,2048]{1,0:T(8,128)(2,1)S(1)} %add_convert_fusion.1), channel_id=1, source_target_pairs={{0,2},{1,3},{2,0},{3,1},{4,6},{5,7},{6,4},{7,5},{8,10},{9,11},{10,... | collective-permute-start | bytes 3145736 | tf_op jit(solution)/shard_map/ppermute | solution.py:190
  227.7 33.9 %all-to-all-start.4 = ((bf16[8,32,2048]{2,1,0:T(8,128)(2,1)}), bf16[8,32,2048]{2,1,0:T(8,128)(2,1)S(1)}, u32[]{:S(2)}, u32[]{:S(2)}) async-start(bf16[8,32,2048]{2,1,0:T(8,128)(2,1)} %bitcast.45), calls=%async_computation.4 | async-start | bytes 2097152 | tf_op jit(solution)/shard_map/all_to_all | solution.py:407
  234.4 24.5 %collective-permute-start.14 = (bf16[256,2048]{1,0:T(8,128)(2,1)S(1)}, bf16[256,2048]{1,0:T(8,128)(2,1)S(1)}, u32[]{:S(2)}, u32[]{:S(2)}) collective-permute-start(bf16[256,2048]{1,0:T(8,128)(2,1)S(1)} %add_convert_fusion.3), channel_id=1, source_target_pairs={{0,2},{1,3},{2,0},{3,1},{4,6},{5,7},{6,4},{7,5},{8,10},{9,11},{10,... | collective-permute-start | bytes 3145736 | tf_op jit(solution)/shard_map/ppermute | solution.py:190
  261.6 6.0 %copy-start.14 = (f32[128,2]{0,1:T(2,128)S(1)}, f32[128,2]{0,1:T(2,128)}, u32[]{:S(2)}) copy-start(f32[128,2]{0,1:T(2,128)} %param.24) | copy-start | bytes 3076
  261.6 30.2 %copy-start.2 = (bf16[128,2048]{1,0:T(8,128)(2,1)S(1)}, bf16[128,2048]{1,0:T(8,128)(2,1)}, u32[]{:S(2)}) copy-start(bf16[128,2048]{1,0:T(8,128)(2,1)} %copy-done.1) | copy-start | bytes 1572868
  261.6 30.2 %all-to-all-start.2 = ((bf16[8,32,2048]{2,1,0:T(8,128)(2,1)}), bf16[8,32,2048]{2,1,0:T(8,128)(2,1)S(1)}, u32[]{:S(2)}, u32[]{:S(2)}) async-start(bf16[8,32,2048]{2,1,0:T(8,128)(2,1)} %bitcast.46), calls=%async_computation.2 | async-start | bytes 2097152 | tf_op jit(solution)/shard_map/all_to_all | solution.py:407
  (7 other events, 7.0 us)

commit v4 on v3

--- a/solution.py
+++ b/solution.py
@@ -18,10 +18,16 @@
     return [part.astype(jnp.bfloat16) for part in (hi, mid, low)]
 
 
-def attention_kernel(tokens, heads, head_size, tile, sources, *refs):
+def attention_kernel(tokens, heads, head_size, tile, sources, first, last, *refs):
     valid_ref, docs_ref, q_ref, meta_ref, gain_ref = refs[:5]
     kv_refs = refs[5 : 5 + 2 * sources]
-    out_ref, m_ref, l_ref, acc_ref = refs[5 + 2 * sources :]
+    rest = refs[5 + 2 * sources :]
+    if not first:
+        m_in, l_in, acc_in, *rest = rest
+    if last:
+        out_ref, m_ref, l_ref, acc_ref = rest
+    else:
+        m_out, l_out, acc_out, m_ref, l_ref, acc_ref = rest
     width = heads * head_size
     halves = tokens // width
     rows = tokens // head_size
@@ -43,6 +49,7 @@
         first_doc = docs_ref[row0].astype(jnp.float32)
 
         def visit(source):
+            fresh = first and source == 0
             k_ref, v_ref = kv_refs[2 * source], kv_refs[2 * source + 1]
             k = k_ref[:tokens, :]
             v = v_ref[...]
@@ -51,7 +58,7 @@
             doc_rows = extra[3 * rows : 3 * rows + halves]
             k_doc = jnp.concatenate([doc_rows[j : j + 1] for j in range(halves)], axis=1)
             allowed = k_doc == q_doc
-            if source == 0:
+            if fresh:
                 q_pos = row0 + lax.broadcasted_iota(jnp.int32, (tile, tokens), 0)
                 k_pos = lax.broadcasted_iota(jnp.int32, (tile, tokens), 1)
                 allowed = allowed & (k_pos <= q_pos)
@@ -68,7 +75,7 @@
                 s = s * score_scale + (meta[:, h : h + 1] * LOG2E - gate_row)
                 s = jnp.where(allowed, s, NEG)
                 block_max = jnp.max(s, axis=1, keepdims=True)
-                if source == 0:
+                if fresh:
                     new_max = block_max
                 else:
                     old_max = m_ref[h]
@@ -78,18 +85,24 @@
                 p = jnp.exp2(s - new_max)
                 block_sum = jnp.sum(p, axis=1, keepdims=True)
                 m_ref[h] = new_max
-                l_ref[h] = block_sum if source == 0 else l_ref[h] * rescale + block_sum
+                l_ref[h] = block_sum if fresh else l_ref[h] * rescale + block_sum
                 v_h = jnp.where(in_head[h], v, jnp.zeros((), v.dtype))
                 total = total + jnp.dot(
                     p.astype(jnp.bfloat16), v_h, preferred_element_type=jnp.float32
                 )
-            if source == 0:
+            if fresh:
                 acc_ref[...] = total
             else:
                 acc_ref[...] = acc_ref[...] * spread(rescales) + total
 
-        visit(0)
-        for source in range(1, sources):
+        if first:
+            visit(0)
+        else:
+            for h in range(heads):
+                m_ref[h] = m_in[pl.ds(row0, tile), h : h + 1]
+                l_ref[h] = l_in[pl.ds(row0, tile), h : h + 1]
+            acc_ref[...] = acc_in[pl.ds(row0, tile), :]
+        for source in range(1 if first else 0, sources):
             last_doc = jnp.max(
                 kv_refs[2 * source][tokens + 3 * rows : tokens + 3 * rows + halves, :].astype(
                     jnp.float32
@@ -99,6 +112,13 @@
             @pl.when((valid_ref[source] > 0) & (last_doc >= first_doc))
             def _():
                 visit(source)
+
+        if not last:
+            for h in range(heads):
+                m_out[pl.ds(row0, tile), h : h + 1] = m_ref[h]
+                l_out[pl.ds(row0, tile), h : h + 1] = l_ref[h]
+            acc_out[pl.ds(row0, tile), :] = acc_ref[...]
+            return carry
 
         attended = acc_ref[...] / spread([l_ref[h] for h in range(heads)])
         squares = attended * attended
@@ -163,39 +183,51 @@
         elif step == reach:
             exists = exists & (member == 0)
         valid.append(exists)
-    sources = len(valid)
-    valid = jnp.stack(valid).astype(jnp.int32)
-
-    def kernel(*refs):
-        attention_kernel(tokens, heads, head_size, tile, sources, *refs)
-
     vmem = pl.BlockSpec(memory_space=pltpu.VMEM)
     smem = pl.BlockSpec(memory_space=pltpu.SMEM)
-    return pl.pallas_call(
-        kernel,
-        out_shape=jax.ShapeDtypeStruct((tokens, width), jnp.bfloat16),
-        in_specs=[smem, smem] + [vmem] * (3 + len(blocks)),
-        out_specs=vmem,
-        scratch_shapes=[
-            pltpu.VMEM((heads, tile, 1), jnp.float32),
-            pltpu.VMEM((heads, tile, 1), jnp.float32),
-            pltpu.VMEM((tile, width), jnp.float32),
-        ],
-        compiler_params=pltpu.CompilerParams(vmem_limit_bytes=50 * 2**20),
-        name="attention",
-    )(valid, documents, queries, meta, head_gain[None, :], *blocks)
+    state = [
+        jax.ShapeDtypeStruct((tokens, heads), jnp.float32),
+        jax.ShapeDtypeStruct((tokens, heads), jnp.float32),
+        jax.ShapeDtypeStruct((tokens, width), jnp.float32),
+    ]
+
+    def run(places, carried, first, last):
+        flags = jnp.stack([valid[i] for i in places]).astype(jnp.int32)
+        pieces = [x for i in places for x in blocks[2 * i : 2 * i + 2]]
+
+        def kernel(*refs):
+            attention_kernel(tokens, heads, head_size, tile, len(places), first, last, *refs)
+
+        return pl.pallas_call(
+            kernel,
+            out_shape=[jax.ShapeDtypeStruct((tokens, width), jnp.bfloat16)] if last else state,
+            in_specs=[smem, smem] + [vmem] * (3 + len(pieces) + len(carried)),
+            out_specs=[vmem] if last else [vmem] * 3,
+            scratch_shapes=[
+                pltpu.VMEM((heads, tile, 1), jnp.float32),
+                pltpu.VMEM((heads, tile, 1), jnp.float32),
+                pltpu.VMEM((tile, width), jnp.float32),
+            ],
+            compiler_params=pltpu.CompilerParams(vmem_limit_bytes=40 * 2**20),
+            name="attention",
+        )(flags, documents, queries, meta, head_gain[None, :], *pieces, *carried)
+
+    early, late = list(range(len(valid) - 1)), [len(valid) - 1]
+    carried = run(early, [], True, False)
+    return run(late, carried, False, True)[0]
 
 
 def swap(x, axis, bits):
     return lax.ppermute(x, axis, [(i, i ^ bits) for i in range(lax.axis_size(axis))])
 
 
-CHUNKS = 2
-
-
-def project_kernel(experts, capacity, x_ref, weight_ref, resid_ref, routes_ref, gain_ref, *refs):
-    outs = refs[:CHUNKS]
-    stream_ref, wide_ref, pick_ref = refs[CHUNKS:]
+def chunk_count(n_sp):
+    return 4 if n_sp <= 8 else 2
+
+
+def project_kernel(chunks, experts, capacity, x_ref, weight_ref, resid_ref, routes_ref, gain_ref, *refs):
+    outs = refs[:chunks]
+    stream_ref, wide_ref, pick_ref = refs[chunks:]
     rows, width = resid_ref.shape
     n_tile = 512
     total = jnp.zeros((rows, 1), jnp.float32)
@@ -219,8 +251,8 @@
         chosen = chosen + (routes_ref[route : route + 1, :] == expert_ids).astype(jnp.float32)
     ranks = jnp.dot(chosen.astype(jnp.bfloat16), before, preferred_element_type=jnp.float32)
     slots = jnp.where(chosen > 0.0, ranks, -1.0)
-    span = capacity // CHUNKS
-    for c in range(CHUNKS):
+    span = capacity // chunks
+    for c in range(chunks):
         slot_ids = lax.broadcasted_iota(jnp.int32, (span, rows), 0) + c * span
         for e in range(experts):
             pick = (slot_ids.astype(jnp.float32) == slots[e : e + 1, :]).astype(jnp.float32)
@@ -232,7 +264,7 @@
         cols = slice(n * n_tile, (n + 1) * n_tile)
         normed = (wide_ref[:, cols] * scale * gain_ref[:, cols]).astype(jnp.bfloat16)
         picked = jnp.dot(picks, normed, preferred_element_type=jnp.float32).astype(jnp.bfloat16)
-        for c in range(CHUNKS):
+        for c in range(chunks):
             outs[c][:, cols] = picked[c * each : (c + 1) * each]
 
 
@@ -272,13 +304,13 @@
             other_ref[:, cols] = out[mine_rows:]
 
 
-def combine_kernel(experts, stream_ref, routes_ref, weights_ref, *refs):
-    outs = refs[:CHUNKS]
-    mixed_ref, stack_ref = refs[CHUNKS:]
+def combine_kernel(chunks, experts, stream_ref, routes_ref, weights_ref, *refs):
+    outs = refs[:chunks]
+    mixed_ref, stack_ref = refs[chunks:]
     rows, width = stream_ref.shape
     each = outs[0].shape[0]
     span = each // experts
-    for c in range(CHUNKS):
+    for c in range(chunks):
         stack_ref[c * each : (c + 1) * each, :] = outs[c][...]
     expert_ids = lax.broadcasted_iota(jnp.int32, (rows, experts), 1)
     named = [
@@ -291,7 +323,7 @@
     ranks = jnp.dot(
         before, (named[0] + named[1]).astype(jnp.bfloat16), preferred_element_type=jnp.float32
     )
-    slot_ids = lax.broadcasted_iota(jnp.int32, (rows, CHUNKS * each), 1)
+    slot_ids = lax.broadcasted_iota(jnp.int32, (rows, chunks * each), 1)
     picks = []
     for route in range(2):
         rank = jnp.sum(named[route] * ranks, axis=1, keepdims=True).astype(jnp.int32)
@@ -329,7 +361,8 @@
     blocks = n_tp // 2
     local_rows, model_width = resid.shape
     capacity = 2 * routes.shape[1] * tokens // (n_tp * n_sp)
-    span = capacity // CHUNKS
+    chunks = chunk_count(n_sp)
+    span = capacity // chunks
     vmem = pl.BlockSpec(memory_space=pltpu.VMEM)
     route_rows = routes.T.astype(jnp.float32)
 
@@ -337,14 +370,14 @@
     regrouped = lax.all_to_all(head_normed, "tp", split_axis=0, concat_axis=1, tiled=True)
 
     def project(*refs):
-        project_kernel(n_sp, capacity, *refs)
+        project_kernel(chunks, n_sp, capacity, *refs)
 
     *outbound, stream = pl.pallas_call(
         project,
-        out_shape=[jax.ShapeDtypeStruct((n_sp * span, model_width), jnp.bfloat16)] * CHUNKS
+        out_shape=[jax.ShapeDtypeStruct((n_sp * span, model_width), jnp.bfloat16)] * chunks
         + [jax.ShapeDtypeStruct((local_rows, model_width), jnp.bfloat16)],
         in_specs=[vmem] * 5,
-        out_specs=[vmem] * (CHUNKS + 1),
+        out_specs=[vmem] * (chunks + 1),
         scratch_shapes=[
             pltpu.VMEM((local_rows, model_width), jnp.float32),
             pltpu.VMEM((n_sp * capacity, local_rows), jnp.float32),
@@ -358,11 +391,11 @@
     each = n_sp * span
     rows = n_tp * each
     arrived, crossed = [], []
-    for c in range(CHUNKS):
+    for c in range(chunks):
         arrived.append(lax.all_to_all(outbound[c], "sp", 0, 0, tiled=True))
         crossed.append([swap(arrived[c], "tp", 2 * j) for j in range(1, blocks)])
     returned = []
-    for c in range(CHUNKS):
+    for c in range(chunks):
         inputs = [arrived[c], *crossed[c]]
         inputs += [swap(x, "tp", 1) for x in inputs]
 
@@ -408,12 +441,12 @@
         )
 
     def combine(*refs):
-        combine_kernel(n_sp, *refs)
+        combine_kernel(chunks, n_sp, *refs)
 
     return pl.pallas_call(
         combine,
         out_shape=jax.ShapeDtypeStruct((local_rows, model_width), jnp.bfloat16),
-        in_specs=[vmem] * (3 + CHUNKS),
+        in_specs=[vmem] * (3 + chunks),
         out_specs=vmem,
         scratch_shapes=[pltpu.VMEM((n_sp * capacity, model_width), jnp.bfloat16)],
         compiler_params=pltpu.CompilerParams(vmem_limit_bytes=24 * 2**20),

time: 295 us -> 293 us (level)
  waiting for transfers between devices: 145 us -> 97.6 us
  starting transfers between devices: 49.8 us -> 64.6 us
  Pallas kernels: 43.4 us -> 54.3 us
  other arithmetic: 8.54 us -> 15.4 us
  blocking collectives: 35.8 us -> 42.3 us
  local copies, waits for them, and re-layouts: 10.8 us -> 16.7 us
    ppermute x10 -> x20, waiting for transfers between devices: 70.4 us -> 9.19 us  [swap(): lax.ppermute(x, axis, [(i, i ^ bits) for i in range(lax.axis_size(axis))])]
    all_to_all x2 -> x4, waiting for transfers between devices: 24.1 us -> 41.7 us  [on_device(): lax.all_to_all(result.astype(jnp.bfloat16), 'sp', 0, 0, tiled=True)]
    pallas_call x2 -> x4, Pallas kernels: 32.2 us -> 40.9 us  [on_device(): pl.pallas_call(expert, grid=(hidden_width // h_tile,), out_shape=[jax.Sha...]
    all_to_all x1 -> x2, blocking collectives: 35.8 us -> 42.3 us  [on_device(): arrived.append(lax.all_to_all(outbound[c], 'sp', 0, 0, tiled=True))]
    unnamed x32 -> x42, local copies, waits for them, and re-layouts: 9.38 us -> 15.3 us
    all_to_all x2 -> x4, starting transfers between devices: 11 us -> 16.8 us  [on_device(): lax.all_to_all(result.astype(jnp.bfloat16), 'sp', 0, 0, tiled=True)]
    ppermute x10 -> x20, starting transfers between devices: 4.45 us -> 9.82 us  [swap(): lax.ppermute(x, axis, [(i, i ^ bits) for i in range(lax.axis_size(axis))])]
    convert_element_type x2 -> x4, other arithmetic: 4.3 us -> 7.93 us  [on_device(): result.astype(jnp.bfloat16)]
  transfers between devices with their start and end apart: 24 -> 37, of which waited for: 10 -> 14; matrix products, arithmetic and copies ran while one was open for 3% -> 5% of each run, Pallas kernels for 11% -> 16%
where the time goes in v4:
time: 293 us; the launch traced here: 291 us
  waiting for transfers between devices  97.6 us (33%)
  starting transfers between devices  64.6 us (22%)
  Pallas kernels  54.3 us (19%)
  blocking collectives  42.3 us (14%)
  local copies, waits for them, and re-layouts  16.7 us (6%)
  other arithmetic  15.4 us (5%)
    all_to_all x2, blocking collectives, on_device(): arrived.append(lax.all_to_all(outbound[c], 'sp', 0, 0, tiled=True))  42.3 us
    all_to_all x4, waiting for transfers between devices, on_device(): lax.all_to_all(result.astype(jnp.bfloat16), 'sp', 0, 0, tiled=True)  41.7 us
    pallas_call x4, Pallas kernels, on_device(): pl.pallas_call(expert, grid=(hidden_width // h_tile,), out_shape=[jax.Sha...  40.9 us
    all_to_all x2, waiting for transfers between devices, on_device(): arrived.append(lax.all_to_all(outbound[c], 'sp', 0, 0, tiled=True))  23.3 us
    all_to_all x4, starting transfers between devices, on_device(): lax.all_to_all(result.astype(jnp.bfloat16), 'sp', 0, 0, tiled=True)  16.8 us
    ppermute x4, starting transfers between devices, chain(): own.append(lax.ppermute(own[-1], 'sp', ahead))  16.3 us
    unnamed x42, local copies, waits for them, and re-layouts  15.3 us
    ppermute x6, waiting for transfers between devices, chain(): other.append(lax.ppermute(own[-1], 'sp', pairs))  13.9 us
  transfers between devices with their start and end apart: 37, of which 14 were waited for; matrix products, arithmetic and copies ran while one was open for 5% of the time, Pallas kernels for 16%

profile of v4, /device:TPU:0, one launch (start us, length us, event | category | flops | bytes accessed | tf_op | source)
XLA Modules:
  0.0 291.3 jit_solution(11648652484810279960)
XLA Ops:
  2.7 5.0 %collective-permute-start = (bf16[544,256]{1,0:T(8,128)(2,1)S(1)}, bf16[544,256]{1,0:T(8,128)(2,1)S(1)}, u32[]{:S(2)}, u32[]{:S(2)}) collective-permute-start(bf16[544,256]{1,0:T(8,128)(2,1)S(1)} %concatenate.7.refs_5_), channel_id=1, source_target_pairs={{0,8},{4,12},{8,16},{12,20},{16,24},{20,28},{1,9},{5,13},{9,17},{1... | collective-permute-start | bytes 835592 | tf_op jit(solution)/shard_map/ppermute | solution.py:168
  7.6 3.5 %collective-permute-start.3 = (bf16[512,256]{1,0:T(8,128)(2,1)}, bf16[512,256]{1,0:T(8,128)(2,1)S(1)}, u32[]{:S(2)}, u32[]{:S(2)}) collective-permute-start(bf16[512,256]{1,0:T(8,128)(2,1)} %refs_6_.1), channel_id=1, source_target_pairs={{0,8},{4,12},{8,16},{12,20},{16,24},{20,28},{1,9},{5,13},{9,17},{1... | collective-permute-start | bytes 786440 | tf_op jit(solution)/shard_map/ppermute | solution.py:168
  11.1 3.5 %collective-permute-done.refs_9_ = bf16[544,256]{1,0:T(8,128)(2,1)S(1)} collective-permute-done((bf16[544,256]{1,0:T(8,128)(2,1)S(1)}, bf16[544,256]{1,0:T(8,128)(2,1)S(1)}, u32[]{:S(2)}, u32[]{:S(2)}) %collective-permute-start) | collective-permute-done | bytes 278560 | tf_op jit(solution)/shard_map/ppermute | solution.py:168
  14.6 4.4 %collective-permute-start.1 = (bf16[544,256]{1,0:T(8,128)(2,1)S(1)}, bf16[544,256]{1,0:T(8,128)(2,1)S(1)}, u32[]{:S(2)}, u32[]{:S(2)}) collective-permute-start(bf16[544,256]{1,0:T(8,128)(2,1)S(1)} %collective-permute-done.refs_9_), channel_id=1, source_target_pairs={{0,8},{4,12},{8,16},{12,20},{16,24},{20,28},{1,9},{5,13},{9,17},{1... | collective-permute-start | bytes 835592 | tf_op jit(solution)/shard_map/ppermute | solution.py:168
  19.0 3.4 %collective-permute-start.7 = (bf16[512,256]{1,0:T(8,128)(2,1)}, bf16[512,256]{1,0:T(8,128)(2,1)S(1)}, u32[]{:S(2)}, u32[]{:S(2)}) collective-permute-start(bf16[512,256]{1,0:T(8,128)(2,1)} %refs_6_.1), channel_id=1, source_target_pairs={{0,4},{8,12},{16,20},{24,28},{1,5},{9,13},{17,21},{25,29},{2,6},{1... | collective-permute-start | bytes 786440 | tf_op jit(solution)/shard_map/ppermute | solution.py:169
  22.5 3.5 %collective-permute-start.4 = (bf16[512,256]{1,0:T(8,128)(2,1)S(1)}, bf16[512,256]{1,0:T(8,128)(2,1)S(1)}, u32[]{:S(2)}, u32[]{:S(2)}) collective-permute-start(bf16[512,256]{1,0:T(8,128)(2,1)S(1)} %collective-permute-done.3.refs_10_), channel_id=1, source_target_pairs={{0,8},{4,12},{8,16},{12,20},{16,24},{20,28},{1,9},{5,13},{9,17},{1... | collective-permute-start | bytes 786440 | tf_op jit(solution)/shard_map/ppermute | solution.py:168
  29.5 2.7 collective-permute-start.9
  35.1 13.4 %collective-permute-done.9.refs_12_ = bf16[512,256]{1,0:T(8,128)(2,1)} collective-permute-done((bf16[512,256]{1,0:T(8,128)(2,1)S(1)}, bf16[512,256]{1,0:T(8,128)(2,1)}, u32[]{:S(2)}, u32[]{:S(2)}) %collective-permute-start.9) | collective-permute-done | bytes 262176 | tf_op jit(solution)/shard_map/ppermute | solution.py:169
  51.8 5.9 %attention.2 = (f32[512,4]{1,0:T(8,128)S(1)}, f32[512,4]{1,0:T(8,128)S(1)}, f32[512,256]{1,0:T(8,128)S(1)}) custom-call(s32[5]{0:T(128)S(1)} %convert_element_type.119.refs_0_, s32[512]{0:T(512)S(1)} %copy-done.8, bf16[512,256]{1,0:T(8,128)(2,1)S(1)} %copy-done.2, f32[512,8]{1,0:T(8,128)S(1)} %copy.25.refs_3_, f32[1,256]{1,0:T(1,128)S(1)} %bitcast.59, ...), custom_call_target="tpu_custom_call" | custom-call | tf_op jit(solution)/shard_map/attention/pallas_call | solution.py:201
  57.7 3.1 %attention.3 = bf16[512,256]{1,0:T(8,128)(2,1)} custom-call(s32[1]{0:T(128)} %bitcast.refs_0_, s32[512]{0:T(512)S(1)} %copy-done.8, bf16[512,256]{1,0:T(8,128)(2,1)S(1)} %copy-done.3, f32[512,8]{1,0:T(8,128)S(1)} %copy.25.refs_3_, f32[1,256]{1,0:T(1,128)S(1)} %bitcast.60, bf16[544,256]{1,0:T(8,128)(2,1)S(1)} %collective-permute-done.2.refs_5_, ...), custom_call_target="tpu_custom_call" | custom-call | tf_op jit(solution)/shard_map/attention/pallas_call | solution.py:201
  60.8 3.4 %all-to-all-start = ((bf16[4,128,256]{2,1,0:T(8,128)(2,1)}), bf16[4,128,256]{2,1,0:T(8,128)(2,1)S(1)}, u32[]{:S(2)}, u32[]{:S(2)}) async-start(bf16[4,128,256]{2,1,0:T(8,128)(2,1)} %bitcast.10), calls=%async_computation | async-start | bytes 524288 | tf_op jit(solution)/shard_map/all_to_all | solution.py:370
  64.2 6.0 %all-to-all-done = bf16[4,128,256]{2,1,0:T(8,128)(2,1)S(1)} async-done(((bf16[4,128,256]{2,1,0:T(8,128)(2,1)}), bf16[4,128,256]{2,1,0:T(8,128)(2,1)S(1)}, u32[]{:S(2)}, u32[]{:S(2)}) %all-to-all-start) | async-done | bytes 262176 | tf_op jit(solution)/shard_map/all_to_all | solution.py:370
  75.6 24.7 %all_to_all.107 = bf16[8,16,2048]{2,1,0:T(8,128)(2,1)S(1)} all-to-all(bf16[8,16,2048]{2,1,0:T(8,128)(2,1)S(1)} %bitcast.57), channel_id=1, replica_groups=mesh['sp'=8,'tp'=4] {'sp'}, dimensions={0} | all-to-all | bytes 1048576 | tf_op jit(solution)/shard_map/all_to_all | solution.py:395
  100.4 17.5 %all_to_all.108 = bf16[8,16,2048]{2,1,0:T(8,128)(2,1)S(1)} all-to-all(bf16[8,16,2048]{2,1,0:T(8,128)(2,1)S(1)} %bitcast.56), channel_id=1, replica_groups=mesh['sp'=8,'tp'=4] {'sp'}, dimensions={0} | all-to-all | bytes 1048576 | tf_op jit(solution)/shard_map/all_to_all | solution.py:395
  117.9 3.6 %all-to-all-start.3 = ((bf16[8,16,2048]{2,1,0:T(8,128)(2,1)}), bf16[8,16,2048]{2,1,0:T(8,128)(2,1)S(1)}, u32[]{:S(2)}, u32[]{:S(2)}) async-start(bf16[8,16,2048]{2,1,0:T(8,128)(2,1)} %bitcast.21), calls=%async_computation.3 | async-start | bytes 1048576 | tf_op jit(solution)/shard_map/all_to_all | solution.py:395
  122.3 13.3 %all-to-all-done.3 = bf16[8,16,2048]{2,1,0:T(8,128)(2,1)S(1)} async-done(((bf16[8,16,2048]{2,1,0:T(8,128)(2,1)}), bf16[8,16,2048]{2,1,0:T(8,128)(2,1)S(1)}, u32[]{:S(2)}, u32[]{:S(2)}) %all-to-all-start.3) | async-done | bytes 524320 | tf_op jit(solution)/shard_map/all_to_all | solution.py:395
  135.6 3.7 %all-to-all-start.1 = ((bf16[8,16,2048]{2,1,0:T(8,128)(2,1)}), bf16[8,16,2048]{2,1,0:T(8,128)(2,1)S(1)}, u32[]{:S(2)}, u32[]{:S(2)}) async-start(bf16[8,16,2048]{2,1,0:T(8,128)(2,1)} %bitcast.14), calls=%async_computation.1 | async-start | bytes 1048576 | tf_op jit(solution)/shard_map/all_to_all | solution.py:395
  143.6 10.0 %all-to-all-done.1 = bf16[8,16,2048]{2,1,0:T(8,128)(2,1)S(1)} async-done(((bf16[8,16,2048]{2,1,0:T(8,128)(2,1)}), bf16[8,16,2048]{2,1,0:T(8,128)(2,1)S(1)}, u32[]{:S(2)}, u32[]{:S(2)}) %all-to-all-start.1) | async-done | bytes 524320 | tf_op jit(solution)/shard_map/all_to_all | solution.py:395
  161.3 9.8 %expert.7 = (bf16[256,2048]{1,0:T(8,128)(2,1)S(1)}, bf16[256,2048]{1,0:T(8,128)(2,1)S(1)}) custom-call(bf16[128,2048]{1,0:T(8,128)(2,1)S(1)} %bitcast.55, bf16[128,2048]{1,0:T(8,128)(2,1)S(1)} %copy-done.14, bf16[128,2048]{1,0:T(8,128)(2,1)S(1)} %copy-done.16, bf16[128,2048]{1,0:T(8,128)(2,1)} %collective-permute-done.27.refs_3_, ...), custom_call_target="tpu_custom_call" | custom-call | flops 5637144576 | bytes 15204352 | tf_op jit(solution)/shard_map/expert/pallas_call | solution.py:405
  171.9 4.3 %collective-permute-done.10.refs_1_ = bf16[128,2048]{1,0:T(8,128)(2,1)S(1)} collective-permute-done((bf16[128,2048]{1,0:T(8,128)(2,1)S(1)}, bf16[128,2048]{1,0:T(8,128)(2,1)S(1)}, u32[]{:S(2)}, u32[]{:S(2)}) %collective-permute-start.10) | collective-permute-done | bytes 524320 | tf_op jit(solution)/shard_map/ppermute | solution.py:221
  176.7 10.0 %expert.6 = (bf16[256,2048]{1,0:T(8,128)(2,1)S(1)}, bf16[256,2048]{1,0:T(8,128)(2,1)S(1)}) custom-call(bf16[128,2048]{1,0:T(8,128)(2,1)S(1)} %bitcast.52, bf16[128,2048]{1,0:T(8,128)(2,1)} %collective-permute-done.20.refs_1_, bf16[128,2048]{1,0:T(8,128)(2,1)} %collective-permute-done.21.refs_2_, bf16[128,2048]{1,0:T(8,128)(2,1)S(1)} %collective-permute-done.22.refs_3_, ...), custom_call_target="tpu_custom_call" | custom-call | flops 5637144576 | bytes 15204352 | tf_op jit(solution)/shard_map/expert/pallas_call | solution.py:405
  186.8 11.1 %expert.5 = (bf16[256,2048]{1,0:T(8,128)(2,1)S(1)}, bf16[256,2048]{1,0:T(8,128)(2,1)}) custom-call(bf16[128,2048]{1,0:T(8,128)(2,1)S(1)} %bitcast.49, bf16[128,2048]{1,0:T(8,128)(2,1)} %collective-permute-done.15.refs_1_, bf16[128,2048]{1,0:T(8,128)(2,1)} %collective-permute-done.16.refs_2_, bf16[128,2048]{1,0:T(8,128)(2,1)S(1)} %collective-permute-done.17.refs_3_, ...), custom_call_target="tpu_custom_call" | custom-call | flops 5637144576 | bytes 15204352 | tf_op jit(solution)/shard_map/expert/pallas_call | solution.py:405
  199.4 9.9 %expert.4 = (bf16[256,2048]{1,0:T(8,128)(2,1)S(1)}, bf16[256,2048]{1,0:T(8,128)(2,1)}) custom-call(bf16[128,2048]{1,0:T(8,128)(2,1)S(1)} %bitcast.46, bf16[128,2048]{1,0:T(8,128)(2,1)S(1)} %collective-permute-done.10.refs_1_, bf16[128,2048]{1,0:T(8,128)(2,1)S(1)} %collective-permute-done.11.refs_2_, bf16[128,2048]{1,0:T(8,128)(2,1)S(1)} %collective-permute-done.12.refs_3_, ...), custom_call_target="tpu_custom_call" | custom-call | flops 5637144576 | bytes 15204352 | tf_op jit(solution)/shard_map/expert/pallas_call | solution.py:405
  213.6 5.9 %all-to-all-start.8 = ((bf16[8,16,2048]{2,1,0:T(8,128)(2,1)}), bf16[8,16,2048]{2,1,0:T(8,128)(2,1)S(1)}, u32[]{:S(2)}, u32[]{:S(2)}) async-start(bf16[8,16,2048]{2,1,0:T(8,128)(2,1)} %bitcast.31), calls=%async_computation.8 | async-start | bytes 1048576 | tf_op jit(solution)/shard_map/all_to_all | solution.py:440
  222.3 3.4 %collective-permute-done.24 = bf16[128,2048]{1,0:T(8,128)(2,1)} collective-permute-done((bf16[128,2048]{1,0:T(8,128)(2,1)}, bf16[128,2048]{1,0:T(8,128)(2,1)}, u32[]{:S(2)}, u32[]{:S(2)}) %collective-permute-start.24) | collective-permute-done | bytes 524320 | tf_op jit(solution)/shard_map/ppermute | solution.py:221
  228.1 5.5 %all-to-all-done.8 = bf16[8,16,2048]{2,1,0:T(8,128)(2,1)S(1)} async-done(((bf16[8,16,2048]{2,1,0:T(8,128)(2,1)}), bf16[8,16,2048]{2,1,0:T(8,128)(2,1)S(1)}, u32[]{:S(2)}, u32[]{:S(2)}) %all-to-all-start.8) | async-done | bytes 524320 | tf_op jit(solution)/shard_map/all_to_all | solution.py:440
  233.6 3.6 %all-to-all-start.6 = ((bf16[8,16,2048]{2,1,0:T(8,128)(2,1)}), bf16[8,16,2048]{2,1,0:T(8,128)(2,1)S(1)}, u32[]{:S(2)}, u32[]{:S(2)}) async-start(bf16[8,16,2048]{2,1,0:T(8,128)(2,1)} %bitcast.69), calls=%async_computation.6 | async-start | bytes 1048576 | tf_op jit(solution)/shard_map/all_to_all | solution.py:440
  242.3 9.3 %all-to-all-done.6 = bf16[8,16,2048]{2,1,0:T(8,128)(2,1)S(1)} async-done(((bf16[8,16,2048]{2,1,0:T(8,128)(2,1)}), bf16[8,16,2048]{2,1,0:T(8,128)(2,1)S(1)}, u32[]{:S(2)}, u32[]{:S(2)}) %all-to-all-start.6) | async-done | bytes 524320 | tf_op jit(solution)/shard_map/all_to_all | solution.py:440
  251.7 3.6 %all-to-all-start.4 = ((bf16[8,16,2048]{2,1,0:T(8,128)(2,1)}), bf16[8,16,2048]{2,1,0:T(8,128)(2,1)S(1)}, u32[]{:S(2)}, u32[]{:S(2)}) async-start(bf16[8,16,2048]{2,1,0:T(8,128)(2,1)} %bitcast.70), calls=%async_computation.4 | async-start | bytes 1048576 | tf_op jit(solution)/shard_map/all_to_all | solution.py:440
  257.5 12.4 %all-to-all-done.4 = bf16[8,16,2048]{2,1,0:T(8,128)(2,1)S(1)} async-done(((bf16[8,16,2048]{2,1,0:T(8,128)(2,1)}), bf16[8,16,2048]{2,1,0:T(8,128)(2,1)S(1)}, u32[]{:S(2)}, u32[]{:S(2)}) %all-to-all-start.4) | async-done | bytes 524320 | tf_op jit(solution)/shard_map/all_to_all | solution.py:440
  270.0 3.6 %all-to-all-start.2 = ((bf16[8,16,2048]{2,1,0:T(8,128)(2,1)}), bf16[8,16,2048]{2,1,0:T(8,128)(2,1)S(1)}, u32[]{:S(2)}, u32[]{:S(2)}) async-start(bf16[8,16,2048]{2,1,0:T(8,128)(2,1)} %bitcast.71), calls=%async_computation.2 | async-start | bytes 1048576 | tf_op jit(solution)/shard_map/all_to_all | solution.py:440
  273.8 14.4 %all-to-all-done.2 = bf16[8,16,2048]{2,1,0:T(8,128)(2,1)S(1)} async-done(((bf16[8,16,2048]{2,1,0:T(8,128)(2,1)}), bf16[8,16,2048]{2,1,0:T(8,128)(2,1)S(1)}, u32[]{:S(2)}, u32[]{:S(2)}) %all-to-all-start.2) | async-done | bytes 524320 | tf_op jit(solution)/shard_map/all_to_all | solution.py:440
  (118 shorter events, 53.2 us)
Async XLA Ops:
  2.7 12.0 %collective-permute-start = (bf16[544,256]{1,0:T(8,128)(2,1)S(1)}, bf16[544,256]{1,0:T(8,128)(2,1)S(1)}, u32[]{:S(2)}, u32[]{:S(2)}) collective-permute-start(bf16[544,256]{1,0:T(8,128)(2,1)S(1)} %concatenate.7.refs_5_), channel_id=1, source_target_pairs={{0,8},{4,12},{8,16},{12,20},{16,24},{20,28},{1,9},{5,13},{9,17},{1... | collective-permute-start | bytes 835592 | tf_op jit(solution)/shard_map/ppermute | solution.py:168
  7.6 14.9 %collective-permute-start.3 = (bf16[512,256]{1,0:T(8,128)(2,1)}, bf16[512,256]{1,0:T(8,128)(2,1)S(1)}, u32[]{:S(2)}, u32[]{:S(2)}) collective-permute-start(bf16[512,256]{1,0:T(8,128)(2,1)} %refs_6_.1), channel_id=1, source_target_pairs={{0,8},{4,12},{8,16},{12,20},{16,24},{20,28},{1,9},{5,13},{9,17},{1... | collective-permute-start | bytes 786440 | tf_op jit(solution)/shard_map/ppermute | solution.py:168
  14.6 13.5 %collective-permute-start.1 = (bf16[544,256]{1,0:T(8,128)(2,1)S(1)}, bf16[544,256]{1,0:T(8,128)(2,1)S(1)}, u32[]{:S(2)}, u32[]{:S(2)}) collective-permute-start(bf16[544,256]{1,0:T(8,128)(2,1)S(1)} %collective-permute-done.refs_9_), channel_id=1, source_target_pairs={{0,8},{4,12},{8,16},{12,20},{16,24},{20,28},{1,9},{5,13},{9,17},{1... | collective-permute-start | bytes 835592 | tf_op jit(solution)/shard_map/ppermute | solution.py:168
  28.1 20.4 %collective-permute-start.8 = (bf16[544,256]{1,0:T(8,128)(2,1)S(1)}, bf16[544,256]{1,0:T(8,128)(2,1)S(1)}, u32[]{:S(2)}, u32[]{:S(2)}) collective-permute-start(bf16[544,256]{1,0:T(8,128)(2,1)S(1)} %collective-permute-done.refs_9_), channel_id=1, source_target_pairs={{0,4},{8,12},{16,20},{24,28},{4,0},{12,8},{20,16},{28,24},{1,5},{9... | collective-permute-start | bytes 835592 | tf_op jit(solution)/shard_map/ppermute | solution.py:169
  28.2 29.5 %collective-permute-start.2 = (bf16[544,256]{1,0:T(8,128)(2,1)S(1)}, bf16[544,256]{1,0:T(8,128)(2,1)S(1)}, u32[]{:S(2)}, u32[]{:S(2)}) collective-permute-start(bf16[544,256]{1,0:T(8,128)(2,1)S(1)} %collective-permute-done.1.refs_13_), channel_id=1, source_target_pairs={{4,0},{12,8},{20,16},{28,24},{5,1},{13,9},{21,17},{29,25},{6,2},{1... | collective-permute-start | bytes 835592 | tf_op jit(solution)/shard_map/ppermute | solution.py:169
  29.5 19.0 %collective-permute-start.9 = (bf16[512,256]{1,0:T(8,128)(2,1)S(1)}, bf16[512,256]{1,0:T(8,128)(2,1)}, u32[]{:S(2)}, u32[]{:S(2)}) collective-permute-start(bf16[512,256]{1,0:T(8,128)(2,1)S(1)} %collective-permute-done.3.refs_10_), channel_id=1, source_target_pairs={{0,4},{8,12},{16,20},{24,28},{4,0},{12,8},{20,16},{28,24},{1,5},{9... | collective-permute-start | bytes 786440 | tf_op jit(solution)/shard_map/ppermute | solution.py:169
  32.2 25.4 %collective-permute-start.5 = (bf16[512,256]{1,0:T(8,128)(2,1)S(1)}, bf16[512,256]{1,0:T(8,128)(2,1)}, u32[]{:S(2)}, u32[]{:S(2)}) collective-permute-start(bf16[512,256]{1,0:T(8,128)(2,1)S(1)} %collective-permute-done.4.refs_14_), channel_id=1, source_target_pairs={{4,0},{12,8},{20,16},{28,24},{5,1},{13,9},{21,17},{29,25},{6,2},{1... | collective-permute-start | bytes 786440 | tf_op jit(solution)/shard_map/ppermute | solution.py:169
  117.9 17.7 %all-to-all-start.3 = ((bf16[8,16,2048]{2,1,0:T(8,128)(2,1)}), bf16[8,16,2048]{2,1,0:T(8,128)(2,1)S(1)}, u32[]{:S(2)}, u32[]{:S(2)}) async-start(bf16[8,16,2048]{2,1,0:T(8,128)(2,1)} %bitcast.21), calls=%async_computation.3 | async-start | bytes 1048576 | tf_op jit(solution)/shard_map/all_to_all | solution.py:395
  121.5 18.7 %collective-permute-start.25 = (bf16[128,2048]{1,0:T(8,128)(2,1)S(1)}, bf16[128,2048]{1,0:T(8,128)(2,1)S(1)}, u32[]{:S(2)}, u32[]{:S(2)}) collective-permute-start(bf16[128,2048]{1,0:T(8,128)(2,1)S(1)} %bitcast.53), channel_id=1, source_target_pairs={{0,2},{1,3},{2,0},{3,1},{4,6},{5,7},{6,4},{7,5},{8,10},{9,11},{10,... | collective-permute-start | bytes 1572872 | tf_op jit(solution)/shard_map/ppermute | solution.py:221
  135.6 18.0 %all-to-all-start.1 = ((bf16[8,16,2048]{2,1,0:T(8,128)(2,1)}), bf16[8,16,2048]{2,1,0:T(8,128)(2,1)S(1)}, u32[]{:S(2)}, u32[]{:S(2)}) async-start(bf16[8,16,2048]{2,1,0:T(8,128)(2,1)} %bitcast.14), calls=%async_computation.1 | async-start | bytes 1048576 | tf_op jit(solution)/shard_map/all_to_all | solution.py:395
  139.4 15.0 %collective-permute-start.20 = (bf16[128,2048]{1,0:T(8,128)(2,1)S(1)}, bf16[128,2048]{1,0:T(8,128)(2,1)}, u32[]{:S(2)}, u32[]{:S(2)}) collective-permute-start(bf16[128,2048]{1,0:T(8,128)(2,1)S(1)} %bitcast.50), channel_id=1, source_target_pairs={{0,2},{1,3},{2,0},{3,1},{4,6},{5,7},{6,4},{7,5},{8,10},{9,11},{10,... | collective-permute-start | bytes 1572872 | tf_op jit(solution)/shard_map/ppermute | solution.py:221
  140.3 14.9 %collective-permute-start.27 = (bf16[128,2048]{1,0:T(8,128)(2,1)S(1)}, bf16[128,2048]{1,0:T(8,128)(2,1)}, u32[]{:S(2)}, u32[]{:S(2)}) collective-permute-start(bf16[128,2048]{1,0:T(8,128)(2,1)S(1)} %collective-permute-done.25.refs_1_), channel_id=1, source_target_pairs={{0,1},{1,0},{2,3},{3,2},{4,5},{5,4},{6,7},{7,6},{8,9},{9,8},{10,11... | collective-permute-start | bytes 1572872 | tf_op jit(solution)/shard_map/ppermute | solution.py:221
  141.2 30.0 %collective-permute-start.21 = (bf16[128,2048]{1,0:T(8,128)(2,1)S(1)}, bf16[128,2048]{1,0:T(8,128)(2,1)}, u32[]{:S(2)}, u32[]{:S(2)}) collective-permute-start(bf16[128,2048]{1,0:T(8,128)(2,1)S(1)} %bitcast.51), channel_id=1, source_target_pairs={{0,1},{1,0},{2,3},{3,2},{4,5},{5,4},{6,7},{7,6},{8,9},{9,8},{10,11... | collective-permute-start | bytes 1572872 | tf_op jit(solution)/shard_map/ppermute | solution.py:221
  141.6 30.2 %collective-permute-start.15 = (bf16[128,2048]{1,0:T(8,128)(2,1)S(1)}, bf16[128,2048]{1,0:T(8,128)(2,1)}, u32[]{:S(2)}, u32[]{:S(2)}) collective-permute-start(bf16[128,2048]{1,0:T(8,128)(2,1)S(1)} %bitcast.47), channel_id=1, source_target_pairs={{0,2},{1,3},{2,0},{3,1},{4,6},{5,7},{6,4},{7,5},{8,10},{9,11},{10,... | collective-permute-start | bytes 1572872 | tf_op jit(solution)/shard_map/ppermute | solution.py:221
  143.6 43.1 %collective-permute-start.16 = (bf16[128,2048]{1,0:T(8,128)(2,1)S(1)}, bf16[128,2048]{1,0:T(8,128)(2,1)}, u32[]{:S(2)}, u32[]{:S(2)}) collective-permute-start(bf16[128,2048]{1,0:T(8,128)(2,1)S(1)} %bitcast.48), channel_id=1, source_target_pairs={{0,1},{1,0},{2,3},{3,2},{4,5},{5,4},{6,7},{7,6},{8,9},{9,8},{10,11... | collective-permute-start | bytes 1572872 | tf_op jit(solution)/shard_map/ppermute | solution.py:221
  154.4 21.8 %collective-permute-start.10 = (bf16[128,2048]{1,0:T(8,128)(2,1)S(1)}, bf16[128,2048]{1,0:T(8,128)(2,1)S(1)}, u32[]{:S(2)}, u32[]{:S(2)}) collective-permute-start(bf16[128,2048]{1,0:T(8,128)(2,1)S(1)} %bitcast.44), channel_id=1, source_target_pairs={{0,2},{1,3},{2,0},{3,1},{4,6},{5,7},{6,4},{7,5},{8,10},{9,11},{10,... | collective-permute-start | bytes 1572872 | tf_op jit(solution)/shard_map/ppermute | solution.py:221
  155.2 21.0 %collective-permute-start.22 = (bf16[128,2048]{1,0:T(8,128)(2,1)}, bf16[128,2048]{1,0:T(8,128)(2,1)S(1)}, u32[]{:S(2)}, u32[]{:S(2)}) collective-permute-start(bf16[128,2048]{1,0:T(8,128)(2,1)} %collective-permute-done.20.refs_1_), channel_id=1, source_target_pairs={{0,1},{1,0},{2,3},{3,2},{4,5},{5,4},{6,7},{7,6},{8,9},{9,8},{10,11... | collective-permute-start | bytes 1572872 | tf_op jit(solution)/shard_map/ppermute | solution.py:221
  171.2 28.2 %collective-permute-start.11 = (bf16[128,2048]{1,0:T(8,128)(2,1)S(1)}, bf16[128,2048]{1,0:T(8,128)(2,1)S(1)}, u32[]{:S(2)}, u32[]{:S(2)}) collective-permute-start(bf16[128,2048]{1,0:T(8,128)(2,1)S(1)} %bitcast.45), channel_id=1, source_target_pairs={{0,1},{1,0},{2,3},{3,2},{4,5},{5,4},{6,7},{7,6},{8,9},{9,8},{10,11... | collective-permute-start | bytes 1572872 | tf_op jit(solution)/shard_map/ppermute | solution.py:221
  171.8 15.1 %collective-permute-start.17 = (bf16[128,2048]{1,0:T(8,128)(2,1)}, bf16[128,2048]{1,0:T(8,128)(2,1)S(1)}, u32[]{:S(2)}, u32[]{:S(2)}) collective-permute-start(bf16[128,2048]{1,0:T(8,128)(2,1)} %collective-permute-done.15.refs_1_), channel_id=1, source_target_pairs={{0,1},{1,0},{2,3},{3,2},{4,5},{5,4},{6,7},{7,6},{8,9},{9,8},{10,11... | collective-permute-start | bytes 1572872 | tf_op jit(solution)/shard_map/ppermute | solution.py:221
  176.2 23.2 %collective-permute-start.12 = (bf16[128,2048]{1,0:T(8,128)(2,1)S(1)}, bf16[128,2048]{1,0:T(8,128)(2,1)S(1)}, u32[]{:S(2)}, u32[]{:S(2)}) collective-permute-start(bf16[128,2048]{1,0:T(8,128)(2,1)S(1)} %collective-permute-done.10.refs_1_), channel_id=1, source_target_pairs={{0,1},{1,0},{2,3},{3,2},{4,5},{5,4},{6,7},{7,6},{8,9},{9,8},{10,11... | collective-permute-start | bytes 1572872 | tf_op jit(solution)/shard_map/ppermute | solution.py:221
  176.2 22.2 %collective-permute-start.28 = (bf16[256,2048]{1,0:T(8,128)(2,1)S(1)}, bf16[256,2048]{1,0:T(8,128)(2,1)S(1)}, u32[]{:S(2)}, u32[]{:S(2)}) collective-permute-start(bf16[256,2048]{1,0:T(8,128)(2,1)S(1)} %get-tuple-element.36), channel_id=1, source_target_pairs={{0,1},{1,0},{2,3},{3,2},{4,5},{5,4},{6,7},{7,6},{8,9},{9,8},{10,11... | collective-permute-start | bytes 3145736 | tf_op jit(solution)/shard_map/ppermute | solution.py:221
  186.8 22.7 %collective-permute-start.23 = (bf16[256,2048]{1,0:T(8,128)(2,1)S(1)}, bf16[256,2048]{1,0:T(8,128)(2,1)S(1)}, u32[]{:S(2)}, u32[]{:S(2)}) collective-permute-start(bf16[256,2048]{1,0:T(8,128)(2,1)S(1)} %get-tuple-element.33), channel_id=1, source_target_pairs={{0,1},{1,0},{2,3},{3,2},{4,5},{5,4},{6,7},{7,6},{8,9},{9,8},{10,11... | collective-permute-start | bytes 3145736 | tf_op jit(solution)/shard_map/ppermute | solution.py:221
  197.9 21.6 %collective-permute-start.18 = (bf16[256,2048]{1,0:T(8,128)(2,1)}, bf16[256,2048]{1,0:T(8,128)(2,1)}, u32[]{:S(2)}, u32[]{:S(2)}) collective-permute-start(bf16[256,2048]{1,0:T(8,128)(2,1)} %get-tuple-element.30), channel_id=1, source_target_pairs={{0,1},{1,0},{2,3},{3,2},{4,5},{5,4},{6,7},{7,6},{8,9},{9,8},{10,11... | collective-permute-start | bytes 3145736 | tf_op jit(solution)/shard_map/ppermute | solution.py:221
  198.6 14.0 %collective-permute-start.29 = (bf16[128,2048]{1,0:T(8,128)(2,1)S(1)}, bf16[128,2048]{1,0:T(8,128)(2,1)S(1)}, u32[]{:S(2)}, u32[]{:S(2)}) collective-permute-start(bf16[128,2048]{1,0:T(8,128)(2,1)S(1)} %add_convert_fusion.1), channel_id=1, source_target_pairs={{0,2},{1,3},{2,0},{3,1},{4,6},{5,7},{6,4},{7,5},{8,10},{9,11},{10,... | collective-permute-start | bytes 1572872 | tf_op jit(solution)/shard_map/ppermute | solution.py:221
  209.4 27.9 %collective-permute-start.13 = (bf16[256,2048]{1,0:T(8,128)(2,1)}, bf16[256,2048]{1,0:T(8,128)(2,1)}, u32[]{:S(2)}, u32[]{:S(2)}) collective-permute-start(bf16[256,2048]{1,0:T(8,128)(2,1)} %get-tuple-element.27), channel_id=1, source_target_pairs={{0,1},{1,0},{2,3},{3,2},{4,5},{5,4},{6,7},{7,6},{8,9},{9,8},{10,11... | collective-permute-start | bytes 3145736 | tf_op jit(solution)/shard_map/ppermute | solution.py:221
  210.6 15.1 %collective-permute-start.24 = (bf16[128,2048]{1,0:T(8,128)(2,1)}, bf16[128,2048]{1,0:T(8,128)(2,1)}, u32[]{:S(2)}, u32[]{:S(2)}) collective-permute-start(bf16[128,2048]{1,0:T(8,128)(2,1)} %add_convert_fusion.3), channel_id=1, source_target_pairs={{0,2},{1,3},{2,0},{3,1},{4,6},{5,7},{6,4},{7,5},{8,10},{9,11},{10,... | collective-permute-start | bytes 1572872 | tf_op jit(solution)/shard_map/ppermute | solution.py:221
  213.6 20.0 %all-to-all-start.8 = ((bf16[8,16,2048]{2,1,0:T(8,128)(2,1)}), bf16[8,16,2048]{2,1,0:T(8,128)(2,1)S(1)}, u32[]{:S(2)}, u32[]{:S(2)}) async-start(bf16[8,16,2048]{2,1,0:T(8,128)(2,1)} %bitcast.31), calls=%async_computation.8 | async-start | bytes 1048576 | tf_op jit(solution)/shard_map/all_to_all | solution.py:440
  221.5 18.6 %collective-permute-start.19 = (bf16[128,2048]{1,0:T(8,128)(2,1)}, bf16[128,2048]{1,0:T(8,128)(2,1)}, u32[]{:S(2)}, u32[]{:S(2)}) collective-permute-start(bf16[128,2048]{1,0:T(8,128)(2,1)} %add_convert_fusion.5), channel_id=1, source_target_pairs={{0,2},{1,3},{2,0},{3,1},{4,6},{5,7},{6,4},{7,5},{8,10},{9,11},{10,... | collective-permute-start | bytes 1572872 | tf_op jit(solution)/shard_map/ppermute | solution.py:221
  233.6 18.0 %all-to-all-start.6 = ((bf16[8,16,2048]{2,1,0:T(8,128)(2,1)}), bf16[8,16,2048]{2,1,0:T(8,128)(2,1)S(1)}, u32[]{:S(2)}, u32[]{:S(2)}) async-start(bf16[8,16,2048]{2,1,0:T(8,128)(2,1)} %bitcast.69), calls=%async_computation.6 | async-start | bytes 1048576 | tf_op jit(solution)/shard_map/all_to_all | solution.py:440
  239.3 16.0 %collective-permute-start.14 = (bf16[128,2048]{1,0:T(8,128)(2,1)}, bf16[128,2048]{1,0:T(8,128)(2,1)}, u32[]{:S(2)}, u32[]{:S(2)}) collective-permute-start(bf16[128,2048]{1,0:T(8,128)(2,1)} %add_convert_fusion.7), channel_id=1, source_target_pairs={{0,2},{1,3},{2,0},{3,1},{4,6},{5,7},{6,4},{7,5},{8,10},{9,11},{10,... | collective-permute-start | bytes 1572872 | tf_op jit(solution)/shard_map/ppermute | solution.py:221
  251.7 18.3 %all-to-all-start.4 = ((bf16[8,16,2048]{2,1,0:T(8,128)(2,1)}), bf16[8,16,2048]{2,1,0:T(8,128)(2,1)S(1)}, u32[]{:S(2)}, u32[]{:S(2)}) async-start(bf16[8,16,2048]{2,1,0:T(8,128)(2,1)} %bitcast.70), calls=%async_computation.4 | async-start | bytes 1048576 | tf_op jit(solution)/shard_map/all_to_all | solution.py:440
  270.0 18.3 %all-to-all-start.2 = ((bf16[8,16,2048]{2,1,0:T(8,128)(2,1)}), bf16[8,16,2048]{2,1,0:T(8,128)(2,1)S(1)}, u32[]{:S(2)}, u32[]{:S(2)}) async-start(bf16[8,16,2048]{2,1,0:T(8,128)(2,1)} %bitcast.71), calls=%async_computation.2 | async-start | bytes 1048576 | tf_op jit(solution)/shard_map/all_to_all | solution.py:440
  (25 other events, 378.6 us)

commit v5 on v3

--- a/solution.py
+++ b/solution.py
@@ -239,18 +239,23 @@
 def expert_kernel(count, *refs):
     inputs = refs[:count]
     gate_ref, up_ref, down_hbm = refs[count : count + 3]
-    mine_ref, other_ref, x_ref, hidden_ref, down_ref, sem = refs[count + 3 :]
+    mine_ref, other_ref, x_ref, hidden_ref, down_ref, sems = refs[count + 3 :]
     mine_rows = mine_ref.shape[0]
     step, steps = pl.program_id(0), hidden_ref.shape[0]
-    fetch = pltpu.make_async_copy(down_hbm, down_ref, sem)
+    each = x_ref.shape[0] // count
+    fetch = pltpu.make_async_copy(down_hbm, down_ref, sems.at[count])
+    loads = [
+        pltpu.make_async_copy(ref, x_ref.at[pl.ds(i * each, each)], sems.at[i])
+        for i, ref in enumerate(inputs)
+    ]
 
     @pl.when(step == 0)
     def _():
+        for load in loads:
+            load.start()
         fetch.start()
-        row = 0
-        for ref in inputs:
-            x_ref[row : row + ref.shape[0], :] = ref[...]
-            row += ref.shape[0]
+        for load in loads:
+            load.wait()
 
     both = jnp.concatenate([gate_ref[...], up_ref[...]], axis=1)
     product = jnp.dot(x_ref[...], both, preferred_element_type=jnp.float32)
@@ -373,7 +378,7 @@
             expert,
             grid=(hidden_width // h_tile,),
             out_shape=[jax.ShapeDtypeStruct((rows // 2, model_width), jnp.bfloat16)] * 2,
-            in_specs=[pl.BlockSpec(x.shape, lambda f: (0, 0)) for x in inputs]
+            in_specs=[pl.BlockSpec(memory_space=pltpu.HBM)] * len(inputs)
             + [pl.BlockSpec((model_width, h_tile), lambda f: (0, f))] * 2
             + [pl.BlockSpec(memory_space=pl.ANY)],
             out_specs=[pl.BlockSpec((rows // 2, model_width), lambda f: (0, 0))] * 2,
@@ -381,7 +386,7 @@
                 pltpu.VMEM((rows, model_width), jnp.bfloat16),
                 pltpu.VMEM((hidden_width // h_tile, rows, h_tile), jnp.bfloat16),
                 pltpu.VMEM((hidden_width, model_width), jnp.bfloat16),
-                pltpu.SemaphoreType.DMA,
+                pltpu.SemaphoreType.DMA((n_tp + 1,)),
             ],
             compiler_params=pltpu.CompilerParams(
                 dimension_semantics=("arbitrary",), vmem_limit_bytes=40 * 2**20

time: 295 us -> 295 us (level)
  no operation moved by 1% of the time
where the time goes in v5:
time: 295 us; the launch traced here: 294 us
  waiting for transfers between devices  145 us (49%)
  starting transfers between devices  49.8 us (17%)
  Pallas kernels  43.5 us (15%)
  blocking collectives  35.8 us (12%)
  local copies, waits for them, and re-layouts  10.8 us (4%)
  other arithmetic  8.54 us (3%)
    ppermute x10, waiting for transfers between devices, swap(): lax.ppermute(x, axis, [(i, i ^ bits) for i in range(lax.axis_size(axis))])  70.4 us
    all_to_all x1, blocking collectives, on_device(): arrived.append(lax.all_to_all(outbound[c], 'sp', 0, 0, tiled=True))  35.8 us
    pallas_call x2, Pallas kernels, on_device(): pl.pallas_call(expert, grid=(hidden_width // h_tile,), out_shape=[jax.Sha...  32.3 us
    all_to_all x1, waiting for transfers between devices, on_device(): arrived.append(lax.all_to_all(outbound[c], 'sp', 0, 0, tiled=True))  24.6 us
    all_to_all x2, waiting for transfers between devices, on_device(): lax.all_to_all(result.astype(jnp.bfloat16), 'sp', 0, 0, tiled=True)  24.1 us
    ppermute x6, waiting for transfers between devices, chain(): other.append(lax.ppermute(own[-1], 'sp', pairs))  16.6 us
    ppermute x4, starting transfers between devices, chain(): own.append(lax.ppermute(own[-1], 'sp', ahead))  16.3 us
    all_to_all x2, starting transfers between devices, on_device(): lax.all_to_all(result.astype(jnp.bfloat16), 'sp', 0, 0, tiled=True)  11 us
  transfers between devices with their start and end apart: 24, of which 10 were waited for; matrix products, arithmetic and copies ran while one was open for 3% of the time, Pallas kernels for 11%

profile of v5, /device:TPU:0, one launch (start us, length us, event | category | flops | bytes accessed | tf_op | source)
XLA Modules:
  0.0 294.0 jit_solution(4940586954259557510)
XLA Ops:
  2.5 5.0 %collective-permute-start.2 = (bf16[544,256]{1,0:T(8,128)(2,1)S(1)}, bf16[544,256]{1,0:T(8,128)(2,1)S(1)}, u32[]{:S(2)}, u32[]{:S(2)}) collective-permute-start(bf16[544,256]{1,0:T(8,128)(2,1)S(1)} %concatenate.7.refs_5_), channel_id=1, source_target_pairs={{0,8},{4,12},{8,16},{12,20},{16,24},{20,28},{1,9},{5,13},{9,17},{1... | collective-permute-start | bytes 835592 | tf_op jit(solution)/shard_map/ppermute | solution.py:148
  7.5 3.5 %collective-permute-start.3 = (bf16[512,256]{1,0:T(8,128)(2,1)}, bf16[512,256]{1,0:T(8,128)(2,1)S(1)}, u32[]{:S(2)}, u32[]{:S(2)}) collective-permute-start(bf16[512,256]{1,0:T(8,128)(2,1)} %refs_6_.1), channel_id=1, source_target_pairs={{0,8},{4,12},{8,16},{12,20},{16,24},{20,28},{1,9},{5,13},{9,17},{1... | collective-permute-start | bytes 786440 | tf_op jit(solution)/shard_map/ppermute | solution.py:148
  11.0 3.5 %collective-permute-done.2.refs_9_ = bf16[544,256]{1,0:T(8,128)(2,1)S(1)} collective-permute-done((bf16[544,256]{1,0:T(8,128)(2,1)S(1)}, bf16[544,256]{1,0:T(8,128)(2,1)S(1)}, u32[]{:S(2)}, u32[]{:S(2)}) %collective-permute-start.2) | collective-permute-done | bytes 278560 | tf_op jit(solution)/shard_map/ppermute | solution.py:148
  14.5 4.4 %collective-permute-start.6 = (bf16[544,256]{1,0:T(8,128)(2,1)S(1)}, bf16[544,256]{1,0:T(8,128)(2,1)S(1)}, u32[]{:S(2)}, u32[]{:S(2)}) collective-permute-start(bf16[544,256]{1,0:T(8,128)(2,1)S(1)} %collective-permute-done.2.refs_9_), channel_id=1, source_target_pairs={{0,8},{4,12},{8,16},{12,20},{16,24},{20,28},{1,9},{5,13},{9,17},{1... | collective-permute-start | bytes 835592 | tf_op jit(solution)/shard_map/ppermute | solution.py:148
  18.9 3.4 %collective-permute-start.1 = (bf16[512,256]{1,0:T(8,128)(2,1)}, bf16[512,256]{1,0:T(8,128)(2,1)S(1)}, u32[]{:S(2)}, u32[]{:S(2)}) collective-permute-start(bf16[512,256]{1,0:T(8,128)(2,1)} %refs_6_.1), channel_id=1, source_target_pairs={{0,4},{8,12},{16,20},{24,28},{1,5},{9,13},{17,21},{25,29},{2,6},{1... | collective-permute-start | bytes 786440 | tf_op jit(solution)/shard_map/ppermute | solution.py:149
  22.4 3.5 %collective-permute-start.7 = (bf16[512,256]{1,0:T(8,128)(2,1)S(1)}, bf16[512,256]{1,0:T(8,128)(2,1)S(1)}, u32[]{:S(2)}, u32[]{:S(2)}) collective-permute-start(bf16[512,256]{1,0:T(8,128)(2,1)S(1)} %collective-permute-done.3.refs_10_), channel_id=1, source_target_pairs={{0,8},{4,12},{8,16},{12,20},{16,24},{20,28},{1,9},{5,13},{9,17},{1... | collective-permute-start | bytes 786440 | tf_op jit(solution)/shard_map/ppermute | solution.py:148
  25.9 2.1 collective-permute-start
  28.1 1.3 collective-permute-start.8
  29.4 2.7 collective-permute-start.5
  35.0 13.3 %collective-permute-done.5.refs_12_ = bf16[512,256]{1,0:T(8,128)(2,1)S(1)} collective-permute-done((bf16[512,256]{1,0:T(8,128)(2,1)S(1)}, bf16[512,256]{1,0:T(8,128)(2,1)S(1)}, u32[]{:S(2)}, u32[]{:S(2)}) %collective-permute-start.5) | collective-permute-done | bytes 262176 | tf_op jit(solution)/shard_map/ppermute | solution.py:149
  48.3 2.8 collective-permute-done.9.refs_16_
  56.0 6.6 %attention.1 = bf16[512,256]{1,0:T(8,128)(2,1)} custom-call(s32[6]{0:T(128)S(1)} %convert_element_type.65.refs_0_, s32[512]{0:T(512)S(1)} %copy-done.9, bf16[512,256]{1,0:T(8,128)(2,1)S(1)} %copy-done.4, f32[512,8]{1,0:T(8,128)S(1)} %copy.24.refs_3_, f32[1,256]{1,0:T(1,128)S(1)} %bitcast.42, bf16[544,256]{1,0:T(8,128)(2,1)S(1)} %concatenate.7.refs_5_, ...), custom_call_target="tpu_custom_call" | custom-call | tf_op jit(solution)/shard_map/attention/pallas_call | solution.py:174
  62.7 3.4 %all-to-all-start = ((bf16[4,128,256]{2,1,0:T(8,128)(2,1)}), bf16[4,128,256]{2,1,0:T(8,128)(2,1)S(1)}, u32[]{:S(2)}, u32[]{:S(2)}) async-start(bf16[4,128,256]{2,1,0:T(8,128)(2,1)} %bitcast.10), calls=%async_computation | async-start | bytes 524288 | tf_op jit(solution)/shard_map/all_to_all | solution.py:342
  66.1 6.0 %all-to-all-done = bf16[4,128,256]{2,1,0:T(8,128)(2,1)S(1)} async-done(((bf16[4,128,256]{2,1,0:T(8,128)(2,1)}), bf16[4,128,256]{2,1,0:T(8,128)(2,1)S(1)}, u32[]{:S(2)}, u32[]{:S(2)}) %all-to-all-start) | async-done | bytes 262176 | tf_op jit(solution)/shard_map/all_to_all | solution.py:342
  72.1 2.2 copy-done
  74.3 2.5 project.1
  76.8 35.8 %all_to_all.63 = bf16[8,32,2048]{2,1,0:T(8,128)(2,1)S(1)} all-to-all(bf16[8,32,2048]{2,1,0:T(8,128)(2,1)S(1)} %bitcast.40), channel_id=1, replica_groups=mesh['sp'=8,'tp'=4] {'sp'}, dimensions={0} | all-to-all | bytes 2097152 | tf_op jit(solution)/shard_map/all_to_all | solution.py:367
  112.7 3.7 %all-to-all-start.1 = ((bf16[8,32,2048]{2,1,0:T(8,128)(2,1)}), bf16[8,32,2048]{2,1,0:T(8,128)(2,1)S(1)}, u32[]{:S(2)}, u32[]{:S(2)}) async-start(bf16[8,32,2048]{2,1,0:T(8,128)(2,1)} %bitcast.14), calls=%async_computation.1 | async-start | bytes 2097152 | tf_op jit(solution)/shard_map/all_to_all | solution.py:367
  117.2 24.6 %all-to-all-done.1 = bf16[8,32,2048]{2,1,0:T(8,128)(2,1)S(1)} async-done(((bf16[8,32,2048]{2,1,0:T(8,128)(2,1)}), bf16[8,32,2048]{2,1,0:T(8,128)(2,1)S(1)}, u32[]{:S(2)}, u32[]{:S(2)}) %all-to-all-start.1) | async-done | bytes 1048608 | tf_op jit(solution)/shard_map/all_to_all | solution.py:367
  143.1 22.0 %collective-permute-done.10.refs_1_ = bf16[256,2048]{1,0:T(8,128)(2,1)S(1)} collective-permute-done((bf16[256,2048]{1,0:T(8,128)(2,1)S(1)}, bf16[256,2048]{1,0:T(8,128)(2,1)S(1)}, u32[]{:S(2)}, u32[]{:S(2)}) %collective-permute-start.10) | collective-permute-done | bytes 1048608 | tf_op jit(solution)/shard_map/ppermute | solution.py:190
  165.2 2.0 copy-done.11
  167.2 15.6 %expert.3 = (bf16[512,2048]{1,0:T(8,128)(2,1)S(1)}, bf16[512,2048]{1,0:T(8,128)(2,1)S(1)}) custom-call(bf16[256,2048]{1,0:T(8,128)(2,1)S(1)} %bitcast.39, bf16[256,2048]{1,0:T(8,128)(2,1)S(1)} %collective-permute-done.15.refs_1_, bf16[256,2048]{1,0:T(8,128)(2,1)S(1)} %collective-permute-done.16.refs_2_, ...), custom_call_target="tpu_custom_call" | custom-call | flops 11274289152 | bytes 19398656 | tf_op jit(solution)/shard_map/expert/pallas_call | solution.py:377
  183.4 16.8 %expert.2 = (bf16[512,2048]{1,0:T(8,128)(2,1)S(1)}, bf16[512,2048]{1,0:T(8,128)(2,1)}) custom-call(bf16[256,2048]{1,0:T(8,128)(2,1)S(1)} %bitcast.36, bf16[256,2048]{1,0:T(8,128)(2,1)S(1)} %collective-permute-done.10.refs_1_, bf16[256,2048]{1,0:T(8,128)(2,1)S(1)} %collective-permute-done.11.refs_2_, bf16[256,2048]{1,0:T(8,128)(2,1)S(1)} %collective-permute-done.12.refs_3_, ...), custom_call_target="tpu_custom_call" | custom-call | flops 11274289152 | bytes 19398656 | tf_op jit(solution)/shard_map/expert/pallas_call | solution.py:377
  201.5 24.8 %collective-permute-done.19 = bf16[256,2048]{1,0:T(8,128)(2,1)S(1)} collective-permute-done((bf16[256,2048]{1,0:T(8,128)(2,1)S(1)}, bf16[256,2048]{1,0:T(8,128)(2,1)S(1)}, u32[]{:S(2)}, u32[]{:S(2)}) %collective-permute-start.19) | collective-permute-done | bytes 1048608 | tf_op jit(solution)/shard_map/ppermute | solution.py:190
  226.2 1.6 add_convert_fusion
  227.8 5.1 %all-to-all-start.4 = ((bf16[8,32,2048]{2,1,0:T(8,128)(2,1)}), bf16[8,32,2048]{2,1,0:T(8,128)(2,1)S(1)}, u32[]{:S(2)}, u32[]{:S(2)}) async-start(bf16[8,32,2048]{2,1,0:T(8,128)(2,1)} %bitcast.45), calls=%async_computation.4 | async-start | bytes 2097152 | tf_op jit(solution)/shard_map/all_to_all | solution.py:412
  232.9 1.6 add_convert_fusion.3
  235.4 23.6 %collective-permute-done.14 = bf16[256,2048]{1,0:T(8,128)(2,1)S(1)} collective-permute-done((bf16[256,2048]{1,0:T(8,128)(2,1)S(1)}, bf16[256,2048]{1,0:T(8,128)(2,1)S(1)}, u32[]{:S(2)}, u32[]{:S(2)}) %collective-permute-start.14) | collective-permute-done | bytes 1048608 | tf_op jit(solution)/shard_map/ppermute | solution.py:190
  259.0 2.7 add_convert_fusion.2
  261.7 5.9 %all-to-all-start.2 = ((bf16[8,32,2048]{2,1,0:T(8,128)(2,1)}), bf16[8,32,2048]{2,1,0:T(8,128)(2,1)S(1)}, u32[]{:S(2)}, u32[]{:S(2)}) async-start(bf16[8,32,2048]{2,1,0:T(8,128)(2,1)} %bitcast.46), calls=%async_computation.2 | async-start | bytes 2097152 | tf_op jit(solution)/shard_map/all_to_all | solution.py:412
  267.8 24.1 %all-to-all-done.2 = bf16[8,32,2048]{2,1,0:T(8,128)(2,1)S(1)} async-done(((bf16[8,32,2048]{2,1,0:T(8,128)(2,1)}), bf16[8,32,2048]{2,1,0:T(8,128)(2,1)S(1)}, u32[]{:S(2)}, u32[]{:S(2)}) %all-to-all-start.2) | async-done | bytes 1048608 | tf_op jit(solution)/shard_map/all_to_all | solution.py:412
  292.0 2.0 combine.1
  (74 shorter events, 15.5 us)
Async XLA Ops:
  2.5 12.0 %collective-permute-start.2 = (bf16[544,256]{1,0:T(8,128)(2,1)S(1)}, bf16[544,256]{1,0:T(8,128)(2,1)S(1)}, u32[]{:S(2)}, u32[]{:S(2)}) collective-permute-start(bf16[544,256]{1,0:T(8,128)(2,1)S(1)} %concatenate.7.refs_5_), channel_id=1, source_target_pairs={{0,8},{4,12},{8,16},{12,20},{16,24},{20,28},{1,9},{5,13},{9,17},{1... | collective-permute-start | bytes 835592 | tf_op jit(solution)/shard_map/ppermute | solution.py:148
  7.5 14.9 %collective-permute-start.3 = (bf16[512,256]{1,0:T(8,128)(2,1)}, bf16[512,256]{1,0:T(8,128)(2,1)S(1)}, u32[]{:S(2)}, u32[]{:S(2)}) collective-permute-start(bf16[512,256]{1,0:T(8,128)(2,1)} %refs_6_.1), channel_id=1, source_target_pairs={{0,8},{4,12},{8,16},{12,20},{16,24},{20,28},{1,9},{5,13},{9,17},{1... | collective-permute-start | bytes 786440 | tf_op jit(solution)/shard_map/ppermute | solution.py:148
  14.5 13.5 %collective-permute-start.6 = (bf16[544,256]{1,0:T(8,128)(2,1)S(1)}, bf16[544,256]{1,0:T(8,128)(2,1)S(1)}, u32[]{:S(2)}, u32[]{:S(2)}) collective-permute-start(bf16[544,256]{1,0:T(8,128)(2,1)S(1)} %collective-permute-done.2.refs_9_), channel_id=1, source_target_pairs={{0,8},{4,12},{8,16},{12,20},{16,24},{20,28},{1,9},{5,13},{9,17},{1... | collective-permute-start | bytes 835592 | tf_op jit(solution)/shard_map/ppermute | solution.py:148
  18.9 10.5 %collective-permute-start.1 = (bf16[512,256]{1,0:T(8,128)(2,1)}, bf16[512,256]{1,0:T(8,128)(2,1)S(1)}, u32[]{:S(2)}, u32[]{:S(2)}) collective-permute-start(bf16[512,256]{1,0:T(8,128)(2,1)} %refs_6_.1), channel_id=1, source_target_pairs={{0,4},{8,12},{16,20},{24,28},{1,5},{9,13},{17,21},{25,29},{2,6},{1... | collective-permute-start | bytes 786440 | tf_op jit(solution)/shard_map/ppermute | solution.py:149
  22.4 9.7 %collective-permute-start.7 = (bf16[512,256]{1,0:T(8,128)(2,1)S(1)}, bf16[512,256]{1,0:T(8,128)(2,1)S(1)}, u32[]{:S(2)}, u32[]{:S(2)}) collective-permute-start(bf16[512,256]{1,0:T(8,128)(2,1)S(1)} %collective-permute-done.3.refs_10_), channel_id=1, source_target_pairs={{0,8},{4,12},{8,16},{12,20},{16,24},{20,28},{1,9},{5,13},{9,17},{1... | collective-permute-start | bytes 786440 | tf_op jit(solution)/shard_map/ppermute | solution.py:148
  25.9 9.1 %collective-permute-start = (bf16[544,256]{1,0:T(8,128)(2,1)S(1)}, bf16[544,256]{1,0:T(8,128)(2,1)S(1)}, u32[]{:S(2)}, u32[]{:S(2)}) collective-permute-start(bf16[544,256]{1,0:T(8,128)(2,1)S(1)} %concatenate.7.refs_5_), channel_id=1, source_target_pairs={{0,4},{8,12},{16,20},{24,28},{1,5},{9,13},{17,21},{25,29},{2,6},{1... | collective-permute-start | bytes 835592 | tf_op jit(solution)/shard_map/ppermute | solution.py:149
  28.0 20.3 %collective-permute-start.4 = (bf16[544,256]{1,0:T(8,128)(2,1)S(1)}, bf16[544,256]{1,0:T(8,128)(2,1)S(1)}, u32[]{:S(2)}, u32[]{:S(2)}) collective-permute-start(bf16[544,256]{1,0:T(8,128)(2,1)S(1)} %collective-permute-done.2.refs_9_), channel_id=1, source_target_pairs={{0,4},{8,12},{16,20},{24,28},{4,0},{12,8},{20,16},{28,24},{1,5},{9... | collective-permute-start | bytes 835592 | tf_op jit(solution)/shard_map/ppermute | solution.py:149
  28.1 23.7 %collective-permute-start.8 = (bf16[544,256]{1,0:T(8,128)(2,1)S(1)}, bf16[544,256]{1,0:T(8,128)(2,1)S(1)}, u32[]{:S(2)}, u32[]{:S(2)}) collective-permute-start(bf16[544,256]{1,0:T(8,128)(2,1)S(1)} %collective-permute-done.6.refs_13_), channel_id=1, source_target_pairs={{4,0},{12,8},{20,16},{28,24},{5,1},{13,9},{21,17},{29,25},{6,2},{1... | collective-permute-start | bytes 835592 | tf_op jit(solution)/shard_map/ppermute | solution.py:149
  29.4 18.9 %collective-permute-start.5 = (bf16[512,256]{1,0:T(8,128)(2,1)S(1)}, bf16[512,256]{1,0:T(8,128)(2,1)S(1)}, u32[]{:S(2)}, u32[]{:S(2)}) collective-permute-start(bf16[512,256]{1,0:T(8,128)(2,1)S(1)} %collective-permute-done.3.refs_10_), channel_id=1, source_target_pairs={{0,4},{8,12},{16,20},{24,28},{4,0},{12,8},{20,16},{28,24},{1,5},{9... | collective-permute-start | bytes 786440 | tf_op jit(solution)/shard_map/ppermute | solution.py:149
  32.1 19.0 %collective-permute-start.9 = (bf16[512,256]{1,0:T(8,128)(2,1)S(1)}, bf16[512,256]{1,0:T(8,128)(2,1)S(1)}, u32[]{:S(2)}, u32[]{:S(2)}) collective-permute-start(bf16[512,256]{1,0:T(8,128)(2,1)S(1)} %collective-permute-done.7.refs_14_), channel_id=1, source_target_pairs={{4,0},{12,8},{20,16},{28,24},{5,1},{13,9},{21,17},{29,25},{6,2},{1... | collective-permute-start | bytes 786440 | tf_op jit(solution)/shard_map/ppermute | solution.py:149
  56.0 10.1 %copy-start.13 = (s32[128,2]{0,1:T(2,128)S(1)}, s32[128,2]{0,1:T(2,128)}, u32[]{:S(2)}) copy-start(s32[128,2]{0,1:T(2,128)} %param.23) | copy-start | bytes 3076
  56.0 16.1 %copy-start.3 = (bf16[128,2048]{1,0:T(8,128)(2,1)S(1)}, bf16[128,2048]{1,0:T(8,128)(2,1)}, u32[]{:S(2)}) copy-start(bf16[128,2048]{1,0:T(8,128)(2,1)} %refs_2_.4) | copy-start | bytes 1572868
  56.0 16.1 %copy-start.8 = (f32[2048]{0:T(1024)S(1)}, f32[2048]{0:T(1024)}, u32[]{:S(2)}) copy-start(f32[2048]{0:T(1024)} %param.22) | copy-start | bytes 24580
  62.7 9.4 %all-to-all-start = ((bf16[4,128,256]{2,1,0:T(8,128)(2,1)}), bf16[4,128,256]{2,1,0:T(8,128)(2,1)S(1)}, u32[]{:S(2)}, u32[]{:S(2)}) async-start(bf16[4,128,256]{2,1,0:T(8,128)(2,1)} %bitcast.10), calls=%async_computation | async-start | bytes 524288 | tf_op jit(solution)/shard_map/all_to_all | solution.py:342
  72.1 2.2 copy-start
  76.8 35.9 %copy-start.1 = (bf16[128,2048]{1,0:T(8,128)(2,1)}, bf16[128,2048]{1,0:T(8,128)(2,1)S(1)}, u32[]{:S(2)}) copy-start(bf16[128,2048]{1,0:T(8,128)(2,1)S(1)} %get-tuple-element.12.refs_0_) | copy-start | bytes 1572868
  112.7 29.1 %all-to-all-start.1 = ((bf16[8,32,2048]{2,1,0:T(8,128)(2,1)}), bf16[8,32,2048]{2,1,0:T(8,128)(2,1)S(1)}, u32[]{:S(2)}, u32[]{:S(2)}) async-start(bf16[8,32,2048]{2,1,0:T(8,128)(2,1)} %bitcast.14), calls=%async_computation.1 | async-start | bytes 2097152 | tf_op jit(solution)/shard_map/all_to_all | solution.py:367
  116.4 26.2 %collective-permute-start.15 = (bf16[256,2048]{1,0:T(8,128)(2,1)S(1)}, bf16[256,2048]{1,0:T(8,128)(2,1)S(1)}, u32[]{:S(2)}, u32[]{:S(2)}) collective-permute-start(bf16[256,2048]{1,0:T(8,128)(2,1)S(1)} %bitcast.37), channel_id=1, source_target_pairs={{0,2},{1,3},{2,0},{3,1},{4,6},{5,7},{6,4},{7,5},{8,10},{9,11},{10,... | collective-permute-start | bytes 3145736 | tf_op jit(solution)/shard_map/ppermute | solution.py:190
  141.8 23.3 %collective-permute-start.10 = (bf16[256,2048]{1,0:T(8,128)(2,1)S(1)}, bf16[256,2048]{1,0:T(8,128)(2,1)S(1)}, u32[]{:S(2)}, u32[]{:S(2)}) collective-permute-start(bf16[256,2048]{1,0:T(8,128)(2,1)S(1)} %bitcast.34), channel_id=1, source_target_pairs={{0,2},{1,3},{2,0},{3,1},{4,6},{5,7},{6,4},{7,5},{8,10},{9,11},{10,... | collective-permute-start | bytes 3145736 | tf_op jit(solution)/shard_map/ppermute | solution.py:190
  142.6 22.6 %collective-permute-start.16 = (bf16[256,2048]{1,0:T(8,128)(2,1)S(1)}, bf16[256,2048]{1,0:T(8,128)(2,1)S(1)}, u32[]{:S(2)}, u32[]{:S(2)}) collective-permute-start(bf16[256,2048]{1,0:T(8,128)(2,1)S(1)} %bitcast.38), channel_id=1, source_target_pairs={{0,1},{1,0},{2,3},{3,2},{4,5},{5,4},{6,7},{7,6},{8,9},{9,8},{10,11... | collective-permute-start | bytes 3145736 | tf_op jit(solution)/shard_map/ppermute | solution.py:190
  142.6 22.6 %collective-permute-start.17 = (bf16[256,2048]{1,0:T(8,128)(2,1)S(1)}, bf16[256,2048]{1,0:T(8,128)(2,1)S(1)}, u32[]{:S(2)}, u32[]{:S(2)}) collective-permute-start(bf16[256,2048]{1,0:T(8,128)(2,1)S(1)} %collective-permute-done.15.refs_1_), channel_id=1, source_target_pairs={{0,1},{1,0},{2,3},{3,2},{4,5},{5,4},{6,7},{7,6},{8,9},{9,8},{10,11... | collective-permute-start | bytes 3145736 | tf_op jit(solution)/shard_map/ppermute | solution.py:190
  143.1 40.2 %collective-permute-start.11 = (bf16[256,2048]{1,0:T(8,128)(2,1)S(1)}, bf16[256,2048]{1,0:T(8,128)(2,1)S(1)}, u32[]{:S(2)}, u32[]{:S(2)}) collective-permute-start(bf16[256,2048]{1,0:T(8,128)(2,1)S(1)} %bitcast.35), channel_id=1, source_target_pairs={{0,1},{1,0},{2,3},{3,2},{4,5},{5,4},{6,7},{7,6},{8,9},{9,8},{10,11... | collective-permute-start | bytes 3145736 | tf_op jit(solution)/shard_map/ppermute | solution.py:190
  165.2 18.2 %collective-permute-start.12 = (bf16[256,2048]{1,0:T(8,128)(2,1)S(1)}, bf16[256,2048]{1,0:T(8,128)(2,1)S(1)}, u32[]{:S(2)}, u32[]{:S(2)}) collective-permute-start(bf16[256,2048]{1,0:T(8,128)(2,1)S(1)} %collective-permute-done.10.refs_1_), channel_id=1, source_target_pairs={{0,1},{1,0},{2,3},{3,2},{4,5},{5,4},{6,7},{7,6},{8,9},{9,8},{10,11... | collective-permute-start | bytes 3145736 | tf_op jit(solution)/shard_map/ppermute | solution.py:190
  167.2 16.1 %copy-start.12 = (bf16[1,2048,896]{2,1,0:T(8,128)(2,1)S(1)}, bf16[1,2048,896]{2,1,0:T(8,128)(2,1)}, u32[]{:S(2)}) copy-start(bf16[1,2048,896]{2,1,0:T(8,128)(2,1)} %param.25) | copy-start | bytes 11010052
  182.8 17.5 %collective-permute-start.18 = (bf16[512,2048]{1,0:T(8,128)(2,1)S(1)}, bf16[512,2048]{1,0:T(8,128)(2,1)S(1)}, u32[]{:S(2)}, u32[]{:S(2)}) collective-permute-start(bf16[512,2048]{1,0:T(8,128)(2,1)S(1)} %get-tuple-element.18), channel_id=1, source_target_pairs={{0,1},{1,0},{2,3},{3,2},{4,5},{5,4},{6,7},{7,6},{8,9},{9,8},{10,11... | collective-permute-start | bytes 6291464 | tf_op jit(solution)/shard_map/ppermute | solution.py:190
  200.1 32.8 %collective-permute-start.13 = (bf16[512,2048]{1,0:T(8,128)(2,1)}, bf16[512,2048]{1,0:T(8,128)(2,1)}, u32[]{:S(2)}, u32[]{:S(2)}) collective-permute-start(bf16[512,2048]{1,0:T(8,128)(2,1)} %get-tuple-element.15), channel_id=1, source_target_pairs={{0,1},{1,0},{2,3},{3,2},{4,5},{5,4},{6,7},{7,6},{8,9},{9,8},{10,11... | collective-permute-start | bytes 6291464 | tf_op jit(solution)/shard_map/ppermute | solution.py:190
  200.6 25.6 %collective-permute-start.19 = (bf16[256,2048]{1,0:T(8,128)(2,1)S(1)}, bf16[256,2048]{1,0:T(8,128)(2,1)S(1)}, u32[]{:S(2)}, u32[]{:S(2)}) collective-permute-start(bf16[256,2048]{1,0:T(8,128)(2,1)S(1)} %add_convert_fusion.1), channel_id=1, source_target_pairs={{0,2},{1,3},{2,0},{3,1},{4,6},{5,7},{6,4},{7,5},{8,10},{9,11},{10,... | collective-permute-start | bytes 3145736 | tf_op jit(solution)/shard_map/ppermute | solution.py:190
  227.8 33.9 %all-to-all-start.4 = ((bf16[8,32,2048]{2,1,0:T(8,128)(2,1)}), bf16[8,32,2048]{2,1,0:T(8,128)(2,1)S(1)}, u32[]{:S(2)}, u32[]{:S(2)}) async-start(bf16[8,32,2048]{2,1,0:T(8,128)(2,1)} %bitcast.45), calls=%async_computation.4 | async-start | bytes 2097152 | tf_op jit(solution)/shard_map/all_to_all | solution.py:412
  234.6 24.5 %collective-permute-start.14 = (bf16[256,2048]{1,0:T(8,128)(2,1)S(1)}, bf16[256,2048]{1,0:T(8,128)(2,1)S(1)}, u32[]{:S(2)}, u32[]{:S(2)}) collective-permute-start(bf16[256,2048]{1,0:T(8,128)(2,1)S(1)} %add_convert_fusion.3), channel_id=1, source_target_pairs={{0,2},{1,3},{2,0},{3,1},{4,6},{5,7},{6,4},{7,5},{8,10},{9,11},{10,... | collective-permute-start | bytes 3145736 | tf_op jit(solution)/shard_map/ppermute | solution.py:190
  261.7 6.0 %copy-start.14 = (f32[128,2]{0,1:T(2,128)S(1)}, f32[128,2]{0,1:T(2,128)}, u32[]{:S(2)}) copy-start(f32[128,2]{0,1:T(2,128)} %param.24) | copy-start | bytes 3076
  261.7 30.2 %copy-start.2 = (bf16[128,2048]{1,0:T(8,128)(2,1)S(1)}, bf16[128,2048]{1,0:T(8,128)(2,1)}, u32[]{:S(2)}) copy-start(bf16[128,2048]{1,0:T(8,128)(2,1)} %copy-done.1) | copy-start | bytes 1572868
  261.7 30.2 %all-to-all-start.2 = ((bf16[8,32,2048]{2,1,0:T(8,128)(2,1)}), bf16[8,32,2048]{2,1,0:T(8,128)(2,1)S(1)}, u32[]{:S(2)}, u32[]{:S(2)}) async-start(bf16[8,32,2048]{2,1,0:T(8,128)(2,1)} %bitcast.46), calls=%async_computation.2 | async-start | bytes 2097152 | tf_op jit(solution)/shard_map/all_to_all | solution.py:412
  (7 other events, 7.0 us)

commit v6 on v5

--- a/solution.py
+++ b/solution.py
@@ -21,7 +21,14 @@
 def attention_kernel(tokens, heads, head_size, tile, sources, *refs):
     valid_ref, docs_ref, q_ref, meta_ref, gain_ref = refs[:5]
     kv_refs = refs[5 : 5 + 2 * sources]
-    out_ref, m_ref, l_ref, acc_ref = refs[5 + 2 * sources :]
+    out_ref, m_ref, l_ref, acc_ref, *held, sems = refs[5 + 2 * sources :]
+    loads = [
+        pltpu.make_async_copy(source, target, sems.at[i])
+        for i, (source, target) in enumerate(zip(kv_refs, held))
+    ]
+    for load in loads:
+        load.start()
+    kv_refs = held
     width = heads * head_size
     halves = tokens // width
     rows = tokens // head_size
@@ -88,8 +95,16 @@
             else:
                 acc_ref[...] = acc_ref[...] * spread(rescales) + total
 
+        def arrive(source):
+            @pl.when(step == 0)
+            def _():
+                loads[2 * source].wait()
+                loads[2 * source + 1].wait()
+
+        arrive(0)
         visit(0)
         for source in range(1, sources):
+            arrive(source)
             last_doc = jnp.max(
                 kv_refs[2 * source][tokens + 3 * rows : tokens + 3 * rows + halves, :].astype(
                     jnp.float32
@@ -174,14 +189,16 @@
     return pl.pallas_call(
         kernel,
         out_shape=jax.ShapeDtypeStruct((tokens, width), jnp.bfloat16),
-        in_specs=[smem, smem] + [vmem] * (3 + len(blocks)),
+        in_specs=[smem, smem] + [vmem] * 3 + [pl.BlockSpec(memory_space=pltpu.HBM)] * len(blocks),
         out_specs=vmem,
         scratch_shapes=[
             pltpu.VMEM((heads, tile, 1), jnp.float32),
             pltpu.VMEM((heads, tile, 1), jnp.float32),
             pltpu.VMEM((tile, width), jnp.float32),
+            *[pltpu.VMEM(x.shape, x.dtype) for x in blocks],
+            pltpu.SemaphoreType.DMA((len(blocks),)),
         ],
-        compiler_params=pltpu.CompilerParams(vmem_limit_bytes=50 * 2**20),
+        compiler_params=pltpu.CompilerParams(vmem_limit_bytes=36 * 2**20),
         name="attention",
     )(valid, documents, queries, meta, head_gain[None, :], *blocks)
 

time: 295 us -> 296 us (level)
  no operation moved by 1% of the time
where the time goes in v6:
time: 296 us; the launch traced here: 295 us
  waiting for transfers between devices  145 us (49%)
  starting transfers between devices  49.8 us (17%)
  Pallas kernels  44.2 us (15%)
  blocking collectives  35.9 us (12%)
  local copies, waits for them, and re-layouts  10.8 us (4%)
  other arithmetic  8.54 us (3%)
    ppermute x10, waiting for transfers between devices, swap(): lax.ppermute(x, axis, [(i, i ^ bits) for i in range(lax.axis_size(axis))])  70.3 us
    all_to_all x1, blocking collectives, on_device(): arrived.append(lax.all_to_all(outbound[c], 'sp', 0, 0, tiled=True))  35.9 us
    pallas_call x2, Pallas kernels, on_device(): pl.pallas_call(expert, grid=(hidden_width // h_tile,), out_shape=[jax.Sha...  32.3 us
    all_to_all x1, waiting for transfers between devices, on_device(): arrived.append(lax.all_to_all(outbound[c], 'sp', 0, 0, tiled=True))  24.7 us
    all_to_all x2, waiting for transfers between devices, on_device(): lax.all_to_all(result.astype(jnp.bfloat16), 'sp', 0, 0, tiled=True)  24.1 us
    ppermute x6, waiting for transfers between devices, chain(): other.append(lax.ppermute(own[-1], 'sp', pairs))  16.6 us
    ppermute x4, starting transfers between devices, chain(): own.append(lax.ppermute(own[-1], 'sp', ahead))  16.3 us
    all_to_all x2, starting transfers between devices, on_device(): lax.all_to_all(result.astype(jnp.bfloat16), 'sp', 0, 0, tiled=True)  11.1 us
  transfers between devices with their start and end apart: 24, of which 10 were waited for; matrix products, arithmetic and copies ran while one was open for 3% of the time, Pallas kernels for 11%

profile of v6, /device:TPU:0, one launch (start us, length us, event | category | flops | bytes accessed | tf_op | source)
XLA Modules:
  0.0 294.7 jit_solution(4940387787181537876)
XLA Ops:
  2.5 5.0 %collective-permute-start.2 = (bf16[544,256]{1,0:T(8,128)(2,1)S(1)}, bf16[544,256]{1,0:T(8,128)(2,1)S(1)}, u32[]{:S(2)}, u32[]{:S(2)}) collective-permute-start(bf16[544,256]{1,0:T(8,128)(2,1)S(1)} %concatenate.7.refs_5_), channel_id=1, source_target_pairs={{0,8},{4,12},{8,16},{12,20},{16,24},{20,28},{1,9},{5,13},{9,17},{1... | collective-permute-start | bytes 835592 | tf_op jit(solution)/shard_map/ppermute | solution.py:163
  7.5 3.5 %collective-permute-start.3 = (bf16[512,256]{1,0:T(8,128)(2,1)}, bf16[512,256]{1,0:T(8,128)(2,1)S(1)}, u32[]{:S(2)}, u32[]{:S(2)}) collective-permute-start(bf16[512,256]{1,0:T(8,128)(2,1)} %refs_6_.1), channel_id=1, source_target_pairs={{0,8},{4,12},{8,16},{12,20},{16,24},{20,28},{1,9},{5,13},{9,17},{1... | collective-permute-start | bytes 786440 | tf_op jit(solution)/shard_map/ppermute | solution.py:163
  11.0 3.5 %collective-permute-done.2.refs_9_ = bf16[544,256]{1,0:T(8,128)(2,1)S(1)} collective-permute-done((bf16[544,256]{1,0:T(8,128)(2,1)S(1)}, bf16[544,256]{1,0:T(8,128)(2,1)S(1)}, u32[]{:S(2)}, u32[]{:S(2)}) %collective-permute-start.2) | collective-permute-done | bytes 278560 | tf_op jit(solution)/shard_map/ppermute | solution.py:163
  14.5 4.4 %collective-permute-start.6 = (bf16[544,256]{1,0:T(8,128)(2,1)S(1)}, bf16[544,256]{1,0:T(8,128)(2,1)S(1)}, u32[]{:S(2)}, u32[]{:S(2)}) collective-permute-start(bf16[544,256]{1,0:T(8,128)(2,1)S(1)} %collective-permute-done.2.refs_9_), channel_id=1, source_target_pairs={{0,8},{4,12},{8,16},{12,20},{16,24},{20,28},{1,9},{5,13},{9,17},{1... | collective-permute-start | bytes 835592 | tf_op jit(solution)/shard_map/ppermute | solution.py:163
  18.9 3.4 %collective-permute-start.1 = (bf16[512,256]{1,0:T(8,128)(2,1)}, bf16[512,256]{1,0:T(8,128)(2,1)S(1)}, u32[]{:S(2)}, u32[]{:S(2)}) collective-permute-start(bf16[512,256]{1,0:T(8,128)(2,1)} %refs_6_.1), channel_id=1, source_target_pairs={{0,4},{8,12},{16,20},{24,28},{1,5},{9,13},{17,21},{25,29},{2,6},{1... | collective-permute-start | bytes 786440 | tf_op jit(solution)/shard_map/ppermute | solution.py:164
  22.4 3.5 %collective-permute-start.7 = (bf16[512,256]{1,0:T(8,128)(2,1)S(1)}, bf16[512,256]{1,0:T(8,128)(2,1)S(1)}, u32[]{:S(2)}, u32[]{:S(2)}) collective-permute-start(bf16[512,256]{1,0:T(8,128)(2,1)S(1)} %collective-permute-done.3.refs_10_), channel_id=1, source_target_pairs={{0,8},{4,12},{8,16},{12,20},{16,24},{20,28},{1,9},{5,13},{9,17},{1... | collective-permute-start | bytes 786440 | tf_op jit(solution)/shard_map/ppermute | solution.py:163
  25.9 2.1 collective-permute-start
  28.1 1.3 collective-permute-start.8
  29.4 2.7 collective-permute-start.5
  35.0 13.3 %collective-permute-done.5.refs_12_ = bf16[512,256]{1,0:T(8,128)(2,1)S(1)} collective-permute-done((bf16[512,256]{1,0:T(8,128)(2,1)S(1)}, bf16[512,256]{1,0:T(8,128)(2,1)S(1)}, u32[]{:S(2)}, u32[]{:S(2)}) %collective-permute-start.5) | collective-permute-done | bytes 262176 | tf_op jit(solution)/shard_map/ppermute | solution.py:164
  48.3 2.8 collective-permute-done.9.refs_16_
  56.0 7.3 %attention.1 = bf16[512,256]{1,0:T(8,128)(2,1)} custom-call(s32[6]{0:T(128)S(1)} %convert_element_type.65.refs_0_, s32[512]{0:T(512)S(1)} %copy-done.9, bf16[512,256]{1,0:T(8,128)(2,1)S(1)} %copy-done.4, f32[512,8]{1,0:T(8,128)S(1)} %copy.24.refs_3_, f32[1,256]{1,0:T(1,128)S(1)} %bitcast.42, bf16[544,256]{1,0:T(8,128)(2,1)S(1)} %concatenate.7.refs_5_, ...), custom_call_target="tpu_custom_call" | custom-call | tf_op jit(solution)/shard_map/attention/pallas_call | solution.py:189
  63.4 3.4 %all-to-all-start = ((bf16[4,128,256]{2,1,0:T(8,128)(2,1)}), bf16[4,128,256]{2,1,0:T(8,128)(2,1)S(1)}, u32[]{:S(2)}, u32[]{:S(2)}) async-start(bf16[4,128,256]{2,1,0:T(8,128)(2,1)} %bitcast.10), calls=%async_computation | async-start | bytes 524288 | tf_op jit(solution)/shard_map/all_to_all | solution.py:359
  66.8 6.0 %all-to-all-done = bf16[4,128,256]{2,1,0:T(8,128)(2,1)S(1)} async-done(((bf16[4,128,256]{2,1,0:T(8,128)(2,1)}), bf16[4,128,256]{2,1,0:T(8,128)(2,1)S(1)}, u32[]{:S(2)}, u32[]{:S(2)}) %all-to-all-start) | async-done | bytes 262176 | tf_op jit(solution)/shard_map/all_to_all | solution.py:359
  72.8 2.2 copy-done
  75.0 2.5 project.1
  77.5 35.9 %all_to_all.63 = bf16[8,32,2048]{2,1,0:T(8,128)(2,1)S(1)} all-to-all(bf16[8,32,2048]{2,1,0:T(8,128)(2,1)S(1)} %bitcast.40), channel_id=1, replica_groups=mesh['sp'=8,'tp'=4] {'sp'}, dimensions={0} | all-to-all | bytes 2097152 | tf_op jit(solution)/shard_map/all_to_all | solution.py:384
  113.4 3.6 %all-to-all-start.1 = ((bf16[8,32,2048]{2,1,0:T(8,128)(2,1)}), bf16[8,32,2048]{2,1,0:T(8,128)(2,1)S(1)}, u32[]{:S(2)}, u32[]{:S(2)}) async-start(bf16[8,32,2048]{2,1,0:T(8,128)(2,1)} %bitcast.14), calls=%async_computation.1 | async-start | bytes 2097152 | tf_op jit(solution)/shard_map/all_to_all | solution.py:384
  117.8 24.7 %all-to-all-done.1 = bf16[8,32,2048]{2,1,0:T(8,128)(2,1)S(1)} async-done(((bf16[8,32,2048]{2,1,0:T(8,128)(2,1)}), bf16[8,32,2048]{2,1,0:T(8,128)(2,1)S(1)}, u32[]{:S(2)}, u32[]{:S(2)}) %all-to-all-start.1) | async-done | bytes 1048608 | tf_op jit(solution)/shard_map/all_to_all | solution.py:384
  143.8 22.0 %collective-permute-done.10.refs_1_ = bf16[256,2048]{1,0:T(8,128)(2,1)S(1)} collective-permute-done((bf16[256,2048]{1,0:T(8,128)(2,1)S(1)}, bf16[256,2048]{1,0:T(8,128)(2,1)S(1)}, u32[]{:S(2)}, u32[]{:S(2)}) %collective-permute-start.10) | collective-permute-done | bytes 1048608 | tf_op jit(solution)/shard_map/ppermute | solution.py:207
  165.8 2.0 copy-done.11
  167.8 15.6 %expert.3 = (bf16[512,2048]{1,0:T(8,128)(2,1)S(1)}, bf16[512,2048]{1,0:T(8,128)(2,1)S(1)}) custom-call(bf16[256,2048]{1,0:T(8,128)(2,1)S(1)} %bitcast.39, bf16[256,2048]{1,0:T(8,128)(2,1)S(1)} %collective-permute-done.15.refs_1_, bf16[256,2048]{1,0:T(8,128)(2,1)S(1)} %collective-permute-done.16.refs_2_, ...), custom_call_target="tpu_custom_call" | custom-call | flops 11274289152 | bytes 19398656 | tf_op jit(solution)/shard_map/expert/pallas_call | solution.py:394
  184.0 16.8 %expert.2 = (bf16[512,2048]{1,0:T(8,128)(2,1)S(1)}, bf16[512,2048]{1,0:T(8,128)(2,1)}) custom-call(bf16[256,2048]{1,0:T(8,128)(2,1)S(1)} %bitcast.36, bf16[256,2048]{1,0:T(8,128)(2,1)S(1)} %collective-permute-done.10.refs_1_, bf16[256,2048]{1,0:T(8,128)(2,1)S(1)} %collective-permute-done.11.refs_2_, bf16[256,2048]{1,0:T(8,128)(2,1)S(1)} %collective-permute-done.12.refs_3_, ...), custom_call_target="tpu_custom_call" | custom-call | flops 11274289152 | bytes 19398656 | tf_op jit(solution)/shard_map/expert/pallas_call | solution.py:394
  202.1 24.7 %collective-permute-done.19 = bf16[256,2048]{1,0:T(8,128)(2,1)S(1)} collective-permute-done((bf16[256,2048]{1,0:T(8,128)(2,1)S(1)}, bf16[256,2048]{1,0:T(8,128)(2,1)S(1)}, u32[]{:S(2)}, u32[]{:S(2)}) %collective-permute-start.19) | collective-permute-done | bytes 1048608 | tf_op jit(solution)/shard_map/ppermute | solution.py:207
  226.9 1.6 add_convert_fusion
  228.5 5.2 %all-to-all-start.4 = ((bf16[8,32,2048]{2,1,0:T(8,128)(2,1)}), bf16[8,32,2048]{2,1,0:T(8,128)(2,1)S(1)}, u32[]{:S(2)}, u32[]{:S(2)}) async-start(bf16[8,32,2048]{2,1,0:T(8,128)(2,1)} %bitcast.45), calls=%async_computation.4 | async-start | bytes 2097152 | tf_op jit(solution)/shard_map/all_to_all | solution.py:429
  233.7 1.6 add_convert_fusion.3
  236.2 23.6 %collective-permute-done.14 = bf16[256,2048]{1,0:T(8,128)(2,1)S(1)} collective-permute-done((bf16[256,2048]{1,0:T(8,128)(2,1)S(1)}, bf16[256,2048]{1,0:T(8,128)(2,1)S(1)}, u32[]{:S(2)}, u32[]{:S(2)}) %collective-permute-start.14) | collective-permute-done | bytes 1048608 | tf_op jit(solution)/shard_map/ppermute | solution.py:207
  259.8 2.7 add_convert_fusion.2
  262.5 5.9 %all-to-all-start.2 = ((bf16[8,32,2048]{2,1,0:T(8,128)(2,1)}), bf16[8,32,2048]{2,1,0:T(8,128)(2,1)S(1)}, u32[]{:S(2)}, u32[]{:S(2)}) async-start(bf16[8,32,2048]{2,1,0:T(8,128)(2,1)} %bitcast.46), calls=%async_computation.2 | async-start | bytes 2097152 | tf_op jit(solution)/shard_map/all_to_all | solution.py:429
  268.6 24.1 %all-to-all-done.2 = bf16[8,32,2048]{2,1,0:T(8,128)(2,1)S(1)} async-done(((bf16[8,32,2048]{2,1,0:T(8,128)(2,1)}), bf16[8,32,2048]{2,1,0:T(8,128)(2,1)S(1)}, u32[]{:S(2)}, u32[]{:S(2)}) %all-to-all-start.2) | async-done | bytes 1048608 | tf_op jit(solution)/shard_map/all_to_all | solution.py:429
  292.7 2.0 combine.1
  (74 shorter events, 15.6 us)
Async XLA Ops:
  2.5 12.0 %collective-permute-start.2 = (bf16[544,256]{1,0:T(8,128)(2,1)S(1)}, bf16[544,256]{1,0:T(8,128)(2,1)S(1)}, u32[]{:S(2)}, u32[]{:S(2)}) collective-permute-start(bf16[544,256]{1,0:T(8,128)(2,1)S(1)} %concatenate.7.refs_5_), channel_id=1, source_target_pairs={{0,8},{4,12},{8,16},{12,20},{16,24},{20,28},{1,9},{5,13},{9,17},{1... | collective-permute-start | bytes 835592 | tf_op jit(solution)/shard_map/ppermute | solution.py:163
  7.5 14.9 %collective-permute-start.3 = (bf16[512,256]{1,0:T(8,128)(2,1)}, bf16[512,256]{1,0:T(8,128)(2,1)S(1)}, u32[]{:S(2)}, u32[]{:S(2)}) collective-permute-start(bf16[512,256]{1,0:T(8,128)(2,1)} %refs_6_.1), channel_id=1, source_target_pairs={{0,8},{4,12},{8,16},{12,20},{16,24},{20,28},{1,9},{5,13},{9,17},{1... | collective-permute-start | bytes 786440 | tf_op jit(solution)/shard_map/ppermute | solution.py:163
  14.5 13.5 %collective-permute-start.6 = (bf16[544,256]{1,0:T(8,128)(2,1)S(1)}, bf16[544,256]{1,0:T(8,128)(2,1)S(1)}, u32[]{:S(2)}, u32[]{:S(2)}) collective-permute-start(bf16[544,256]{1,0:T(8,128)(2,1)S(1)} %collective-permute-done.2.refs_9_), channel_id=1, source_target_pairs={{0,8},{4,12},{8,16},{12,20},{16,24},{20,28},{1,9},{5,13},{9,17},{1... | collective-permute-start | bytes 835592 | tf_op jit(solution)/shard_map/ppermute | solution.py:163
  18.9 10.5 %collective-permute-start.1 = (bf16[512,256]{1,0:T(8,128)(2,1)}, bf16[512,256]{1,0:T(8,128)(2,1)S(1)}, u32[]{:S(2)}, u32[]{:S(2)}) collective-permute-start(bf16[512,256]{1,0:T(8,128)(2,1)} %refs_6_.1), channel_id=1, source_target_pairs={{0,4},{8,12},{16,20},{24,28},{1,5},{9,13},{17,21},{25,29},{2,6},{1... | collective-permute-start | bytes 786440 | tf_op jit(solution)/shard_map/ppermute | solution.py:164
  22.4 9.7 %collective-permute-start.7 = (bf16[512,256]{1,0:T(8,128)(2,1)S(1)}, bf16[512,256]{1,0:T(8,128)(2,1)S(1)}, u32[]{:S(2)}, u32[]{:S(2)}) collective-permute-start(bf16[512,256]{1,0:T(8,128)(2,1)S(1)} %collective-permute-done.3.refs_10_), channel_id=1, source_target_pairs={{0,8},{4,12},{8,16},{12,20},{16,24},{20,28},{1,9},{5,13},{9,17},{1... | collective-permute-start | bytes 786440 | tf_op jit(solution)/shard_map/ppermute | solution.py:163
  25.9 9.1 %collective-permute-start = (bf16[544,256]{1,0:T(8,128)(2,1)S(1)}, bf16[544,256]{1,0:T(8,128)(2,1)S(1)}, u32[]{:S(2)}, u32[]{:S(2)}) collective-permute-start(bf16[544,256]{1,0:T(8,128)(2,1)S(1)} %concatenate.7.refs_5_), channel_id=1, source_target_pairs={{0,4},{8,12},{16,20},{24,28},{1,5},{9,13},{17,21},{25,29},{2,6},{1... | collective-permute-start | bytes 835592 | tf_op jit(solution)/shard_map/ppermute | solution.py:164
  28.0 20.3 %collective-permute-start.4 = (bf16[544,256]{1,0:T(8,128)(2,1)S(1)}, bf16[544,256]{1,0:T(8,128)(2,1)S(1)}, u32[]{:S(2)}, u32[]{:S(2)}) collective-permute-start(bf16[544,256]{1,0:T(8,128)(2,1)S(1)} %collective-permute-done.2.refs_9_), channel_id=1, source_target_pairs={{0,4},{8,12},{16,20},{24,28},{4,0},{12,8},{20,16},{28,24},{1,5},{9... | collective-permute-start | bytes 835592 | tf_op jit(solution)/shard_map/ppermute | solution.py:164
  28.1 23.7 %collective-permute-start.8 = (bf16[544,256]{1,0:T(8,128)(2,1)S(1)}, bf16[544,256]{1,0:T(8,128)(2,1)S(1)}, u32[]{:S(2)}, u32[]{:S(2)}) collective-permute-start(bf16[544,256]{1,0:T(8,128)(2,1)S(1)} %collective-permute-done.6.refs_13_), channel_id=1, source_target_pairs={{4,0},{12,8},{20,16},{28,24},{5,1},{13,9},{21,17},{29,25},{6,2},{1... | collective-permute-start | bytes 835592 | tf_op jit(solution)/shard_map/ppermute | solution.py:164
  29.4 18.9 %collective-permute-start.5 = (bf16[512,256]{1,0:T(8,128)(2,1)S(1)}, bf16[512,256]{1,0:T(8,128)(2,1)S(1)}, u32[]{:S(2)}, u32[]{:S(2)}) collective-permute-start(bf16[512,256]{1,0:T(8,128)(2,1)S(1)} %collective-permute-done.3.refs_10_), channel_id=1, source_target_pairs={{0,4},{8,12},{16,20},{24,28},{4,0},{12,8},{20,16},{28,24},{1,5},{9... | collective-permute-start | bytes 786440 | tf_op jit(solution)/shard_map/ppermute | solution.py:164
  32.1 19.0 %collective-permute-start.9 = (bf16[512,256]{1,0:T(8,128)(2,1)S(1)}, bf16[512,256]{1,0:T(8,128)(2,1)S(1)}, u32[]{:S(2)}, u32[]{:S(2)}) collective-permute-start(bf16[512,256]{1,0:T(8,128)(2,1)S(1)} %collective-permute-done.7.refs_14_), channel_id=1, source_target_pairs={{4,0},{12,8},{20,16},{28,24},{5,1},{13,9},{21,17},{29,25},{6,2},{1... | collective-permute-start | bytes 786440 | tf_op jit(solution)/shard_map/ppermute | solution.py:164
  56.0 10.8 %copy-start.13 = (s32[128,2]{0,1:T(2,128)S(1)}, s32[128,2]{0,1:T(2,128)}, u32[]{:S(2)}) copy-start(s32[128,2]{0,1:T(2,128)} %param.23) | copy-start | bytes 3076
  56.0 16.8 %copy-start.3 = (bf16[128,2048]{1,0:T(8,128)(2,1)S(1)}, bf16[128,2048]{1,0:T(8,128)(2,1)}, u32[]{:S(2)}) copy-start(bf16[128,2048]{1,0:T(8,128)(2,1)} %refs_2_.4) | copy-start | bytes 1572868
  56.0 16.8 %copy-start.8 = (f32[2048]{0:T(1024)S(1)}, f32[2048]{0:T(1024)}, u32[]{:S(2)}) copy-start(f32[2048]{0:T(1024)} %param.22) | copy-start | bytes 24580
  63.4 9.4 %all-to-all-start = ((bf16[4,128,256]{2,1,0:T(8,128)(2,1)}), bf16[4,128,256]{2,1,0:T(8,128)(2,1)S(1)}, u32[]{:S(2)}, u32[]{:S(2)}) async-start(bf16[4,128,256]{2,1,0:T(8,128)(2,1)} %bitcast.10), calls=%async_computation | async-start | bytes 524288 | tf_op jit(solution)/shard_map/all_to_all | solution.py:359
  72.8 2.2 copy-start
  77.5 35.9 %copy-start.1 = (bf16[128,2048]{1,0:T(8,128)(2,1)}, bf16[128,2048]{1,0:T(8,128)(2,1)S(1)}, u32[]{:S(2)}) copy-start(bf16[128,2048]{1,0:T(8,128)(2,1)S(1)} %get-tuple-element.12.refs_0_) | copy-start | bytes 1572868
  113.4 29.1 %all-to-all-start.1 = ((bf16[8,32,2048]{2,1,0:T(8,128)(2,1)}), bf16[8,32,2048]{2,1,0:T(8,128)(2,1)S(1)}, u32[]{:S(2)}, u32[]{:S(2)}) async-start(bf16[8,32,2048]{2,1,0:T(8,128)(2,1)} %bitcast.14), calls=%async_computation.1 | async-start | bytes 2097152 | tf_op jit(solution)/shard_map/all_to_all | solution.py:384
  117.0 26.4 %collective-permute-start.15 = (bf16[256,2048]{1,0:T(8,128)(2,1)S(1)}, bf16[256,2048]{1,0:T(8,128)(2,1)S(1)}, u32[]{:S(2)}, u32[]{:S(2)}) collective-permute-start(bf16[256,2048]{1,0:T(8,128)(2,1)S(1)} %bitcast.37), channel_id=1, source_target_pairs={{0,2},{1,3},{2,0},{3,1},{4,6},{5,7},{6,4},{7,5},{8,10},{9,11},{10,... | collective-permute-start | bytes 3145736 | tf_op jit(solution)/shard_map/ppermute | solution.py:207
  142.5 23.3 %collective-permute-start.10 = (bf16[256,2048]{1,0:T(8,128)(2,1)S(1)}, bf16[256,2048]{1,0:T(8,128)(2,1)S(1)}, u32[]{:S(2)}, u32[]{:S(2)}) collective-permute-start(bf16[256,2048]{1,0:T(8,128)(2,1)S(1)} %bitcast.34), channel_id=1, source_target_pairs={{0,2},{1,3},{2,0},{3,1},{4,6},{5,7},{6,4},{7,5},{8,10},{9,11},{10,... | collective-permute-start | bytes 3145736 | tf_op jit(solution)/shard_map/ppermute | solution.py:207
  143.3 22.5 %collective-permute-start.16 = (bf16[256,2048]{1,0:T(8,128)(2,1)S(1)}, bf16[256,2048]{1,0:T(8,128)(2,1)S(1)}, u32[]{:S(2)}, u32[]{:S(2)}) collective-permute-start(bf16[256,2048]{1,0:T(8,128)(2,1)S(1)} %bitcast.38), channel_id=1, source_target_pairs={{0,1},{1,0},{2,3},{3,2},{4,5},{5,4},{6,7},{7,6},{8,9},{9,8},{10,11... | collective-permute-start | bytes 3145736 | tf_op jit(solution)/shard_map/ppermute | solution.py:207
  143.3 22.5 %collective-permute-start.17 = (bf16[256,2048]{1,0:T(8,128)(2,1)S(1)}, bf16[256,2048]{1,0:T(8,128)(2,1)S(1)}, u32[]{:S(2)}, u32[]{:S(2)}) collective-permute-start(bf16[256,2048]{1,0:T(8,128)(2,1)S(1)} %collective-permute-done.15.refs_1_), channel_id=1, source_target_pairs={{0,1},{1,0},{2,3},{3,2},{4,5},{5,4},{6,7},{7,6},{8,9},{9,8},{10,11... | collective-permute-start | bytes 3145736 | tf_op jit(solution)/shard_map/ppermute | solution.py:207
  143.8 40.2 %collective-permute-start.11 = (bf16[256,2048]{1,0:T(8,128)(2,1)S(1)}, bf16[256,2048]{1,0:T(8,128)(2,1)S(1)}, u32[]{:S(2)}, u32[]{:S(2)}) collective-permute-start(bf16[256,2048]{1,0:T(8,128)(2,1)S(1)} %bitcast.35), channel_id=1, source_target_pairs={{0,1},{1,0},{2,3},{3,2},{4,5},{5,4},{6,7},{7,6},{8,9},{9,8},{10,11... | collective-permute-start | bytes 3145736 | tf_op jit(solution)/shard_map/ppermute | solution.py:207
  165.8 18.2 %collective-permute-start.12 = (bf16[256,2048]{1,0:T(8,128)(2,1)S(1)}, bf16[256,2048]{1,0:T(8,128)(2,1)S(1)}, u32[]{:S(2)}, u32[]{:S(2)}) collective-permute-start(bf16[256,2048]{1,0:T(8,128)(2,1)S(1)} %collective-permute-done.10.refs_1_), channel_id=1, source_target_pairs={{0,1},{1,0},{2,3},{3,2},{4,5},{5,4},{6,7},{7,6},{8,9},{9,8},{10,11... | collective-permute-start | bytes 3145736 | tf_op jit(solution)/shard_map/ppermute | solution.py:207
  167.8 16.1 %copy-start.12 = (bf16[1,2048,896]{2,1,0:T(8,128)(2,1)S(1)}, bf16[1,2048,896]{2,1,0:T(8,128)(2,1)}, u32[]{:S(2)}) copy-start(bf16[1,2048,896]{2,1,0:T(8,128)(2,1)} %param.25) | copy-start | bytes 11010052
  183.4 17.5 %collective-permute-start.18 = (bf16[512,2048]{1,0:T(8,128)(2,1)S(1)}, bf16[512,2048]{1,0:T(8,128)(2,1)S(1)}, u32[]{:S(2)}, u32[]{:S(2)}) collective-permute-start(bf16[512,2048]{1,0:T(8,128)(2,1)S(1)} %get-tuple-element.18), channel_id=1, source_target_pairs={{0,1},{1,0},{2,3},{3,2},{4,5},{5,4},{6,7},{7,6},{8,9},{9,8},{10,11... | collective-permute-start | bytes 6291464 | tf_op jit(solution)/shard_map/ppermute | solution.py:207
  200.8 32.9 %collective-permute-start.13 = (bf16[512,2048]{1,0:T(8,128)(2,1)}, bf16[512,2048]{1,0:T(8,128)(2,1)}, u32[]{:S(2)}, u32[]{:S(2)}) collective-permute-start(bf16[512,2048]{1,0:T(8,128)(2,1)} %get-tuple-element.15), channel_id=1, source_target_pairs={{0,1},{1,0},{2,3},{3,2},{4,5},{5,4},{6,7},{7,6},{8,9},{9,8},{10,11... | collective-permute-start | bytes 6291464 | tf_op jit(solution)/shard_map/ppermute | solution.py:207
  201.3 25.6 %collective-permute-start.19 = (bf16[256,2048]{1,0:T(8,128)(2,1)S(1)}, bf16[256,2048]{1,0:T(8,128)(2,1)S(1)}, u32[]{:S(2)}, u32[]{:S(2)}) collective-permute-start(bf16[256,2048]{1,0:T(8,128)(2,1)S(1)} %add_convert_fusion.1), channel_id=1, source_target_pairs={{0,2},{1,3},{2,0},{3,1},{4,6},{5,7},{6,4},{7,5},{8,10},{9,11},{10,... | collective-permute-start | bytes 3145736 | tf_op jit(solution)/shard_map/ppermute | solution.py:207
  228.5 34.0 %all-to-all-start.4 = ((bf16[8,32,2048]{2,1,0:T(8,128)(2,1)}), bf16[8,32,2048]{2,1,0:T(8,128)(2,1)S(1)}, u32[]{:S(2)}, u32[]{:S(2)}) async-start(bf16[8,32,2048]{2,1,0:T(8,128)(2,1)} %bitcast.45), calls=%async_computation.4 | async-start | bytes 2097152 | tf_op jit(solution)/shard_map/all_to_all | solution.py:429
  235.3 24.5 %collective-permute-start.14 = (bf16[256,2048]{1,0:T(8,128)(2,1)S(1)}, bf16[256,2048]{1,0:T(8,128)(2,1)S(1)}, u32[]{:S(2)}, u32[]{:S(2)}) collective-permute-start(bf16[256,2048]{1,0:T(8,128)(2,1)S(1)} %add_convert_fusion.3), channel_id=1, source_target_pairs={{0,2},{1,3},{2,0},{3,1},{4,6},{5,7},{6,4},{7,5},{8,10},{9,11},{10,... | collective-permute-start | bytes 3145736 | tf_op jit(solution)/shard_map/ppermute | solution.py:207
  262.5 6.0 %copy-start.14 = (f32[128,2]{0,1:T(2,128)S(1)}, f32[128,2]{0,1:T(2,128)}, u32[]{:S(2)}) copy-start(f32[128,2]{0,1:T(2,128)} %param.24) | copy-start | bytes 3076
  262.5 30.2 %copy-start.2 = (bf16[128,2048]{1,0:T(8,128)(2,1)S(1)}, bf16[128,2048]{1,0:T(8,128)(2,1)}, u32[]{:S(2)}) copy-start(bf16[128,2048]{1,0:T(8,128)(2,1)} %copy-done.1) | copy-start | bytes 1572868
  262.5 30.2 %all-to-all-start.2 = ((bf16[8,32,2048]{2,1,0:T(8,128)(2,1)}), bf16[8,32,2048]{2,1,0:T(8,128)(2,1)S(1)}, u32[]{:S(2)}, u32[]{:S(2)}) async-start(bf16[8,32,2048]{2,1,0:T(8,128)(2,1)} %bitcast.46), calls=%async_computation.2 | async-start | bytes 2097152 | tf_op jit(solution)/shard_map/all_to_all | solution.py:429
  (7 other events, 7.0 us)
